TPU v7x, 256 devices: a whole 4x4x8 slice. The times are simulated.
256 devices in a mesh: sp: 32 (over z, y), dp: 8 (over x, core).
Axes of the slice: x: 4, y: 4, z: 8, core: 2. Of those that a mesh axis runs over, the one named last changes fastest.
Arguments:
- cotangent: bfloat16 [8, 8192, 4096], P('dp', 'sp'), may hold values from -6 to 6
- up_pre: bfloat16 [8, 8192, 4096], P('dp', 'sp'), may hold values from -6 to 6
- value_pre: bfloat16 [8, 8192, 4096], P('dp', 'sp'), may hold values from -6 to 6
- spatial_weight: bfloat16 [32, 1024, 1024], P('sp', 'dp'), may hold values from -0.1875 to 0.1875
- spatial_bias: float32 [32, 1024], P('sp'), may hold values from 0.5 to 1.5
- value_gain: float32 [4096], replicated, may hold values from 0.1 to 1.9
Outputs:
- up_grad: bfloat16 [8, 8192, 4096], P('dp', 'sp')
- value_grad: bfloat16 [8, 8192, 4096], P('dp', 'sp')
- weight_grad: float32 [32, 1024, 1024], P('sp', 'dp')
- bias_grad: float32 [32, 1024], P('sp', 'dp')
- gain_grad: float32 [4096], replicated
All inputs are finite; a program needn't handle non-finite values.
Results may differ from a plain program's by a relative error of at most 0.0064.
Values may be sent and summed in bfloat16 or wider, within the bound.
No kernel may reach another device: no remote copies, remote signals or barrier semaphores. Data moves between devices by JAX's collectives and lax.ppermute only.
A program may use at most 128 MiB of HBM per device.

v0:
```python
import functools
import math

import jax
import jax.numpy as jnp
from jax import lax
from jax.sharding import Mesh
from jax.sharding import PartitionSpec as P

SP = ("sp_0", "sp_1")
DP = ("dp_0", "dp_1")
SP_DP = ("sp_0", "sp_1", "dp_0", "dp_1")


norm_floor = 0.5
root_half = 1.0 / math.sqrt(2.0)
inv_root_tau = 1.0 / math.sqrt(2.0 * math.pi)


def joined_along(blocks, dim):
    blocks = jnp.moveaxis(blocks, 0, dim)
    shape = blocks.shape
    return blocks.reshape(*shape[:dim], shape[dim] * shape[dim + 1], *shape[dim + 2 :])


def from_everyone(shard, axis):
    copies = jnp.broadcast_to(shard, (lax.axis_size(axis), *shard.shape))
    return lax.all_to_all(copies, axis, split_axis=0, concat_axis=0, tiled=True)


def gathered_copies(shard, axis, dim):
    return joined_along(from_everyone(shard, axis), dim)


def in_one_piece(arrays, axis, dim, along):
    columns = [a.reshape(*a.shape[:along], -1) for a in arrays]
    both = jnp.concatenate(columns, axis=along)
    result, at, done = (lax.psum_scatter(both, axis, scatter_dimension=dim, tiled=True), 0, [])
    for a, column in zip(arrays, columns):
        slab = result[..., at : at + column.shape[along]]
        done.append(slab.reshape(*slab.shape[:along], *a.shape[along:]))
        at += column.shape[along]
    return tuple(done)


def sent_together(arrays, axis, split_dim, concat_dim, along):
    widths = [a.shape[along] for a in arrays]
    both = jnp.concatenate(arrays, axis=along)
    result = lax.all_to_all(both, axis, split_axis=split_dim, concat_axis=concat_dim, tiled=True)
    return tuple(jnp.split(result, [sum(widths[:k]) for k in range(1, len(widths))], axis=along))


def by_axis(shard, axes):
    return functools.reduce(lax.psum, axes, shard)


def gelu_slope(values):
    return (
        0.5 * (1.0 + jax.scipy.special.erf(values * root_half))
        + values * jnp.exp(-0.5 * values * values) * inv_root_tau
    )


def shards(cotangent, up_pre, value_pre, spatial_weight, spatial_bias, value_gain):
    tok_rows = cotangent.shape[1]
    model_width = cotangent.shape[2]
    grp_dev = spatial_weight.shape[0]
    block_len = spatial_weight.shape[2]
    sp_count = lax.axis_size(SP)
    all_groups = grp_dev * sp_count
    group_dim = model_width // all_groups
    seq_len = tok_rows * sp_count
    blocks = seq_len // block_len
    grad_tok = cotangent[0].astype(jnp.float32)
    up_arg = up_pre[0].astype(jnp.float32)
    value_arg = value_pre[0].astype(jnp.float32)
    up_act = lax.optimization_barrier(jax.nn.gelu(up_arg, approximate=False).astype(jnp.bfloat16))
    value_act = jax.nn.gelu(value_arg, approximate=False)
    inv_rms = lax.rsqrt(jnp.mean(value_act * value_act, axis=-1, keepdims=True) + norm_floor)
    normed = value_act * inv_rms
    value_norm = (normed * value_gain).astype(jnp.bfloat16)
    split_shape = (tok_rows, all_groups, group_dim)
    gate_tok = (grad_tok * up_act.astype(jnp.float32)).astype(jnp.bfloat16)
    gate_heads, value_heads = (
        lax.all_to_all(gate_tok.reshape(split_shape), SP, split_axis=1, concat_axis=0, tiled=True),
        lax.all_to_all(
            value_norm.reshape(split_shape), SP, split_axis=1, concat_axis=0, tiled=True
        ),
    )
    block_shape = (blocks, block_len, grp_dev, group_dim)
    gate_blocks = gate_heads.reshape(block_shape)
    value_blocks = value_heads.reshape(block_shape)
    portion = gathered_copies(spatial_weight, DP, 1)
    mixed_rows = jnp.einsum(
        "gpq,nqgc->npgc", portion, value_blocks, preferred_element_type=jnp.float32
    )
    mixed_acc = mixed_rows
    back_acc = jnp.einsum(
        "gpq,npgc->nqgc", portion, gate_blocks, preferred_element_type=jnp.float32
    )
    mixed_acc, back_acc = (mixed_acc, back_acc)
    mixed_out = lax.optimization_barrier(
        (mixed_acc + spatial_bias.T[None, :, :, None]).astype(jnp.bfloat16)
    )
    back_heads = back_acc.astype(jnp.bfloat16)
    weight_term = jnp.einsum(
        "npgc,nqgc->gpq", gate_blocks, value_blocks, preferred_element_type=jnp.float32
    )
    bias_term = jnp.sum(gate_blocks, axis=(0, 3), dtype=jnp.float32).T
    weight_grad, bias_grad = in_one_piece((weight_term, bias_term), DP, 1, 2)
    heads_shape = (seq_len, grp_dev, group_dim)
    first_heads = mixed_out.reshape(heads_shape)
    first_tok, back_tok = sent_together((first_heads, back_heads.reshape(heads_shape)), SP, 0, 1, 2)
    up_mid = lax.optimization_barrier(
        (grad_tok * first_tok.reshape(tok_rows, model_width).astype(jnp.float32)).astype(
            jnp.bfloat16
        )
    )
    up_grad = (up_mid.astype(jnp.float32) * gelu_slope(up_arg)).astype(jnp.bfloat16)[None]
    back_full = back_tok.reshape(tok_rows, model_width).astype(jnp.float32)
    gain_grad = by_axis(jnp.sum(back_full * normed, axis=0), SP_DP)
    scaled = back_full * value_gain
    value_slope = inv_rms * scaled - inv_rms**3 * value_act * jnp.mean(
        scaled * value_act, axis=-1, keepdims=True
    )
    value_grad = (value_slope * gelu_slope(value_arg)).astype(jnp.bfloat16)[None]
    return (up_grad, value_grad, weight_grad, bias_grad, gain_grad)


def solution(mesh):
    torus = Mesh(mesh.devices.reshape(8, 4, 4, 2), ("sp_0", "sp_1", "dp_0", "dp_1"))
    in_specs = (
        P(DP, SP, None),
        P(DP, SP, None),
        P(DP, SP, None),
        P(SP, DP, None),
        P(SP, None),
        P(),
    )
    out_specs = (P(DP, SP, None), P(DP, SP, None), P(SP, DP, None), P(SP, DP), P())
    return jax.shard_map(
        shards, mesh=torus, in_specs=in_specs, out_specs=out_specs, check_vma=False
    )
```

profile of v0, /device:TPU:1, one launch (start us, length us, event | category | flops | bytes accessed | tf_op | source)
XLA Modules:
  0.0 442.2 jit_solution(10742665178344789631)
XLA Ops:
  9.7 7.4 %all-to-all-start.1 = ((bf16[8,1,128,1024]{3,2,1,0:T(8,128)(2,1)}), bf16[8,1,128,1024]{3,2,1,0:T(8,128)(2,1)}, u32[]{:S(2)}, u32[]{:S(2)}) async-start(bf16[8,1,128,1024]{3,2,1,0:T(8,128)(2,1)} %broadcast_in_dim.4), calls=%async_computation.1 | async-start | bytes 4194304 | tf_op jit(solution)/shard_map/all_to_all | solution.py:28
  20.4 9.4 %fusion.7 = f32[256]{0:T(256)S(1)} fusion(bf16[1,256,4096]{1,2,0:T(8,128)(2,1)S(1)} %copy.47), kind=kLoop, calls=%fused_computation.26 | loop fusion | flops 70254336 | bytes 2098176 | tf_op jit(solution)/shard_map/reduce_sum | solution.py:79
  29.7 4.1 copy.51
  33.8 10.9 %fusion.10 = bf16[256,4096]{0,1:T(8,128)(2,1)} fusion(bf16[1,256,4096]{1,2,0:T(8,128)(2,1)} %copy.51), kind=kLoop, calls=%fused_computation.29 | loop fusion | flops 69206016 | bytes 4194304 | tf_op jit(solution)/shard_map/convert_element_type | solution.py:77
  44.7 4.1 copy.46
  48.8 4.1 fusion
  52.9 9.7 %all-to-all-start.2 = ((bf16[256,32,128]{0,2,1:T(8,128)(2,1)}), bf16[256,32,128]{0,2,1:T(8,128)(2,1)}, u32[]{:S(2)}, u32[]{:S(2)}) async-start(bf16[256,32,128]{0,2,1:T(8,128)(2,1)} %bitcast.156), calls=%async_computation.2 | async-start | bytes 4194304 | tf_op jit(solution)/shard_map/all_to_all | solution.py:85
  63.3 10.0 %multiply_convert_fusion = (bf16[256,32,128]{0,2,1:T(8,128)(2,1)}, f32[256,32,128]{0,2,1:T(8,128)}) fusion(f32[32,128]{1,0:T(8,128)S(1)} %bitcast.164, f32[256]{0:T(256)S(1)} %get-tuple-element.39, f32[256,32,128]{0,2,1:T(8,128)S(1)} %bitcast.154, f32[256,32,128]{0,2,1:T(8,128)S(1)} %bitcast.153), kind=kLoop, calls=%fused_computation.141 | loop fusion | flops 67108864 | bytes 14697472 | tf_op jit(solution)/shard_map/convert_element_type | solution.py:81
  73.4 37.7 %all-to-all-done.2 = bf16[256,32,128]{0,2,1:T(8,128)(2,1)} async-done(((bf16[256,32,128]{0,2,1:T(8,128)(2,1)}), bf16[256,32,128]{0,2,1:T(8,128)(2,1)}, u32[]{:S(2)}, u32[]{:S(2)}) %all-to-all-start.2) | async-done | bytes 2097184 | tf_op jit(solution)/shard_map/all_to_all | solution.py:85
  111.1 7.6 %all-to-all-start = ((bf16[256,32,128]{0,2,1:T(8,128)(2,1)}), bf16[256,32,128]{0,2,1:T(8,128)(2,1)}, u32[]{:S(2)}, u32[]{:S(2)}) async-start(bf16[256,32,128]{0,2,1:T(8,128)(2,1)} %get-tuple-element.32), calls=%async_computation | async-start | bytes 4194304 | tf_op jit(solution)/shard_map/all_to_all | solution.py:86
  118.7 4.1 copy.52
  122.7 5.9 %convert_bitcast_fusion = bf16[8,1024,1,128]{1,3,0,2:T(8,128)(2,1)} fusion(bf16[8,1024,128]{2,1,0:T(8,128)(2,1)} %bitcast.159, bf16[1024,1024,1]{1,0,2:T(8,128)(2,1)} %bitcast.11), kind=kOutput, calls=%fused_computation.158 | convolution fusion | flops 2148532224 | bytes 6291456 | tf_op jit(solution)/shard_map/gpq,npgc->nqgc/dot_general | solution.py:98
  128.6 3.9 copy.54
  132.5 34.3 %all-to-all-done = bf16[256,32,128]{0,2,1:T(8,128)(2,1)} async-done(((bf16[256,32,128]{0,2,1:T(8,128)(2,1)}), bf16[256,32,128]{0,2,1:T(8,128)(2,1)}, u32[]{:S(2)}, u32[]{:S(2)}) %all-to-all-start) | async-done | bytes 2097184 | tf_op jit(solution)/shard_map/all_to_all | solution.py:86
  166.8 4.1 copy.48
  170.9 6.0 %fusion.120 = bf16[8,1024,1,128]{1,3,0,2:T(8,128)(2,1)} fusion(f32[1024]{0:T(1024)S(1)} %bitcast.168, bf16[8,1024,128]{2,1,0:T(8,128)(2,1)} %bitcast.161, bf16[1024,1024,1]{1,0,2:T(8,128)(2,1)} %bitcast.11), kind=kOutput, calls=%fused_computation.160 | convolution fusion | flops 2149580800 | bytes 6295552 | tf_op jit(solution)/shard_map/gpq,nqgc->npgc/dot_general | solution.py:94
  176.8 3.9 copy.50
  180.7 4.6 %pad_maximum_fusion.1 = bf16[8192,1,256]{2,0,1:T(8,128)(2,1)} fusion(bf16[8192,1,128]{2,0,1:T(8,128)(2,1)} %bitcast.157, bf16[8192,1,128]{2,0,1:T(8,128)(2,1)} %bitcast.158), kind=kLoop, calls=%fused_computation.79 | loop fusion | flops 8388608 | bytes 8388608 | tf_op jit(solution)/shard_map/concatenate | solution.py:48
  185.9 6.7 %reduce.6 = bf16[8192,256]{1,0:T(8,128)(2,1)} reduce(bf16[8192,1,256]{2,0,1:T(8,128)(2,1)} %pad_maximum_fusion.1, bf16[]{:T(256)} %broadcast.719), dimensions={1}, to_apply=%copy.55.reduce_sub_computation | reduce | bytes 8388610 | tf_op jit(solution)/shard_map/concatenate | solution.py:48
  192.6 6.9 %reshape.207 = bf16[32,2,32768]{2,1,0:T(2,128)(2,1)} reshape(bf16[8192,256]{1,0:T(8,128)(2,1)} %reduce.6) | data formatting | bytes 8388608
  199.5 6.5 %all-to-all-start.3 = ((bf16[32,2,32768]{2,1,0:T(2,128)(2,1)}), bf16[32,2,32768]{2,1,0:T(2,128)(2,1)}, u32[]{:S(2)}, u32[]{:S(2)}) async-start(bf16[32,2,32768]{2,1,0:T(2,128)(2,1)} %reshape.207), calls=%async_computation.3 | async-start | bytes 8388608 | tf_op jit(solution)/shard_map/all_to_all | solution.py:49
  208.2 4.6 %convolution_bitcast_fusion = f32[1,1024,1024]{1,2,0:T(8,128)S(1)} fusion(bf16[8,1024,128]{2,1,0:T(8,128)(2,1)} %bitcast.160, bf16[8,1024,128]{2,1,0:T(8,128)(2,1)} %bitcast.162), kind=kOutput, calls=%fused_computation.156 | convolution fusion | flops 2147483648 | bytes 8388608 | tf_op jit(solution)/shard_map/npgc,nqgc->gpq/dot_general | solution.py:106
  215.1 83.6 %all-to-all-done.3 = bf16[32,2,32768]{2,1,0:T(2,128)(2,1)} async-done(((bf16[32,2,32768]{2,1,0:T(2,128)(2,1)}), bf16[32,2,32768]{2,1,0:T(2,128)(2,1)}, u32[]{:S(2)}, u32[]{:S(2)}) %all-to-all-start.3) | async-done | bytes 4194336 | tf_op jit(solution)/shard_map/all_to_all | solution.py:49
  298.7 19.8 %reshape.208 = bf16[8192,1,256]{2,1,0:T(2,128)(2,1)} reshape(bf16[32,2,32768]{2,1,0:T(2,128)(2,1)} %all-to-all-done.3) | data formatting | bytes 8388608
  318.4 6.0 %copy.62 = bf16[8192,1,256]{2,0,1:T(8,128)(2,1)} copy(bf16[8192,1,256]{2,1,0:T(2,128)(2,1)} %reshape.208) | data formatting | bytes 8388608
  324.5 6.4 %copy.56 = bf16[32,256,1,256]{1,3,0,2:T(8,128)(2,1)} copy(bf16[32,256,1,256]{3,1,0,2:T(8,128)(2,1)} %bitcast.155) | data formatting | bytes 8388608 | tf_op jit(solution)/shard_map/all_to_all | solution.py:49
  337.0 14.7 %fusion.17 = bf16[1,256,4096]{1,2,0:T(8,128)(2,1)} fusion(bf16[1,256,4096]{1,2,0:T(8,128)(2,1)S(1)} %copy.47, f32[256,32,128]{0,2,1:T(8,128)S(1)} %get-tuple-element.34, f32[256]{0:T(256)S(1)} %broadcast_multiply_fusion, f32[256]{0:T(256)S(1)} %get-tuple-element.38, f32[4096]{0:T(1024)S(1)} %copy-done.3, f32[256]{0:T(256)S(1)} %get-tuple-element.39), kind=kLoop, calls=%fused_computation.36 | loop fusion | flops 83886080 | bytes 8408064 | tf_op jit(solution)/shard_map/convert_element_type | solution.py:126
  351.8 4.2 copy.58
  363.2 20.6 %psum.28 = f32[4096]{0:T(1024)S(1)} all-reduce(f32[4096]{0:T(1024)S(1)} %bitcast.166), channel_id=1, replica_groups=mesh['sp_0'=8,'sp_1'=4,'dp_0'=4,'dp_1'=2] {'sp_0'}, use_global_device_ids=true, to_apply=%region_6.0 | all-reduce | flops 4096 | bytes 32768 | tf_op jit(solution)/shard_map/psum | solution.py:54
  383.8 14.6 %psum.29 = f32[4096]{0:T(1024)S(1)} all-reduce(f32[4096]{0:T(1024)S(1)} %psum.28), channel_id=1, replica_groups=mesh['sp_0'=8,'sp_1'=4,'dp_0'=4,'dp_1'=2] {'sp_1'}, use_global_device_ids=true, to_apply=%region_7.0 | all-reduce | flops 4096 | bytes 32768 | tf_op jit(solution)/shard_map/psum | solution.py:54
  398.3 13.1 %psum.30 = f32[4096]{0:T(1024)S(1)} all-reduce(f32[4096]{0:T(1024)S(1)} %psum.29), channel_id=1, replica_groups=mesh['sp_0'=8,'sp_1'=4,'dp_0'=4,'dp_1'=2] {'dp_0'}, use_global_device_ids=true, to_apply=%region_8.0 | all-reduce | flops 4096 | bytes 32768 | tf_op jit(solution)/shard_map/psum | solution.py:54
  411.5 20.6 %psum.31 = f32[4096]{0:T(1024)} all-reduce(f32[4096]{0:T(1024)S(1)} %psum.30), channel_id=1, replica_groups=mesh['sp_0'=8,'sp_1'=4,'dp_0'=4,'dp_1'=2] {'dp_1'}, use_global_device_ids=true, to_apply=%region_9.10 | all-reduce | flops 4096 | bytes 32768 | tf_op jit(solution)/shard_map/psum | solution.py:54
  (32 shorter events, 28.2 us)
Async XLA Ops:
  9.7 43.2 %all-to-all-start.1 = ((bf16[8,1,128,1024]{3,2,1,0:T(8,128)(2,1)}), bf16[8,1,128,1024]{3,2,1,0:T(8,128)(2,1)}, u32[]{:S(2)}, u32[]{:S(2)}) async-start(bf16[8,1,128,1024]{3,2,1,0:T(8,128)(2,1)} %broadcast_in_dim.4), calls=%async_computation.1 | async-start | bytes 4194304 | tf_op jit(solution)/shard_map/all_to_all | solution.py:28
  52.9 58.2 %all-to-all-start.2 = ((bf16[256,32,128]{0,2,1:T(8,128)(2,1)}), bf16[256,32,128]{0,2,1:T(8,128)(2,1)}, u32[]{:S(2)}, u32[]{:S(2)}) async-start(bf16[256,32,128]{0,2,1:T(8,128)(2,1)} %bitcast.156), calls=%async_computation.2 | async-start | bytes 4194304 | tf_op jit(solution)/shard_map/all_to_all | solution.py:85
  62.6 0.7 copy-start.3
  111.1 55.7 %all-to-all-start = ((bf16[256,32,128]{0,2,1:T(8,128)(2,1)}), bf16[256,32,128]{0,2,1:T(8,128)(2,1)}, u32[]{:S(2)}, u32[]{:S(2)}) async-start(bf16[256,32,128]{0,2,1:T(8,128)(2,1)} %get-tuple-element.32), calls=%async_computation | async-start | bytes 4194304 | tf_op jit(solution)/shard_map/all_to_all | solution.py:86
  128.6 42.2 %copy-start.4 = (f32[1,1024]{1,0:T(1,128)S(1)}, f32[1,1024]{1,0:T(1,128)}, u32[]{:S(2)}) copy-start(f32[1,1024]{1,0:T(1,128)} %param.10) | copy-start | bytes 12292
  199.5 99.2 %all-to-all-start.3 = ((bf16[32,2,32768]{2,1,0:T(2,128)(2,1)}), bf16[32,2,32768]{2,1,0:T(2,128)(2,1)}, u32[]{:S(2)}, u32[]{:S(2)}) async-start(bf16[32,2,32768]{2,1,0:T(2,128)(2,1)} %reshape.207), calls=%async_computation.3 | async-start | bytes 8388608 | tf_op jit(solution)/shard_map/all_to_all | solution.py:49
  205.9 226.2 %reduce-scatter.2.cloned.1.call-start = ((), (), s32[]{:S(2)}) async-start(), calls=%async_computation.5 | async-start | bytes 4755456 | tf_op jit(solution)/shard_map/reduce_scatter | solution.py:38
  330.9 4.1 copy-start
  351.8 4.2 copy-start.1
  356.0 2.3 copy-start.2
Sparse Core Ops, SparseCore 0:
  215.2 41.5 reduce-scatter.1
where the time goes:
time: 444 us; the launch traced here: 442 us
  waiting for transfers between devices  156 us (35%)
  local copies, waits for them, and re-layouts  80.4 us (18%)
  other arithmetic  75.4 us (17%)
  blocking collectives  68.9 us (16%)
  starting transfers between devices  31.4 us (7%)
  matrix products  16.4 us (4%)
  between operations  14.2 us (3%)
    all_to_all x1, waiting for transfers between devices, sent_together(): lax.all_to_all(both, axis, split_axis=split_dim, concat_axis=concat_dim,...  83.6 us
    psum x4, blocking collectives, by_axis(): return functools.reduce(lax.psum, axes, shard)  68.9 us
    unnamed x19, local copies, waits for them, and re-layouts  52.7 us
    all_to_all x1, waiting for transfers between devices, shards(): lax.all_to_all(gate_tok.reshape(split_shape), SP, split_axis=1, concat_ax...  37.7 us
    all_to_all x1, waiting for transfers between devices, shards(): lax.all_to_all(value_norm.reshape(split_shape), SP, split_axis=1, concat_...  34.3 us
    convert_element_type x1, other arithmetic, shards(): (value_slope * gelu_slope(value_arg)).astype(jnp.bfloat16)[None]  14.7 us
    concatenate x2, other arithmetic, sent_together(): both = jnp.concatenate(arrays, axis=along)  11.3 us
    convert_element_type x1, other arithmetic, shards(): jax.nn.gelu(up_arg, approximate=False).astype(jnp.bfloat16)  10.9 us
  transfers between devices with their start and end apart: 5, of which 3 were waited for; matrix products, arithmetic and copies ran while one was open for 30% of the time, Pallas kernels for 0%

commit v1 on v0

v1 whole, which is shorter than its diff:
```python
import functools
import math

import jax
import jax.numpy as jnp
from jax import lax
from jax.experimental import pallas as pl
from jax.experimental.pallas import tpu as pltpu
from jax.sharding import Mesh
from jax.sharding import PartitionSpec as P

Z = "sp_0"
SP = ("sp_0", "sp_1")
DP = ("dp_0", "dp_1")
PLANE = ("dp_0", "dp_1", "sp_1")
Z_DP = ("sp_0", "dp_0", "dp_1")

norm_floor = 0.5
root_half = 1.0 / math.sqrt(2.0)
inv_root_tau = 1.0 / math.sqrt(2.0 * math.pi)
LANES = 128
F32 = jnp.float32
BF16 = jnp.bfloat16
VMEM_LIMIT = 56 * 1024 * 1024


def normal_cdf(x):
    return 0.5 * (1.0 + lax.erf(x * root_half))


def params(*semantics):
    return pltpu.CompilerParams(dimension_semantics=semantics, vmem_limit_bytes=VMEM_LIMIT)


def prologue_kernel(groups, cot_ref, up_ref, val_ref, gain_ref, out_ref, inv_ref, act_ref):
    rows = cot_ref.shape[0]

    def first(g, squares):
        at = pl.ds(pl.multiple_of(g * LANES, LANES), LANES)
        up = up_ref[:, at].astype(F32)
        up_act = (up * normal_cdf(up)).astype(BF16).astype(F32)
        out_ref[g, 0] = (cot_ref[:, at].astype(F32) * up_act).astype(BF16)
        val = val_ref[:, at].astype(F32)
        act = val * normal_cdf(val)
        act_ref[:, at] = act
        return squares + act * act

    squares = lax.fori_loop(0, groups, first, jnp.zeros((rows, LANES), F32), unroll=2)
    mean = jnp.sum(squares, axis=1, keepdims=True) * (1.0 / (groups * LANES))
    inv = lax.rsqrt(mean + norm_floor)
    inv_ref[...] = jnp.broadcast_to(inv, (rows, LANES))

    def second(g, carry):
        at = pl.ds(pl.multiple_of(g * LANES, LANES), LANES)
        out_ref[g, 1] = (act_ref[:, at] * inv * gain_ref[:, at]).astype(BF16)
        return carry

    lax.fori_loop(0, groups, second, 0, unroll=4)


def prologue(cot, up, val, gain, rows=32):
    toks, width = cot.shape
    groups = width // LANES
    row = pl.BlockSpec((rows, width), lambda i: (i, 0))
    return pl.pallas_call(
        functools.partial(prologue_kernel, groups),
        grid=(toks // rows,),
        in_specs=[row, row, row, pl.BlockSpec((1, width), lambda i: (0, 0))],
        out_specs=[
            pl.BlockSpec((groups, 2, rows, LANES), lambda i: (0, 0, i, 0)),
            pl.BlockSpec((rows, LANES), lambda i: (i, 0)),
        ],
        out_shape=[
            jax.ShapeDtypeStruct((groups, 2, toks, LANES), BF16),
            jax.ShapeDtypeStruct((toks, LANES), F32),
        ],
        scratch_shapes=[pltpu.VMEM((rows, width), F32)],
        compiler_params=params("arbitrary"),
        cost_estimate=pl.CostEstimate(
            flops=100 * toks * width, bytes_accessed=10 * toks * width, transcendentals=0
        ),
        name="prologue",
    )(cot, up, val, gain)


def slopes_kernel(up_ref, val_ref, up_slope_ref, val_slope_ref, act_ref):
    groups = up_ref.shape[1] // LANES

    def step(g, carry):
        at = pl.ds(pl.multiple_of(g * LANES, LANES), LANES)
        up = up_ref[:, at].astype(F32)
        up_slope_ref[:, at] = normal_cdf(up) + up * (jnp.exp(-0.5 * up * up) * inv_root_tau)
        val = val_ref[:, at].astype(F32)
        phi = normal_cdf(val)
        act_ref[:, at] = val * phi
        val_slope_ref[:, at] = phi + val * (jnp.exp(-0.5 * val * val) * inv_root_tau)
        return carry

    lax.fori_loop(0, groups, step, 0, unroll=2)


def slopes(up, val, rows=32):
    toks, width = up.shape
    row = pl.BlockSpec((rows, width), lambda i: (i, 0))
    out = jax.ShapeDtypeStruct((toks, width), F32)
    return pl.pallas_call(
        slopes_kernel,
        grid=(toks // rows,),
        in_specs=[row, row],
        out_specs=[row, row, row],
        out_shape=[out, out, out],
        compiler_params=params("arbitrary"),
        cost_estimate=pl.CostEstimate(
            flops=100 * toks * width, bytes_accessed=16 * toks * width, transcendentals=0
        ),
        name="slopes",
    )(up, val)


def gathered(ref, which, seqs, parts):
    return jnp.concatenate(
        [
            jnp.concatenate([ref[b * parts + y, which] for y in range(parts)], axis=0)
            for b in range(seqs)
        ],
        axis=1,
    )


def weight_grad_kernel(seqs, parts, slab, recv_ref, out_ref, value_ref):
    i = pl.program_id(0)

    @pl.when(i == 0)
    def _():
        for b in range(seqs):
            for y in range(parts):
                toks = recv_ref.shape[2]
                value_ref[y * toks : (y + 1) * toks, b * LANES : (b + 1) * LANES] = recv_ref[
                    b * parts + y, 1
                ]

    per = recv_ref.shape[2] // slab
    y = i // per
    at = pl.ds(pl.multiple_of((i % per) * slab, slab), slab)
    gate = jnp.concatenate([recv_ref[b * parts + y, 0, at] for b in range(seqs)], axis=1)
    across = (((1,), (1,)), ((), ()))
    out_ref[:slab] = lax.dot_general(
        gate, value_ref[...], across, preferred_element_type=F32
    ).astype(out_ref.dtype)
    sums = lax.dot_general(
        jnp.ones((8, gate.shape[1]), BF16), gate, across, preferred_element_type=F32
    )
    out_ref[slab:] = jnp.zeros((8, out_ref.shape[1]), out_ref.dtype)
    out_ref[slab:, :slab] = sums.astype(out_ref.dtype)


def weight_grads(recv, seqs, parts, slab, dtype):
    toks = recv.shape[2]
    block = parts * toks
    slabs = block // slab
    return pl.pallas_call(
        functools.partial(weight_grad_kernel, seqs, parts, slab),
        grid=(slabs,),
        in_specs=[pl.BlockSpec(recv.shape, lambda i: (0, 0, 0, 0))],
        out_specs=pl.BlockSpec((slab + 8, block), lambda i: (i, 0)),
        out_shape=jax.ShapeDtypeStruct((slabs * (slab + 8), block), dtype),
        scratch_shapes=[pltpu.VMEM((block, seqs * LANES), BF16)],
        compiler_params=params("arbitrary"),
        cost_estimate=pl.CostEstimate(
            flops=2 * block * block * seqs * LANES, bytes_accessed=8 * block * block, transcendentals=0
        ),
        name="weight_grads",
    )(recv)


def mix_kernel(seqs, parts, recv_ref, w_ref, bias_ref, out_ref, gain_ref, gate_ref, value_ref):
    y = pl.program_id(0)
    toks = recv_ref.shape[2]

    @pl.when(y == 0)
    def _():
        gain_ref[...] = jnp.zeros_like(gain_ref)
        for b in range(seqs):
            for k in range(parts):
                rows, cols = pl.ds(k * toks, toks), pl.ds(b * LANES, LANES)
                gate_ref[rows, cols] = recv_ref[b * parts + k, 0]
                value_ref[rows, cols] = recv_ref[b * parts + k, 1]

    at = pl.ds(pl.multiple_of(y * toks, toks), toks)
    back = lax.dot_general(
        w_ref[:, at], gate_ref[...], (((0,), (0,)), ((), ())), preferred_element_type=F32
    ).astype(BF16)
    terms = back.astype(F32) * value_ref[at].astype(F32)
    total = jnp.zeros((8, LANES), F32)
    for b in range(seqs):
        out_ref[b, 0, 1] = back[:, b * LANES : (b + 1) * LANES]
        total += jnp.sum(
            terms[:, b * LANES : (b + 1) * LANES].reshape(toks // 8, 8, LANES), axis=0
        )
    gain_ref[...] += total
    mixed = jnp.dot(w_ref[at], value_ref[...], preferred_element_type=F32)
    mixed = (mixed + bias_ref[at, :1]).astype(BF16)
    for b in range(seqs):
        out_ref[b, 0, 0] = mixed[:, b * LANES : (b + 1) * LANES]


def mix(recv, w, bias, seqs, parts):
    toks = recv.shape[2]
    block = parts * toks
    out, gain = pl.pallas_call(
        functools.partial(mix_kernel, seqs, parts),
        grid=(parts,),
        in_specs=[
            pl.BlockSpec(recv.shape, lambda y: (0, 0, 0, 0)),
            pl.BlockSpec(w.shape, lambda y: (0, 0)),
            pl.BlockSpec(bias.shape, lambda y: (0, 0)),
        ],
        out_specs=[
            pl.BlockSpec((seqs, 1, 2, toks, LANES), lambda y: (0, y, 0, 0, 0)),
            pl.BlockSpec((8, LANES), lambda y: (0, 0)),
        ],
        out_shape=[
            jax.ShapeDtypeStruct((seqs, parts, 2, toks, LANES), BF16),
            jax.ShapeDtypeStruct((8, LANES), F32),
        ],
        scratch_shapes=[pltpu.VMEM((block, seqs * LANES), BF16)] * 2,
        compiler_params=params("arbitrary"),
        cost_estimate=pl.CostEstimate(
            flops=4 * block * block * seqs * LANES, bytes_accessed=10 * block * block, transcendentals=0
        ),
        name="mix",
    )(recv, w, bias)
    return out.reshape(recv.shape), gain


def epilogue_kernel(
    groups, recv_ref, cot_ref, up_slope_ref, val_slope_ref, act_ref, inv_ref, gain_ref, up_ref, val_ref
):
    rows = cot_ref.shape[0]

    def first(g, dots):
        at = pl.ds(pl.multiple_of(g * LANES, LANES), LANES)
        mid = (cot_ref[:, at].astype(F32) * recv_ref[g, 0].astype(F32)).astype(BF16)
        up_ref[:, at] = (mid.astype(F32) * up_slope_ref[:, at]).astype(BF16)
        scaled = recv_ref[g, 1].astype(F32) * gain_ref[:, at]
        return dots + scaled * act_ref[:, at]

    dots = lax.fori_loop(0, groups, first, jnp.zeros((rows, LANES), F32), unroll=2)
    mean = jnp.sum(dots, axis=1, keepdims=True) * (1.0 / (groups * LANES))
    inv = inv_ref[...]
    pull = inv * inv * inv * mean

    def second(g, carry):
        at = pl.ds(pl.multiple_of(g * LANES, LANES), LANES)
        scaled = recv_ref[g, 1].astype(F32) * gain_ref[:, at]
        slope = inv * scaled - pull * act_ref[:, at]
        val_ref[:, at] = (slope * val_slope_ref[:, at]).astype(BF16)
        return carry

    lax.fori_loop(0, groups, second, 0, unroll=4)


def epilogue(recv, cot, up_slope, val_slope, act, inv, gain, rows=32):
    toks, width = cot.shape
    groups = width // LANES
    row = pl.BlockSpec((rows, width), lambda i: (i, 0))
    out = jax.ShapeDtypeStruct((toks, width), BF16)
    return pl.pallas_call(
        functools.partial(epilogue_kernel, groups),
        grid=(toks // rows,),
        in_specs=[
            pl.BlockSpec((groups, 2, rows, LANES), lambda i: (0, 0, i, 0)),
            row,
            row,
            row,
            row,
            pl.BlockSpec((rows, LANES), lambda i: (i, 0)),
            pl.BlockSpec((1, width), lambda i: (0, 0)),
        ],
        out_specs=[row, row],
        out_shape=[out, out],
        compiler_params=params("arbitrary"),
        cost_estimate=pl.CostEstimate(
            flops=20 * toks * width, bytes_accessed=22 * toks * width, transcendentals=0
        ),
        name="epilogue",
    )(recv, cot, up_slope, val_slope, act, inv, gain)


def shards(cotangent, up_pre, value_pre, spatial_weight, spatial_bias, value_gain):
    planes = lax.axis_size(Z)
    seqs = lax.axis_size(DP)
    parts = lax.axis_size("sp_1")
    slab = spatial_weight.shape[1]
    cot, up, val = cotangent[0], up_pre[0], value_pre[0]
    gain = value_gain[None]

    swap = [(k * seqs + a, a * seqs + k) for k in range(planes) for a in range(seqs)]
    high = spatial_bias.astype(BF16)
    middle = (spatial_bias - high.astype(F32)).astype(BF16)
    low = (spatial_bias - high.astype(F32) - middle.astype(F32)).astype(BF16)
    pad = jnp.zeros((5, slab * seqs), BF16)
    own = jnp.concatenate([spatial_weight[0], high, middle, low, pad], axis=0)
    own = lax.ppermute(own, Z_DP, swap)
    bias = jnp.sum(own[slab : slab + 3].astype(F32), axis=0)
    weights = lax.all_gather(own[:slab], Z, axis=0, tiled=True)

    sent, inv = prologue(cot, up, val, gain)
    recv = lax.all_to_all(sent, PLANE, split_axis=0, concat_axis=0, tiled=True)
    up_slope, val_slope, act = slopes(up, val)

    grads = weight_grads(recv, seqs, parts, slab, F32)
    grads = lax.psum_scatter(grads, Z, scatter_dimension=0, tiled=True)
    grads = lax.ppermute(grads, Z_DP, swap)

    bias_col = jnp.broadcast_to(bias[:, None], (bias.shape[0], LANES))
    back, gain_part = mix(recv, weights, bias_col, seqs, parts)
    back = lax.all_to_all(back, PLANE, split_axis=0, concat_axis=0, tiled=True)
    gain_part = lax.psum(jnp.sum(gain_part, axis=0, keepdims=True), Z)
    gain_grad = lax.all_gather(gain_part, PLANE, axis=0, tiled=True).reshape(-1) / value_gain
    up_grad, value_grad = epilogue(back, cot, up_slope, val_slope, act, inv, gain)
    return (
        up_grad[None],
        value_grad[None],
        grads[None, :slab].astype(F32),
        grads[slab : slab + 1, :slab].astype(F32),
        gain_grad,
    )


def solution(mesh):
    torus = Mesh(mesh.devices.reshape(8, 4, 4, 2), ("sp_0", "sp_1", "dp_0", "dp_1"))
    in_specs = (
        P(DP, SP, None),
        P(DP, SP, None),
        P(DP, SP, None),
        P(SP, DP, None),
        P(SP, None),
        P(),
    )
    out_specs = (P(DP, SP, None), P(DP, SP, None), P(SP, DP, None), P(SP, DP), P())
    return jax.shard_map(
        shards, mesh=torus, in_specs=in_specs, out_specs=out_specs, check_vma=False
    )
```

time: 444 us -> 264 us (0.59)
  local copies, waits for them, and re-layouts: 80.4 us -> 3.21 us
  other arithmetic: 75.4 us -> 0.66 us
  waiting for transfers between devices: 156 us -> 95.9 us
  Pallas kernels: 0 us -> 52.6 us
  matrix products: 16.4 us -> 0 us
  starting transfers between devices: 31.4 us -> 25.9 us
    all_to_all x4 -> x2, waiting for transfers between devices: 156 us -> 49.6 us  [the longest x1 49.6 us: shards(): recv = lax.all_to_all(sent, PLANE, split_axis=0, concat_axis=0, tiled=True)]
    unnamed x19 -> x8, local copies, waits for them, and re-layouts: 52.7 us -> 0.02 us
    pallas_call x0 -> x5, Pallas kernels: none -> 52.6 us  [the longest x1 11.7 us: epilogue(): pl.pallas_call(functools.partial(epilogue_kernel, groups), grid=(toks //...]
    convert_element_type x6 -> x1, other arithmetic: 44.1 us -> 0.01 us  [shards(): low = (spatial_bias - high.astype(F32) - middle.astype(F32)).astype(BF16)]
    reduce_scatter x1, waiting for transfers between devices: 0.01 us -> 41 us  [shards(): grads = lax.psum_scatter(grads, Z, scatter_dimension=0, tiled=True)]
    all_gather x0 -> x1, blocking collectives: none -> 36.4 us  [shards(): lax.all_gather(gain_part, PLANE, axis=0, tiled=True).reshape(-1)]
    psum x4 -> x1, blocking collectives: 68.9 us -> 34.7 us  [shards(): gain_part = lax.psum(jnp.sum(gain_part, axis=0, keepdims=True), Z)]
    dot_general x3 -> x0, matrix products: 16.4 us -> none  [the longest x1 5.96 us: shards(): jnp.einsum('gpq,nqgc->npgc', portion, value_blocks, preferred_element_typ...]
  transfers between devices with their start and end apart: 5 -> 6, of which waited for: 3 -> 3; matrix products, arithmetic and copies ran while one was open for 30% -> 1% of each run, Pallas kernels for 0% -> 16%
where the time goes in v1:
time: 264 us
  waiting for transfers between devices  95.9 us (36%)
  blocking collectives  71.1 us (27%)
  Pallas kernels  52.6 us (20%)
  starting transfers between devices  25.9 us (10%)
  between operations  14.1 us (5%)
  local copies, waits for them, and re-layouts  3.21 us (1%)
    all_to_all x1, waiting for transfers between devices, shards(): recv = lax.all_to_all(sent, PLANE, split_axis=0, concat_axis=0, tiled=True)  49.6 us
    reduce_scatter x1, waiting for transfers between devices, shards(): grads = lax.psum_scatter(grads, Z, scatter_dimension=0, tiled=True)  41 us
    all_gather x1, blocking collectives, shards(): lax.all_gather(gain_part, PLANE, axis=0, tiled=True).reshape(-1)  36.4 us
    psum x1, blocking collectives, shards(): gain_part = lax.psum(jnp.sum(gain_part, axis=0, keepdims=True), Z)  34.7 us
    pallas_call x1, Pallas kernels, epilogue(): pl.pallas_call(functools.partial(epilogue_kernel, groups), grid=(toks //...  11.7 us
    all_to_all x1, starting transfers between devices, shards(): back = lax.all_to_all(back, PLANE, split_axis=0, concat_axis=0, tiled=True)  11.3 us
    pallas_call x1, Pallas kernels, weight_grads(): pl.pallas_call(functools.partial(weight_grad_kernel, seqs, parts, slab),...  10.8 us
    pallas_call x1, Pallas kernels, mix(): pl.pallas_call(functools.partial(mix_kernel, seqs, parts), grid=(parts,),...  10.5 us
  transfers between devices with their start and end apart: 6, of which 3 were waited for; matrix products, arithmetic and copies ran while one was open for 1% of the time, Pallas kernels for 16%

profile of v1, /device:TPU:1, one launch (start us, length us, event | category | flops | bytes accessed | tf_op | source)
XLA Modules:
  0.0 263.6 jit_solution(6095997103426138185)
XLA Ops:
  7.2 9.4 %prologue.1 = (bf16[32,2,256,128]{3,2,1,0:T(8,128)(2,1)}, f32[256,128]{1,0:T(8,128)}) custom-call(bf16[256,4096]{1,0:T(8,128)(2,1)} %bitcast.17, bf16[256,4096]{1,0:T(8,128)(2,1)} %bitcast.13, bf16[256,4096]{1,0:T(8,128)(2,1)} %bitcast.15, f32[1,4096]{1,0:T(1,128)} %bitcast.21), custom_call_target="tpu_custom_call" | custom-call | flops 104857600 | bytes 10485760 | tf_op jit(solution)/shard_map/prologue/pallas_call | solution.py:65
  16.6 8.8 %all-to-all-start = ((bf16[32,2,256,128]{3,2,1,0:T(8,128)(2,1)}), bf16[32,2,256,128]{3,2,1,0:T(8,128)(2,1)}, u32[]{:S(2)}, u32[]{:S(2)}) async-start(bf16[32,2,256,128]{3,2,1,0:T(8,128)(2,1)} %get-tuple-element.14), calls=%async_computation | async-start | bytes 8388608 | tf_op jit(solution)/shard_map/all_to_all | solution.py:309
  25.4 0.0 all-gather.3.cloned.1.call-start
  25.4 0.0 copy-done.3
  25.4 0.0 copy-done
  25.5 0.1 concatenate.3
  25.6 3.7 %collective-permute-start = (bf16[136,1024]{1,0:T(8,128)(2,1)S(1)}, bf16[136,1024]{1,0:T(8,128)(2,1)S(1)}, u32[]{:S(2)}, u32[]{:S(2)}) collective-permute-start(bf16[136,1024]{1,0:T(8,128)(2,1)S(1)} %concatenate.3), channel_id=1, source_target_pairs={{0,0},{1,32},{2,64},{3,96},{4,128},{5,160},{6,192},{7,224},{32,1},... | collective-permute-start | bytes 835592 | tf_op jit(solution)/shard_map/ppermute | solution.py:304
  29.3 5.3 %collective-permute-done = bf16[136,1024]{1,0:T(8,128)(2,1)S(1)} collective-permute-done((bf16[136,1024]{1,0:T(8,128)(2,1)S(1)}, bf16[136,1024]{1,0:T(8,128)(2,1)S(1)}, u32[]{:S(2)}, u32[]{:S(2)}) %collective-permute-start) | collective-permute-done | bytes 278560 | tf_op jit(solution)/shard_map/ppermute | solution.py:304
  34.7 0.7 slice.16
  35.4 0.0 all-gather.3.cloned.1.call-update
  35.4 0.0 reduce-scatter.2.cloned.1.call-start
  35.5 49.6 %all-to-all-done.recv_ref = bf16[32,2,256,128]{3,2,1,0:T(8,128)(2,1)} async-done(((bf16[32,2,256,128]{3,2,1,0:T(8,128)(2,1)}), bf16[32,2,256,128]{3,2,1,0:T(8,128)(2,1)}, u32[]{:S(2)}, u32[]{:S(2)}) %all-to-all-start) | async-done | bytes 4194336 | tf_op jit(solution)/shard_map/all_to_all | solution.py:309
  85.0 10.8 %weight_grads.1 = f32[1088,1024]{1,0:T(8,128)} custom-call(bf16[32,2,256,128]{3,2,1,0:T(8,128)(2,1)} %all-to-all-done.recv_ref), custom_call_target="tpu_custom_call" | custom-call | flops 2147483648 | bytes 8388608 | tf_op jit(solution)/shard_map/weight_grads/pallas_call | solution.py:161
  95.8 0.0 reduce-scatter.2.cloned.1.call-update
  95.8 0.0 all-gather.3.cloned.1.call-done.w_ref
  95.9 1.0 broadcast_in_dim.26.bias_ref
  96.9 10.5 %mix.1 = (bf16[8,4,2,256,128]{4,3,2,1,0:T(8,128)(2,1)}, f32[8,128]{1,0:T(8,128)}) custom-call(bf16[32,2,256,128]{3,2,1,0:T(8,128)(2,1)} %all-to-all-done.recv_ref, bf16[1024,1024]{1,0:T(8,128)(2,1)} %all-gather.3.cloned.1.call-done.w_ref, f32[1024,128]{1,0:T(8,128)} %broadcast_in_dim.26.bias_ref), custom_call_target="tpu_custom_call" | custom-call | flops 4294967296 | bytes 10485760 | tf_op jit(solution)/shard_map/mix/pallas_call | solution.py:210
  107.3 11.3 %all-to-all-start.1 = ((bf16[32,2,256,128]{3,2,1,0:T(8,128)(2,1)}), bf16[32,2,256,128]{3,2,1,0:T(8,128)(2,1)}, u32[]{:S(2)}, u32[]{:S(2)}) async-start(bf16[32,2,256,128]{3,2,1,0:T(8,128)(2,1)} %bitcast.19), calls=%async_computation.1 | async-start | bytes 8388608 | tf_op jit(solution)/shard_map/all_to_all | solution.py:318
  118.7 0.0 copy-start.2
  118.7 0.0 copy-start.1
  118.7 41.0 %reduce-scatter.2.cloned.1.call-done = f32[136,1024]{1,0:T(8,128)} async-done(((f32[1088,1024]{1,0:T(8,128)}), f32[136,1024]{1,0:T(8,128)}) %reduce-scatter.2.cloned.1.call-update) | async-done | bytes 557072 | tf_op jit(solution)/shard_map/reduce_scatter | solution.py:313
  159.7 2.0 collective-permute-start.1
  161.7 10.3 %slopes.1 = (f32[256,4096]{1,0:T(8,128)}, f32[256,4096]{1,0:T(8,128)}, f32[256,4096]{1,0:T(8,128)}) custom-call(bf16[256,4096]{1,0:T(8,128)(2,1)} %bitcast.14, bf16[256,4096]{1,0:T(8,128)(2,1)} %bitcast.16), custom_call_target="tpu_custom_call" | custom-call | flops 104857600 | bytes 16777216 | tf_op jit(solution)/shard_map/slopes/pallas_call | solution.py:106
  172.0 0.0 copy-done.2
  172.0 34.7 %psum.7 = f32[1,128]{1,0:T(1,128)S(1)} all-reduce(f32[1,128]{1,0:T(1,128)S(1)} %bitcast.24), channel_id=1, replica_groups=mesh['sp_0'=8,'sp_1'=4,'dp_0'=4,'dp_1'=2] {'sp_0'}, use_global_device_ids=true, to_apply=%region_3.0 | all-reduce | flops 128 | bytes 1024 | tf_op jit(solution)/shard_map/psum | solution.py:319
  206.7 36.4 %all-gather = f32[32,1,128]{2,1,0:T(1,128)S(1)} all-gather(f32[1,1,128]{2,1,0:T(1,128)S(1)} %bitcast.25), channel_id=1, replica_groups=mesh['sp_0'=8,'sp_1'=4,'dp_0'=4,'dp_1'=2] {'dp_0','dp_1','sp_1'}, dimensions={0}, use_global_device_ids=true | all-gather | bytes 16896 | tf_op jit(solution)/shard_map/all_gather | solution.py:320
  243.1 0.6 div.3
  243.7 0.0 all-to-all-done.1.recv_ref
  243.7 11.7 %epilogue.1 = (bf16[256,4096]{1,0:T(8,128)(2,1)}, bf16[256,4096]{1,0:T(8,128)(2,1)}) custom-call(bf16[32,2,256,128]{3,2,1,0:T(8,128)(2,1)} %all-to-all-done.1.recv_ref, bf16[256,4096]{1,0:T(8,128)(2,1)} %bitcast.18, f32[256,4096]{1,0:T(8,128)} %get-tuple-element.16.up_slope_ref, f32[256,4096]{1,0:T(8,128)} %get-tuple-element.17.val_slope_ref, ...), custom_call_target="tpu_custom_call" | custom-call | flops 20971520 | bytes 23068672 | tf_op jit(solution)/shard_map/epilogue/pallas_call | solution.py:268
  255.4 0.0 collective-permute-done.1
  255.4 0.5 slice.19
  255.9 0.8 slice_bitcast_fusion
  (7 shorter events, 0.1 us)
Async XLA Ops:
  16.6 8.8 %copy-start.3 = (f32[1,1024]{1,0:T(1,128)S(1)}, f32[1,1024]{1,0:T(1,128)}, u32[]{:S(2)}) copy-start(f32[1,1024]{1,0:T(1,128)} %param.10) | copy-start | bytes 12292
  16.6 8.9 %copy-start = (bf16[1,128,1024]{2,1,0:T(8,128)(2,1)S(1)}, bf16[1,128,1024]{2,1,0:T(8,128)(2,1)}, u32[]{:S(2)}) copy-start(bf16[1,128,1024]{2,1,0:T(8,128)(2,1)} %param.9) | copy-start | bytes 786436
  16.6 68.4 %all-to-all-start = ((bf16[32,2,256,128]{3,2,1,0:T(8,128)(2,1)}), bf16[32,2,256,128]{3,2,1,0:T(8,128)(2,1)}, u32[]{:S(2)}, u32[]{:S(2)}) async-start(bf16[32,2,256,128]{3,2,1,0:T(8,128)(2,1)} %get-tuple-element.14), calls=%async_computation | async-start | bytes 8388608 | tf_op jit(solution)/shard_map/all_to_all | solution.py:309
  25.4 70.5 %all-gather.3.cloned.1.call-start = ((), (), s32[]{:S(2)}) async-start(), calls=%async_computation.3 | async-start | bytes 2359296 | tf_op jit(solution)/shard_map/all_gather | solution.py:306
  25.6 9.1 %collective-permute-start = (bf16[136,1024]{1,0:T(8,128)(2,1)S(1)}, bf16[136,1024]{1,0:T(8,128)(2,1)S(1)}, u32[]{:S(2)}, u32[]{:S(2)}) collective-permute-start(bf16[136,1024]{1,0:T(8,128)(2,1)S(1)} %concatenate.3), channel_id=1, source_target_pairs={{0,0},{1,32},{2,64},{3,96},{4,128},{5,160},{6,192},{7,224},{32,1},... | collective-permute-start | bytes 835592 | tf_op jit(solution)/shard_map/ppermute | solution.py:304
  35.4 124.2 %reduce-scatter.2.cloned.1.call-start = ((), (), s32[]{:S(2)}) async-start(), calls=%async_computation.4 | async-start | bytes 5013504 | tf_op jit(solution)/shard_map/reduce_scatter | solution.py:313
  107.3 136.4 %all-to-all-start.1 = ((bf16[32,2,256,128]{3,2,1,0:T(8,128)(2,1)}), bf16[32,2,256,128]{3,2,1,0:T(8,128)(2,1)}, u32[]{:S(2)}, u32[]{:S(2)}) async-start(bf16[32,2,256,128]{3,2,1,0:T(8,128)(2,1)} %bitcast.19), calls=%async_computation.1 | async-start | bytes 8388608 | tf_op jit(solution)/shard_map/all_to_all | solution.py:318
  118.7 53.3 %copy-start.2 = (f32[8,128]{1,0:T(8,128)S(1)}, f32[8,128]{1,0:T(8,128)}, u32[]{:S(2)}) copy-start(f32[8,128]{1,0:T(8,128)} %get-tuple-element.22) | copy-start | bytes 12292
  118.7 124.4 %copy-start.1 = (f32[4096]{0:T(1024)S(1)}, f32[4096]{0:T(1024)}, u32[]{:S(2)}) copy-start(f32[4096]{0:T(1024)} %param.11) | copy-start | bytes 49156
  159.7 95.8 %collective-permute-start.1 = (f32[136,1024]{1,0:T(8,128)}, f32[136,1024]{1,0:T(8,128)S(1)}, u32[]{:S(2)}, u32[]{:S(2)}) collective-permute-start(f32[136,1024]{1,0:T(8,128)} %reduce-scatter.2.cloned.1.call-done), channel_id=1, source_target_pairs={{0,0},{1,32},{2,64},{3,96},{4,128},{5,160},{6,192},{7,224},{32,1},... | collective-permute-start | bytes 1671176 | tf_op jit(solution)/shard_map/ppermute | solution.py:314
Sparse Core Ops, SparseCore 0:
  35.5 54.3 all-gather.2
  95.9 63.6 reduce-scatter.1

commit v2 on v1

--- a/solution.py
+++ b/solution.py
@@ -21,15 +21,16 @@
 LANES = 128
 F32 = jnp.float32
 BF16 = jnp.bfloat16
-VMEM_LIMIT = 56 * 1024 * 1024
 
 
 def normal_cdf(x):
     return 0.5 * (1.0 + lax.erf(x * root_half))
 
 
-def params(*semantics):
-    return pltpu.CompilerParams(dimension_semantics=semantics, vmem_limit_bytes=VMEM_LIMIT)
+def params(mib):
+    return pltpu.CompilerParams(
+        dimension_semantics=("arbitrary",), vmem_limit_bytes=mib * 1024 * 1024
+    )
 
 
 def prologue_kernel(groups, cot_ref, up_ref, val_ref, gain_ref, out_ref, inv_ref, act_ref):
@@ -75,7 +76,7 @@
             jax.ShapeDtypeStruct((toks, LANES), F32),
         ],
         scratch_shapes=[pltpu.VMEM((rows, width), F32)],
-        compiler_params=params("arbitrary"),
+        compiler_params=params(60),
         cost_estimate=pl.CostEstimate(
             flops=100 * toks * width, bytes_accessed=10 * toks * width, transcendentals=0
         ),
@@ -109,7 +110,7 @@
         in_specs=[row, row],
         out_specs=[row, row, row],
         out_shape=[out, out, out],
-        compiler_params=params("arbitrary"),
+        compiler_params=params(60),
         cost_estimate=pl.CostEstimate(
             flops=100 * toks * width, bytes_accessed=16 * toks * width, transcendentals=0
         ),
@@ -117,69 +118,14 @@
     )(up, val)
 
 
-def gathered(ref, which, seqs, parts):
-    return jnp.concatenate(
-        [
-            jnp.concatenate([ref[b * parts + y, which] for y in range(parts)], axis=0)
-            for b in range(seqs)
-        ],
-        axis=1,
-    )
-
-
-def weight_grad_kernel(seqs, parts, slab, recv_ref, out_ref, value_ref):
-    i = pl.program_id(0)
-
-    @pl.when(i == 0)
-    def _():
-        for b in range(seqs):
-            for y in range(parts):
-                toks = recv_ref.shape[2]
-                value_ref[y * toks : (y + 1) * toks, b * LANES : (b + 1) * LANES] = recv_ref[
-                    b * parts + y, 1
-                ]
-
-    per = recv_ref.shape[2] // slab
-    y = i // per
-    at = pl.ds(pl.multiple_of((i % per) * slab, slab), slab)
-    gate = jnp.concatenate([recv_ref[b * parts + y, 0, at] for b in range(seqs)], axis=1)
-    across = (((1,), (1,)), ((), ()))
-    out_ref[:slab] = lax.dot_general(
-        gate, value_ref[...], across, preferred_element_type=F32
-    ).astype(out_ref.dtype)
-    sums = lax.dot_general(
-        jnp.ones((8, gate.shape[1]), BF16), gate, across, preferred_element_type=F32
-    )
-    out_ref[slab:] = jnp.zeros((8, out_ref.shape[1]), out_ref.dtype)
-    out_ref[slab:, :slab] = sums.astype(out_ref.dtype)
-
-
-def weight_grads(recv, seqs, parts, slab, dtype):
-    toks = recv.shape[2]
-    block = parts * toks
-    slabs = block // slab
-    return pl.pallas_call(
-        functools.partial(weight_grad_kernel, seqs, parts, slab),
-        grid=(slabs,),
-        in_specs=[pl.BlockSpec(recv.shape, lambda i: (0, 0, 0, 0))],
-        out_specs=pl.BlockSpec((slab + 8, block), lambda i: (i, 0)),
-        out_shape=jax.ShapeDtypeStruct((slabs * (slab + 8), block), dtype),
-        scratch_shapes=[pltpu.VMEM((block, seqs * LANES), BF16)],
-        compiler_params=params("arbitrary"),
-        cost_estimate=pl.CostEstimate(
-            flops=2 * block * block * seqs * LANES, bytes_accessed=8 * block * block, transcendentals=0
-        ),
-        name="weight_grads",
-    )(recv)
-
-
-def mix_kernel(seqs, parts, recv_ref, w_ref, bias_ref, out_ref, gain_ref, gate_ref, value_ref):
+def core_kernel(
+    seqs, parts, recv_ref, w_ref, bias_ref, grad_ref, out_ref, sums_ref, gate_ref, value_ref
+):
     y = pl.program_id(0)
     toks = recv_ref.shape[2]
 
     @pl.when(y == 0)
     def _():
-        gain_ref[...] = jnp.zeros_like(gain_ref)
         for b in range(seqs):
             for k in range(parts):
                 rows, cols = pl.ds(k * toks, toks), pl.ds(b * LANES, LANES)
@@ -187,6 +133,14 @@
                 value_ref[rows, cols] = recv_ref[b * parts + k, 1]
 
     at = pl.ds(pl.multiple_of(y * toks, toks), toks)
+    across = (((1,), (1,)), ((), ()))
+    gate = gate_ref[at]
+    grad_ref[...] = lax.dot_general(
+        gate, value_ref[...], across, preferred_element_type=F32
+    ).astype(grad_ref.dtype)
+    ones = jnp.ones((8, gate.shape[1]), BF16)
+    shift = pl.ds(pl.multiple_of(LANES + y * toks, LANES), toks)
+    sums_ref[:, shift] = lax.dot_general(ones, gate, across, preferred_element_type=F32)
     back = lax.dot_general(
         w_ref[:, at], gate_ref[...], (((0,), (0,)), ((), ())), preferred_element_type=F32
     ).astype(BF16)
@@ -197,18 +151,27 @@
         total += jnp.sum(
             terms[:, b * LANES : (b + 1) * LANES].reshape(toks // 8, 8, LANES), axis=0
         )
-    gain_ref[...] += total
+    total = jnp.broadcast_to(jnp.sum(total, axis=0, keepdims=True), (8, LANES))
+
+    @pl.when(y == 0)
+    def _():
+        sums_ref[:, :LANES] = total
+
+    @pl.when(y > 0)
+    def _():
+        sums_ref[:, :LANES] += total
+
     mixed = jnp.dot(w_ref[at], value_ref[...], preferred_element_type=F32)
     mixed = (mixed + bias_ref[at, :1]).astype(BF16)
     for b in range(seqs):
         out_ref[b, 0, 0] = mixed[:, b * LANES : (b + 1) * LANES]
 
 
-def mix(recv, w, bias, seqs, parts):
+def core(recv, w, bias, seqs, parts):
     toks = recv.shape[2]
     block = parts * toks
-    out, gain = pl.pallas_call(
-        functools.partial(mix_kernel, seqs, parts),
+    grads, out, sums = pl.pallas_call(
+        functools.partial(core_kernel, seqs, parts),
         grid=(parts,),
         in_specs=[
             pl.BlockSpec(recv.shape, lambda y: (0, 0, 0, 0)),
@@ -216,21 +179,23 @@
             pl.BlockSpec(bias.shape, lambda y: (0, 0)),
         ],
         out_specs=[
+            pl.BlockSpec((toks, block), lambda y: (y, 0)),
             pl.BlockSpec((seqs, 1, 2, toks, LANES), lambda y: (0, y, 0, 0, 0)),
-            pl.BlockSpec((8, LANES), lambda y: (0, 0)),
+            pl.BlockSpec((8, LANES + block), lambda y: (0, 0)),
         ],
         out_shape=[
+            jax.ShapeDtypeStruct((block, block), BF16),
             jax.ShapeDtypeStruct((seqs, parts, 2, toks, LANES), BF16),
-            jax.ShapeDtypeStruct((8, LANES), F32),
+            jax.ShapeDtypeStruct((8, LANES + block), F32),
         ],
         scratch_shapes=[pltpu.VMEM((block, seqs * LANES), BF16)] * 2,
-        compiler_params=params("arbitrary"),
+        compiler_params=params(60),
         cost_estimate=pl.CostEstimate(
-            flops=4 * block * block * seqs * LANES, bytes_accessed=10 * block * block, transcendentals=0
+            flops=6 * block * block * seqs * LANES, bytes_accessed=12 * block * block, transcendentals=0
         ),
-        name="mix",
+        name="core",
     )(recv, w, bias)
-    return out.reshape(recv.shape), gain
+    return grads, out.reshape(recv.shape), sums[:1]
 
 
 def epilogue_kernel(
@@ -279,7 +244,7 @@
         ],
         out_specs=[row, row],
         out_shape=[out, out],
-        compiler_params=params("arbitrary"),
+        compiler_params=params(60),
         cost_estimate=pl.CostEstimate(
             flops=20 * toks * width, bytes_accessed=22 * toks * width, transcendentals=0
         ),
@@ -287,45 +252,59 @@
     )(recv, cot, up_slope, val_slope, act, inv, gain)
 
 
+def pack_kernel(seqs, parts, sums_ref, out_ref):
+    out_ref[...] = jnp.zeros_like(out_ref)
+    for a in range(seqs):
+        at = slice((a + 1) * LANES, (a + 2) * LANES)
+        for y in range(parts):
+            out_ref[a * parts + y, :1] = sums_ref[:, :LANES]
+            out_ref[a * parts + y, 1:2] = sums_ref[:, at]
+
+
+def pack(sums, seqs, parts):
+    shape = (seqs * parts, 8, LANES)
+    return pl.pallas_call(
+        functools.partial(pack_kernel, seqs, parts),
+        grid=(1,),
+        in_specs=[pl.BlockSpec(sums.shape, lambda i: (0, 0))],
+        out_specs=pl.BlockSpec(shape, lambda i: (0, 0, 0)),
+        out_shape=jax.ShapeDtypeStruct(shape, F32),
+        compiler_params=params(60),
+        name="pack",
+    )(sums)
+
+
 def shards(cotangent, up_pre, value_pre, spatial_weight, spatial_bias, value_gain):
     planes = lax.axis_size(Z)
     seqs = lax.axis_size(DP)
     parts = lax.axis_size("sp_1")
-    slab = spatial_weight.shape[1]
+    block = spatial_weight.shape[2]
     cot, up, val = cotangent[0], up_pre[0], value_pre[0]
     gain = value_gain[None]
-
     swap = [(k * seqs + a, a * seqs + k) for k in range(planes) for a in range(seqs)]
-    high = spatial_bias.astype(BF16)
-    middle = (spatial_bias - high.astype(F32)).astype(BF16)
-    low = (spatial_bias - high.astype(F32) - middle.astype(F32)).astype(BF16)
-    pad = jnp.zeros((5, slab * seqs), BF16)
-    own = jnp.concatenate([spatial_weight[0], high, middle, low, pad], axis=0)
-    own = lax.ppermute(own, Z_DP, swap)
-    bias = jnp.sum(own[slab : slab + 3].astype(F32), axis=0)
-    weights = lax.all_gather(own[:slab], Z, axis=0, tiled=True)
-
+
+    def exchange(x):
+        return lax.all_to_all(x, PLANE, split_axis=0, concat_axis=0, tiled=True)
+
+    weights = lax.ppermute(spatial_weight[0], Z_DP, swap)
+    weights = lax.all_gather(weights, Z, axis=0, tiled=True)
     sent, inv = prologue(cot, up, val, gain)
-    recv = lax.all_to_all(sent, PLANE, split_axis=0, concat_axis=0, tiled=True)
+    recv = exchange(sent)
+    bias = lax.ppermute(spatial_bias, Z_DP, swap)
+    bias = jnp.broadcast_to(bias.reshape(block, 1), (block, LANES))
     up_slope, val_slope, act = slopes(up, val)
-
-    grads = weight_grads(recv, seqs, parts, slab, F32)
+    grads, back, sums = core(recv, weights, bias, seqs, parts)
     grads = lax.psum_scatter(grads, Z, scatter_dimension=0, tiled=True)
+    back = exchange(back)
+    sums = lax.psum(sums, Z)
     grads = lax.ppermute(grads, Z_DP, swap)
-
-    bias_col = jnp.broadcast_to(bias[:, None], (bias.shape[0], LANES))
-    back, gain_part = mix(recv, weights, bias_col, seqs, parts)
-    back = lax.all_to_all(back, PLANE, split_axis=0, concat_axis=0, tiled=True)
-    gain_part = lax.psum(jnp.sum(gain_part, axis=0, keepdims=True), Z)
-    gain_grad = lax.all_gather(gain_part, PLANE, axis=0, tiled=True).reshape(-1) / value_gain
+    small = pack(sums, seqs, parts)
+    small = exchange(small)
+    gain_grad = small[:, 0].reshape(-1) / value_gain
+    mine = lax.axis_index(Z) * parts + lax.axis_index("sp_1")
+    bias_grad = lax.dynamic_slice_in_dim(small, mine, 1, axis=0)[:, 1]
     up_grad, value_grad = epilogue(back, cot, up_slope, val_slope, act, inv, gain)
-    return (
-        up_grad[None],
-        value_grad[None],
-        grads[None, :slab].astype(F32),
-        grads[slab : slab + 1, :slab].astype(F32),
-        gain_grad,
-    )
+    return (up_grad[None], value_grad[None], grads[None].astype(F32), bias_grad, gain_grad)
 
 
 def solution(mesh):

time: 264 us -> 230 us (0.87); the launches traced: 264 us -> 226 us
  blocking collectives: 71.1 us -> 36.5 us
  waiting for transfers between devices: 95.9 us -> 102 us
  Pallas kernels: 52.6 us -> 46.6 us
  starting transfers between devices: 25.9 us -> 22.2 us
    all_gather x1, waiting for transfers between devices: 0.02 us -> 49 us  [shards(): weights = lax.all_gather(weights, Z, axis=0, tiled=True)]
    reduce_scatter x1, waiting for transfers between devices: 41 us -> 0.01 us  [shards(): grads = lax.psum_scatter(grads, Z, scatter_dimension=0, tiled=True)]
    all_gather x1 -> x0, blocking collectives: 36.4 us -> none  [shards(): lax.all_gather(gain_part, PLANE, axis=0, tiled=True).reshape(-1)]
    all_to_all x0 -> x1, blocking collectives: none -> 22.3 us  [exchange(): return lax.all_to_all(x, PLANE, split_axis=0, concat_axis=0, tiled=True)]
    psum x1, blocking collectives: 34.7 us -> 14.2 us  [shards(): sums = lax.psum(sums, Z)]
    all_to_all x2, starting transfers between devices: 20.1 us -> 13.7 us  [exchange(): return lax.all_to_all(x, PLANE, split_axis=0, concat_axis=0, tiled=True)]
    pallas_call x2, Pallas kernels: 21.3 us -> 15.2 us  [the longest x1 13.8 us: core(): pl.pallas_call(functools.partial(core_kernel, seqs, parts), grid=(parts,)...]
    all_to_all x2, waiting for transfers between devices: 49.6 us -> 45.5 us  [exchange(): return lax.all_to_all(x, PLANE, split_axis=0, concat_axis=0, tiled=True)]
  transfers between devices with their start and end apart: 6 -> 7, of which waited for: 3 -> 4; matrix products, arithmetic and copies ran while one was open for 1% -> 1% of each run, Pallas kernels for 16% -> 10%
where the time goes in v2:
time: 230 us; the launch traced here: 226 us
  waiting for transfers between devices  102 us (44%)
  Pallas kernels  46.6 us (20%)
  blocking collectives  36.5 us (16%)
  starting transfers between devices  22.2 us (10%)
  between operations  14.1 us (6%)
  local copies, waits for them, and re-layouts  3.02 us (1%)
    all_gather x1, waiting for transfers between devices, shards(): weights = lax.all_gather(weights, Z, axis=0, tiled=True)  49 us
    all_to_all x2, waiting for transfers between devices, exchange(): return lax.all_to_all(x, PLANE, split_axis=0, concat_axis=0, tiled=True)  45.5 us
    all_to_all x1, blocking collectives, exchange(): return lax.all_to_all(x, PLANE, split_axis=0, concat_axis=0, tiled=True)  22.3 us
    psum x1, blocking collectives, shards(): sums = lax.psum(sums, Z)  14.2 us
    pallas_call x1, Pallas kernels, core(): pl.pallas_call(functools.partial(core_kernel, seqs, parts), grid=(parts,)...  13.8 us
    all_to_all x2, starting transfers between devices, exchange(): return lax.all_to_all(x, PLANE, split_axis=0, concat_axis=0, tiled=True)  13.7 us
    pallas_call x1, Pallas kernels, epilogue(): pl.pallas_call(functools.partial(epilogue_kernel, groups), grid=(toks //...  11.7 us
    pallas_call x1, Pallas kernels, slopes(): pl.pallas_call(slopes_kernel, grid=(toks // rows,), in_specs=[row, row],...  10.3 us
  transfers between devices with their start and end apart: 7, of which 4 were waited for; matrix products, arithmetic and copies ran while one was open for 1% of the time, Pallas kernels for 10%

profile of v2, /device:TPU:1, one launch (start us, length us, event | category | flops | bytes accessed | tf_op | source)
XLA Modules:
  0.0 225.9 jit_solution(13230042674727409585)
XLA Ops:
  7.2 9.4 %prologue.1 = (bf16[32,2,256,128]{3,2,1,0:T(8,128)(2,1)}, f32[256,128]{1,0:T(8,128)}) custom-call(bf16[256,4096]{1,0:T(8,128)(2,1)} %bitcast.19, bf16[256,4096]{1,0:T(8,128)(2,1)} %bitcast.15, bf16[256,4096]{1,0:T(8,128)(2,1)} %bitcast.17, f32[1,4096]{1,0:T(1,128)} %bitcast.22), custom_call_target="tpu_custom_call" | custom-call | flops 104857600 | bytes 10485760 | tf_op jit(solution)/shard_map/prologue/pallas_call | solution.py:66
  16.6 8.8 %all-to-all-start = ((bf16[32,2,256,128]{3,2,1,0:T(8,128)(2,1)}), bf16[32,2,256,128]{3,2,1,0:T(8,128)(2,1)}, u32[]{:S(2)}, u32[]{:S(2)}) async-start(bf16[32,2,256,128]{3,2,1,0:T(8,128)(2,1)} %get-tuple-element.15), calls=%async_computation | async-start | bytes 8388608 | tf_op jit(solution)/shard_map/all_to_all | solution.py:287
  25.4 0.0 all-gather.2.cloned.1.call-start
  25.4 0.0 copy-done.2
  25.4 3.7 %collective-permute-start = (bf16[128,1024]{1,0:T(8,128)(2,1)S(1)}, bf16[128,1024]{1,0:T(8,128)(2,1)S(1)}, u32[]{:S(2)}, u32[]{:S(2)}) collective-permute-start(bf16[128,1024]{1,0:T(8,128)(2,1)S(1)} %bitcast.28), channel_id=1, source_target_pairs={{0,0},{1,32},{2,64},{3,96},{4,128},{5,160},{6,192},{7,224},{32,1},... | collective-permute-start | bytes 786440 | tf_op jit(solution)/shard_map/ppermute | solution.py:289
  29.2 5.0 %collective-permute-done = bf16[128,1024]{1,0:T(8,128)(2,1)S(1)} collective-permute-done((bf16[128,1024]{1,0:T(8,128)(2,1)S(1)}, bf16[128,1024]{1,0:T(8,128)(2,1)S(1)}, u32[]{:S(2)}, u32[]{:S(2)}) %collective-permute-start) | collective-permute-done | bytes 262176 | tf_op jit(solution)/shard_map/ppermute | solution.py:289
  34.1 0.7 copy-done
  34.8 0.0 all-gather.2.cloned.1.call-update
  34.9 0.0 reduce-scatter.2.cloned.1.call-start
  34.9 0.0 copy-done.3
  34.9 2.7 %collective-permute-start.1 = (f32[1,1024]{1,0:T(1,128)S(1)}, f32[1,1024]{1,0:T(1,128)S(1)}, u32[]{:S(2)}, u32[]{:S(2)}) collective-permute-start(f32[1,1024]{1,0:T(1,128)S(1)} %copy-done.3), channel_id=1, source_target_pairs={{0,0},{1,32},{2,64},{3,96},{4,128},{5,160},{6,192},{7,224},{32,1},... | collective-permute-start | bytes 12296 | tf_op jit(solution)/shard_map/ppermute | solution.py:293
  37.6 2.6 %collective-permute-done.1 = f32[1,1024]{1,0:T(1,128)S(1)} collective-permute-done((f32[1,1024]{1,0:T(1,128)S(1)}, f32[1,1024]{1,0:T(1,128)S(1)}, u32[]{:S(2)}, u32[]{:S(2)}) %collective-permute-start.1) | collective-permute-done | bytes 4128 | tf_op jit(solution)/shard_map/ppermute | solution.py:293
  40.2 49.0 %all-gather.2.cloned.1.call-done.w_ref = bf16[1024,1024]{1,0:T(8,128)(2,1)} async-done(((bf16[128,1024]{1,0:T(8,128)(2,1)}), bf16[1024,1024]{1,0:T(8,128)(2,1)}) %all-gather.2.cloned.1.call-update) | async-done | bytes 2097168 | tf_op jit(solution)/shard_map/all_gather | solution.py:290
  89.2 0.0 all-to-all-done.recv_ref
  89.2 1.0 broadcast_in_dim.19.bias_ref
  90.2 13.8 %core.1 = (bf16[1024,1024]{1,0:T(8,128)(2,1)}, bf16[8,4,2,256,128]{4,3,2,1,0:T(8,128)(2,1)}, f32[8,1152]{1,0:T(8,128)}) custom-call(bf16[32,2,256,128]{3,2,1,0:T(8,128)(2,1)} %all-to-all-done.recv_ref, bf16[1024,1024]{1,0:T(8,128)(2,1)} %all-gather.2.cloned.1.call-done.w_ref, f32[1024,128]{1,0:T(8,128)} %broadcast_in_dim.19.bias_ref), custom_call_target="tpu_custom_call" | custom-call | flops 6442450944 | bytes 12582912 | tf_op jit(solution)/shard_map/core/pallas_call | solution.py:173
  104.1 0.0 reduce-scatter.2.cloned.1.call-update
  104.1 0.8 slice.9
  104.9 14.2 %psum.7.sums_ref = f32[1,1152]{1,0:T(1,128)} all-reduce(f32[1,1152]{1,0:T(1,128)S(1)} %slice.9), channel_id=1, replica_groups=mesh['sp_0'=8,'sp_1'=4,'dp_0'=4,'dp_1'=2] {'sp_0'}, use_global_device_ids=true, to_apply=%region_1.0 | all-reduce | flops 1152 | bytes 9216 | tf_op jit(solution)/shard_map/psum | solution.py:299
  119.1 1.4 pack.1
  120.4 22.3 %all_to_all.15 = f32[32,8,128]{2,1,0:T(8,128)S(1)} all-to-all(f32[32,8,128]{2,1,0:T(8,128)} %pack.1), channel_id=1, replica_groups=mesh['sp_0'=8,'sp_1'=4,'dp_0'=4,'dp_1'=2] {'dp_0','dp_1','sp_1'}, dimensions={0} | all-to-all | bytes 262144 | tf_op jit(solution)/shard_map/all_to_all | solution.py:287
  142.7 5.0 %all-to-all-start.1 = ((bf16[32,2,256,128]{3,2,1,0:T(8,128)(2,1)}), bf16[32,2,256,128]{3,2,1,0:T(8,128)(2,1)}, u32[]{:S(2)}, u32[]{:S(2)}) async-start(bf16[32,2,256,128]{3,2,1,0:T(8,128)(2,1)} %bitcast.21), calls=%async_computation.1 | async-start | bytes 8388608 | tf_op jit(solution)/shard_map/all_to_all | solution.py:287
  147.7 0.0 copy-start.1
  147.7 10.3 %slopes.1 = (f32[256,4096]{1,0:T(8,128)}, f32[256,4096]{1,0:T(8,128)}, f32[256,4096]{1,0:T(8,128)}) custom-call(bf16[256,4096]{1,0:T(8,128)(2,1)} %bitcast.16, bf16[256,4096]{1,0:T(8,128)(2,1)} %bitcast.18), custom_call_target="tpu_custom_call" | custom-call | flops 104857600 | bytes 16777216 | tf_op jit(solution)/shard_map/slopes/pallas_call | solution.py:107
  158.0 1.9 collective-permute-start.2
  160.0 0.0 copy-done.1
  160.0 0.6 div.3
  160.6 0.5 slice_bitcast_fusion
  161.1 45.5 %all-to-all-done.1.recv_ref = bf16[32,2,256,128]{3,2,1,0:T(8,128)(2,1)} async-done(((bf16[32,2,256,128]{3,2,1,0:T(8,128)(2,1)}), bf16[32,2,256,128]{3,2,1,0:T(8,128)(2,1)}, u32[]{:S(2)}, u32[]{:S(2)}) %all-to-all-start.1) | async-done | bytes 4194336 | tf_op jit(solution)/shard_map/all_to_all | solution.py:287
  206.6 11.7 %epilogue.1 = (bf16[256,4096]{1,0:T(8,128)(2,1)}, bf16[256,4096]{1,0:T(8,128)(2,1)}) custom-call(bf16[32,2,256,128]{3,2,1,0:T(8,128)(2,1)} %all-to-all-done.1.recv_ref, bf16[256,4096]{1,0:T(8,128)(2,1)} %bitcast.20, f32[256,4096]{1,0:T(8,128)} %get-tuple-element.17.up_slope_ref, f32[256,4096]{1,0:T(8,128)} %get-tuple-element.18.val_slope_ref, ...), custom_call_target="tpu_custom_call" | custom-call | flops 20971520 | bytes 23068672 | tf_op jit(solution)/shard_map/epilogue/pallas_call | solution.py:233
  218.2 0.0 collective-permute-done.2
  218.3 0.8 bitcast_convert_fusion
  (6 shorter events, 0.0 us)
Async XLA Ops:
  16.6 8.8 %copy-start.2 = (bf16[1,128,1024]{2,1,0:T(8,128)(2,1)S(1)}, bf16[1,128,1024]{2,1,0:T(8,128)(2,1)}, u32[]{:S(2)}) copy-start(bf16[1,128,1024]{2,1,0:T(8,128)(2,1)} %param.9) | copy-start | bytes 786436
  16.6 18.4 %copy-start.3 = (f32[1,1024]{1,0:T(1,128)S(1)}, f32[1,1024]{1,0:T(1,128)}, u32[]{:S(2)}) copy-start(f32[1,1024]{1,0:T(1,128)} %param.10) | copy-start | bytes 12292
  16.6 72.7 %all-to-all-start = ((bf16[32,2,256,128]{3,2,1,0:T(8,128)(2,1)}), bf16[32,2,256,128]{3,2,1,0:T(8,128)(2,1)}, u32[]{:S(2)}, u32[]{:S(2)}) async-start(bf16[32,2,256,128]{3,2,1,0:T(8,128)(2,1)} %get-tuple-element.15), calls=%async_computation | async-start | bytes 8388608 | tf_op jit(solution)/shard_map/all_to_all | solution.py:287
  25.4 63.9 %all-gather.2.cloned.1.call-start = ((), (), s32[]{:S(2)}) async-start(), calls=%async_computation.4 | async-start | bytes 2359296 | tf_op jit(solution)/shard_map/all_gather | solution.py:290
  25.4 8.7 %collective-permute-start = (bf16[128,1024]{1,0:T(8,128)(2,1)S(1)}, bf16[128,1024]{1,0:T(8,128)(2,1)S(1)}, u32[]{:S(2)}, u32[]{:S(2)}) collective-permute-start(bf16[128,1024]{1,0:T(8,128)(2,1)S(1)} %bitcast.28), channel_id=1, source_target_pairs={{0,0},{1,32},{2,64},{3,96},{4,128},{5,160},{6,192},{7,224},{32,1},... | collective-permute-start | bytes 786440 | tf_op jit(solution)/shard_map/ppermute | solution.py:289
  34.1 0.7 copy-start
  34.9 123.2 %reduce-scatter.2.cloned.1.call-start = ((), (), s32[]{:S(2)}) async-start(), calls=%async_computation.5 | async-start | bytes 2359296 | tf_op jit(solution)/shard_map/reduce_scatter | solution.py:297
  34.9 5.3 %collective-permute-start.1 = (f32[1,1024]{1,0:T(1,128)S(1)}, f32[1,1024]{1,0:T(1,128)S(1)}, u32[]{:S(2)}, u32[]{:S(2)}) collective-permute-start(f32[1,1024]{1,0:T(1,128)S(1)} %copy-done.3), channel_id=1, source_target_pairs={{0,0},{1,32},{2,64},{3,96},{4,128},{5,160},{6,192},{7,224},{32,1},... | collective-permute-start | bytes 12296 | tf_op jit(solution)/shard_map/ppermute | solution.py:293
  142.7 63.8 %all-to-all-start.1 = ((bf16[32,2,256,128]{3,2,1,0:T(8,128)(2,1)}), bf16[32,2,256,128]{3,2,1,0:T(8,128)(2,1)}, u32[]{:S(2)}, u32[]{:S(2)}) async-start(bf16[32,2,256,128]{3,2,1,0:T(8,128)(2,1)} %bitcast.21), calls=%async_computation.1 | async-start | bytes 8388608 | tf_op jit(solution)/shard_map/all_to_all | solution.py:287
  147.7 12.3 %copy-start.1 = (f32[4096]{0:T(1024)S(1)}, f32[4096]{0:T(1024)}, u32[]{:S(2)}) copy-start(f32[4096]{0:T(1024)} %param.11) | copy-start | bytes 49156
  158.0 60.2 %collective-permute-start.2 = (bf16[128,1024]{1,0:T(8,128)(2,1)}, bf16[128,1024]{1,0:T(8,128)(2,1)S(1)}, u32[]{:S(2)}, u32[]{:S(2)}) collective-permute-start(bf16[128,1024]{1,0:T(8,128)(2,1)} %reduce-scatter.2.cloned.1.call-done), channel_id=1, source_target_pairs={{0,0},{1,32},{2,64},{3,96},{4,128},{5,160},{6,192},{7,224},{32,1},... | collective-permute-start | bytes 786440 | tf_op jit(solution)/shard_map/ppermute | solution.py:300
Sparse Core Ops, SparseCore 0:
  35.0 54.2 all-gather.1
  104.2 40.9 reduce-scatter.1

commit v3 on v2

--- a/solution.py
+++ b/solution.py
@@ -90,11 +90,13 @@
     def step(g, carry):
         at = pl.ds(pl.multiple_of(g * LANES, LANES), LANES)
         up = up_ref[:, at].astype(F32)
-        up_slope_ref[:, at] = normal_cdf(up) + up * (jnp.exp(-0.5 * up * up) * inv_root_tau)
+        up_slope = normal_cdf(up) + up * (jnp.exp(-0.5 * up * up) * inv_root_tau)
+        up_slope_ref[:, at] = up_slope.astype(BF16)
         val = val_ref[:, at].astype(F32)
         phi = normal_cdf(val)
-        act_ref[:, at] = val * phi
-        val_slope_ref[:, at] = phi + val * (jnp.exp(-0.5 * val * val) * inv_root_tau)
+        act_ref[:, at] = (val * phi).astype(BF16)
+        val_slope = phi + val * (jnp.exp(-0.5 * val * val) * inv_root_tau)
+        val_slope_ref[:, at] = val_slope.astype(BF16)
         return carry
 
     lax.fori_loop(0, groups, step, 0, unroll=2)
@@ -103,7 +105,7 @@
 def slopes(up, val, rows=32):
     toks, width = up.shape
     row = pl.BlockSpec((rows, width), lambda i: (i, 0))
-    out = jax.ShapeDtypeStruct((toks, width), F32)
+    out = jax.ShapeDtypeStruct((toks, width), BF16)
     return pl.pallas_call(
         slopes_kernel,
         grid=(toks // rows,),
@@ -118,84 +120,182 @@
     )(up, val)
 
 
-def core_kernel(
-    seqs, parts, recv_ref, w_ref, bias_ref, grad_ref, out_ref, sums_ref, gate_ref, value_ref
-):
-    y = pl.program_id(0)
+def mix_kernel(seqs, parts, *refs):
+    recv_ref, *w_refs = refs[: 1 + seqs]
+    bias_ref, out_ref, sums_ref, gate_ref, value_ref, w_ref, mixed_ref, back_ref, sems = refs[1 + seqs :]
     toks = recv_ref.shape[2]
-
-    @pl.when(y == 0)
-    def _():
+    block = parts * toks
+    slab = block // seqs
+    key = order_key()
+    gate_sem, value_sem, w_sem, back_sem, mixed_sem = (sems.at[k] for k in range(5))
+    for b in range(seqs):
+        cols = slice(b * LANES, (b + 1) * LANES)
+        pieces = slice(b * parts, (b + 1) * parts)
+        pltpu.make_async_copy(recv_ref.at[pieces, 0], gate_ref.at[:, :, cols], gate_sem).start()
+    for d in range(seqs):
+        rows = pl.ds(pl.multiple_of((d ^ key) * slab, slab), slab)
+        pltpu.make_async_copy(w_refs[d], w_ref.at[rows], w_sem).start()
+    for b in range(seqs):
+        cols = slice(b * LANES, (b + 1) * LANES)
+        pieces = slice(b * parts, (b + 1) * parts)
+        pltpu.make_async_copy(recv_ref.at[pieces, 1], value_ref.at[:, :, cols], value_sem).start()
+    pltpu.make_async_copy(gate_ref, gate_ref, gate_sem).wait()
+    pltpu.make_async_copy(w_ref, w_ref, w_sem).wait()
+
+    gate = gate_ref[...].reshape(block, seqs * LANES)
+    across = (((1,), (1,)), ((), ()))
+    ones = jnp.ones((8, seqs * LANES), BF16)
+    bias_sums = lax.dot_general(ones, gate, across, preferred_element_type=F32)
+    sums_ref[:, LANES:] = bias_sums[:1]
+
+    def back_step(y, carry):
+        at = pl.ds(pl.multiple_of(y * toks, toks), toks)
+        back_ref[y] = lax.dot_general(
+            w_ref[:, at],
+            gate_ref[...].reshape(block, seqs * LANES),
+            (((0,), (0,)), ((), ())),
+            preferred_element_type=F32,
+        ).astype(BF16)
         for b in range(seqs):
-            for k in range(parts):
-                rows, cols = pl.ds(k * toks, toks), pl.ds(b * LANES, LANES)
-                gate_ref[rows, cols] = recv_ref[b * parts + k, 0]
-                value_ref[rows, cols] = recv_ref[b * parts + k, 1]
-
-    at = pl.ds(pl.multiple_of(y * toks, toks), toks)
-    across = (((1,), (1,)), ((), ()))
-    gate = gate_ref[at]
-    grad_ref[...] = lax.dot_general(
-        gate, value_ref[...], across, preferred_element_type=F32
-    ).astype(grad_ref.dtype)
-    ones = jnp.ones((8, gate.shape[1]), BF16)
-    shift = pl.ds(pl.multiple_of(LANES + y * toks, LANES), toks)
-    sums_ref[:, shift] = lax.dot_general(ones, gate, across, preferred_element_type=F32)
-    back = lax.dot_general(
-        w_ref[:, at], gate_ref[...], (((0,), (0,)), ((), ())), preferred_element_type=F32
-    ).astype(BF16)
-    terms = back.astype(F32) * value_ref[at].astype(F32)
-    total = jnp.zeros((8, LANES), F32)
-    for b in range(seqs):
-        out_ref[b, 0, 1] = back[:, b * LANES : (b + 1) * LANES]
-        total += jnp.sum(
-            terms[:, b * LANES : (b + 1) * LANES].reshape(toks // 8, 8, LANES), axis=0
+            cols = slice(b * LANES, (b + 1) * LANES)
+            pltpu.make_async_copy(back_ref.at[y, :, cols], out_ref.at[b, y, 1], back_sem).start()
+        return carry
+
+    lax.fori_loop(0, parts, back_step, 0)
+    pltpu.make_async_copy(value_ref, value_ref, value_sem).wait()
+
+    def mixed_step(y, total):
+        at = pl.ds(pl.multiple_of(y * toks, toks), toks)
+        mixed = jnp.dot(
+            w_ref[at], value_ref[...].reshape(block, seqs * LANES), preferred_element_type=F32
         )
-    total = jnp.broadcast_to(jnp.sum(total, axis=0, keepdims=True), (8, LANES))
-
-    @pl.when(y == 0)
-    def _():
-        sums_ref[:, :LANES] = total
-
-    @pl.when(y > 0)
-    def _():
-        sums_ref[:, :LANES] += total
-
-    mixed = jnp.dot(w_ref[at], value_ref[...], preferred_element_type=F32)
-    mixed = (mixed + bias_ref[at, :1]).astype(BF16)
-    for b in range(seqs):
-        out_ref[b, 0, 0] = mixed[:, b * LANES : (b + 1) * LANES]
-
-
-def core(recv, w, bias, seqs, parts):
+        mixed_ref[y] = (mixed + bias_ref[at, :1]).astype(BF16)
+        for b in range(seqs):
+            cols = slice(b * LANES, (b + 1) * LANES)
+            pltpu.make_async_copy(mixed_ref.at[y, :, cols], out_ref.at[b, y, 0], mixed_sem).start()
+            terms = back_ref[y, :, cols].astype(F32) * value_ref[y, :, cols].astype(F32)
+            total += jnp.sum(terms.reshape(toks // 8, 8, LANES), axis=0)
+        return total
+
+    total = lax.fori_loop(0, parts, mixed_step, jnp.zeros((8, LANES), F32))
+    sums_ref[:, :LANES] = jnp.sum(total, axis=0, keepdims=True)
+    pltpu.make_async_copy(back_ref, back_ref, back_sem).wait()
+    pltpu.make_async_copy(mixed_ref, mixed_ref, mixed_sem).wait()
+
+
+def order_key():
+    return lax.axis_index(Z) ^ (lax.axis_index("dp_0") * 2 + lax.axis_index("dp_1"))
+
+
+ANY = pl.BlockSpec(memory_space=pl.ANY)
+VMEM = pl.BlockSpec(memory_space=pltpu.VMEM)
+
+
+def mix(recv, pieces, bias, seqs, parts):
     toks = recv.shape[2]
     block = parts * toks
-    grads, out, sums = pl.pallas_call(
-        functools.partial(core_kernel, seqs, parts),
-        grid=(parts,),
-        in_specs=[
-            pl.BlockSpec(recv.shape, lambda y: (0, 0, 0, 0)),
-            pl.BlockSpec(w.shape, lambda y: (0, 0)),
-            pl.BlockSpec(bias.shape, lambda y: (0, 0)),
-        ],
-        out_specs=[
-            pl.BlockSpec((toks, block), lambda y: (y, 0)),
-            pl.BlockSpec((seqs, 1, 2, toks, LANES), lambda y: (0, y, 0, 0, 0)),
-            pl.BlockSpec((8, LANES + block), lambda y: (0, 0)),
-        ],
+    flat = pltpu.VMEM((parts, toks, seqs * LANES), BF16)
+    out, sums = pl.pallas_call(
+        functools.partial(mix_kernel, seqs, parts),
+        in_specs=[ANY] * (1 + seqs) + [VMEM],
+        out_specs=[ANY, VMEM],
         out_shape=[
-            jax.ShapeDtypeStruct((block, block), BF16),
             jax.ShapeDtypeStruct((seqs, parts, 2, toks, LANES), BF16),
-            jax.ShapeDtypeStruct((8, LANES + block), F32),
-        ],
-        scratch_shapes=[pltpu.VMEM((block, seqs * LANES), BF16)] * 2,
+            jax.ShapeDtypeStruct((1, LANES + block), F32),
+        ],
+        scratch_shapes=[
+            flat,
+            flat,
+            pltpu.VMEM((block, block), BF16),
+            flat,
+            flat,
+            pltpu.SemaphoreType.DMA((5,)),
+        ],
+        compiler_params=pltpu.CompilerParams(vmem_limit_bytes=60 * 1024 * 1024),
+        cost_estimate=pl.CostEstimate(
+            flops=4 * block * block * seqs * LANES, bytes_accessed=10 * block * block, transcendentals=0
+        ),
+        name="mix",
+    )(recv, *pieces, bias)
+    return out.reshape(recv.shape), sums
+
+
+def grads_kernel(seqs, parts, recv_ref, *refs):
+    outs = refs[:seqs]
+    gate_ref, value_ref, grad_ref, sems = refs[seqs:]
+    toks = recv_ref.shape[2]
+    block = parts * toks
+    slab = block // seqs
+    key = order_key()
+    for b in range(seqs):
+        cols = slice(b * LANES, (b + 1) * LANES)
+        pieces = slice(b * parts, (b + 1) * parts)
+        pltpu.make_async_copy(recv_ref.at[pieces, 0], gate_ref.at[:, :, cols], sems.at[0]).start()
+        pltpu.make_async_copy(recv_ref.at[pieces, 1], value_ref.at[:, :, cols], sems.at[1]).start()
+    pltpu.make_async_copy(gate_ref, gate_ref, sems.at[0]).wait()
+    pltpu.make_async_copy(value_ref, value_ref, sems.at[1]).wait()
+
+    def step(y, carry):
+        grad = lax.dot_general(
+            gate_ref[...].reshape(block, seqs * LANES),
+            value_ref[y],
+            (((1,), (1,)), ((), ())),
+            preferred_element_type=F32,
+        )
+        grad_ref[y] = grad.astype(BF16)
+        at = pl.ds(pl.multiple_of(y * toks, toks), toks)
+        for d in range(seqs):
+            rows = pl.ds(pl.multiple_of((d ^ key) * slab, slab), slab)
+            pltpu.make_async_copy(grad_ref.at[y, rows], outs[d].at[:, at], sems.at[2]).start()
+        return carry
+
+    lax.fori_loop(0, parts, step, 0)
+    pltpu.make_async_copy(grad_ref, grad_ref, sems.at[2]).wait()
+
+
+def weight_grads(recv, seqs, parts):
+    toks = recv.shape[2]
+    block = parts * toks
+    flat = pltpu.VMEM((parts, toks, seqs * LANES), BF16)
+    return pl.pallas_call(
+        functools.partial(grads_kernel, seqs, parts),
+        in_specs=[ANY],
+        out_specs=[ANY] * seqs,
+        out_shape=[jax.ShapeDtypeStruct((block // seqs, block), BF16)] * seqs,
+        scratch_shapes=[
+            flat,
+            flat,
+            pltpu.VMEM((parts, block, toks), BF16),
+            pltpu.SemaphoreType.DMA((3,)),
+        ],
+        compiler_params=pltpu.CompilerParams(vmem_limit_bytes=60 * 1024 * 1024),
+        cost_estimate=pl.CostEstimate(
+            flops=2 * block * block * seqs * LANES, bytes_accessed=6 * block * block, transcendentals=0
+        ),
+        name="weight_grads",
+    )(recv)
+
+
+def add_kernel(*refs):
+    *ins, out_ref = refs
+    out_ref[...] = sum(r[...].astype(F32) for r in ins).astype(BF16)
+
+
+def add(pieces, rows=32):
+    height, width = pieces[0].shape
+    row = pl.BlockSpec((rows, width), lambda i: (i, 0))
+    return pl.pallas_call(
+        add_kernel,
+        grid=(height // rows,),
+        in_specs=[row] * len(pieces),
+        out_specs=row,
+        out_shape=jax.ShapeDtypeStruct((height, width), BF16),
         compiler_params=params(60),
         cost_estimate=pl.CostEstimate(
-            flops=6 * block * block * seqs * LANES, bytes_accessed=12 * block * block, transcendentals=0
-        ),
-        name="core",
-    )(recv, w, bias)
-    return grads, out.reshape(recv.shape), sums[:1]
+            flops=9 * height * width, bytes_accessed=18 * height * width, transcendentals=0
+        ),
+        name="add",
+    )(*pieces)
 
 
 def epilogue_kernel(
@@ -206,9 +306,9 @@
     def first(g, dots):
         at = pl.ds(pl.multiple_of(g * LANES, LANES), LANES)
         mid = (cot_ref[:, at].astype(F32) * recv_ref[g, 0].astype(F32)).astype(BF16)
-        up_ref[:, at] = (mid.astype(F32) * up_slope_ref[:, at]).astype(BF16)
+        up_ref[:, at] = (mid.astype(F32) * up_slope_ref[:, at].astype(F32)).astype(BF16)
         scaled = recv_ref[g, 1].astype(F32) * gain_ref[:, at]
-        return dots + scaled * act_ref[:, at]
+        return dots + scaled * act_ref[:, at].astype(F32)
 
     dots = lax.fori_loop(0, groups, first, jnp.zeros((rows, LANES), F32), unroll=2)
     mean = jnp.sum(dots, axis=1, keepdims=True) * (1.0 / (groups * LANES))
@@ -218,8 +318,8 @@
     def second(g, carry):
         at = pl.ds(pl.multiple_of(g * LANES, LANES), LANES)
         scaled = recv_ref[g, 1].astype(F32) * gain_ref[:, at]
-        slope = inv * scaled - pull * act_ref[:, at]
-        val_ref[:, at] = (slope * val_slope_ref[:, at]).astype(BF16)
+        slope = inv * scaled - pull * act_ref[:, at].astype(F32)
+        val_ref[:, at] = (slope * val_slope_ref[:, at].astype(F32)).astype(BF16)
         return carry
 
     lax.fori_loop(0, groups, second, 0, unroll=4)
@@ -281,23 +381,29 @@
     block = spatial_weight.shape[2]
     cot, up, val = cotangent[0], up_pre[0], value_pre[0]
     gain = value_gain[None]
-    swap = [(k * seqs + a, a * seqs + k) for k in range(planes) for a in range(seqs)]
+    away = [(z * seqs + a, (z ^ a) * seqs + z) for z in range(planes) for a in range(seqs)]
+    home = [(there, here) for here, there in away]
 
     def exchange(x):
         return lax.all_to_all(x, PLANE, split_axis=0, concat_axis=0, tiled=True)
 
-    weights = lax.ppermute(spatial_weight[0], Z_DP, swap)
-    weights = lax.all_gather(weights, Z, axis=0, tiled=True)
+    def across(x, d):
+        return lax.ppermute(x, Z, [(z, z ^ d) for z in range(planes)])
+
+    weights = lax.ppermute(spatial_weight[0], Z_DP, away)
     sent, inv = prologue(cot, up, val, gain)
     recv = exchange(sent)
-    bias = lax.ppermute(spatial_bias, Z_DP, swap)
+    pieces = [weights] + [across(weights, d) for d in range(1, planes)]
+    bias = lax.ppermute(spatial_bias, Z_DP, away)
     bias = jnp.broadcast_to(bias.reshape(block, 1), (block, LANES))
     up_slope, val_slope, act = slopes(up, val)
-    grads, back, sums = core(recv, weights, bias, seqs, parts)
-    grads = lax.psum_scatter(grads, Z, scatter_dimension=0, tiled=True)
+    back, sums = mix(recv, pieces, bias, seqs, parts)
     back = exchange(back)
+    grads = weight_grads(recv, seqs, parts)
+    grads = [grads[0]] + [across(grads[d], d) for d in range(1, planes)]
+    grads = add(grads)
     sums = lax.psum(sums, Z)
-    grads = lax.ppermute(grads, Z_DP, swap)
+    grads = lax.ppermute(grads, Z_DP, home)
     small = pack(sums, seqs, parts)
     small = exchange(small)
     gain_grad = small[:, 0].reshape(-1) / value_gain

time: 230 us -> 294 us (1.28)
  the two profiles are of different devices: /device:TPU:1 before, /device:TPU:7 now
where the time goes in v3:
time: 294 us; the launch traced here: 293 us
  starting transfers between devices  109 us (37%)
  waiting for transfers between devices  82.1 us (28%)
  Pallas kernels  51.8 us (18%)
  blocking collectives  45.3 us (15%)
    ppermute x14, waiting for transfers between devices, across(): return lax.ppermute(x, Z, [(z, z ^ d) for z in range(planes)])  49.1 us
    ppermute x14, starting transfers between devices, across(): return lax.ppermute(x, Z, [(z, z ^ d) for z in range(planes)])  46.1 us
    ppermute x1, starting transfers between devices, shards(): bias = lax.ppermute(spatial_bias, Z_DP, away)  38.4 us
    all_to_all x1, blocking collectives, exchange(): return lax.all_to_all(x, PLANE, split_axis=0, concat_axis=0, tiled=True)  33.7 us
    ppermute x1, waiting for transfers between devices, shards(): grads = lax.ppermute(grads, Z_DP, home)  20.3 us
    all_to_all x2, starting transfers between devices, exchange(): return lax.all_to_all(x, PLANE, split_axis=0, concat_axis=0, tiled=True)  14.9 us
    ppermute x1, waiting for transfers between devices, shards(): weights = lax.ppermute(spatial_weight[0], Z_DP, away)  12.1 us
    pallas_call x1, Pallas kernels, mix(): pl.pallas_call(functools.partial(mix_kernel, seqs, parts), in_specs=[ANY]...  12 us
  transfers between devices with their start and end apart: 19, of which 8 were waited for; matrix products, arithmetic and copies ran while one was open for 1% of the time, Pallas kernels for 6%

profile of v3, /device:TPU:7, one launch (start us, length us, event | category | flops | bytes accessed | tf_op | source)
XLA Modules:
  0.0 293.2 jit_solution(12695795780905400536)
XLA Ops:
  0.6 9.5 %prologue.1 = (bf16[32,2,256,128]{3,2,1,0:T(8,128)(2,1)}, f32[256,128]{1,0:T(8,128)}) custom-call(bf16[256,4096]{1,0:T(8,128)(2,1)} %bitcast.15, bf16[256,4096]{1,0:T(8,128)(2,1)} %bitcast.17, bf16[256,4096]{1,0:T(8,128)(2,1)} %bitcast.19, f32[1,4096]{1,0:T(1,128)} %bitcast.22), custom_call_target="tpu_custom_call" | custom-call | flops 104857600 | bytes 10485760 | tf_op jit(solution)/shard_map/prologue/pallas_call | solution.py:66
  10.1 8.1 %all-to-all-start = ((bf16[32,2,256,128]{3,2,1,0:T(8,128)(2,1)}), bf16[32,2,256,128]{3,2,1,0:T(8,128)(2,1)}, u32[]{:S(2)}, u32[]{:S(2)}) async-start(bf16[32,2,256,128]{3,2,1,0:T(8,128)(2,1)} %get-tuple-element.22), calls=%async_computation | async-start | bytes 8388608 | tf_op jit(solution)/shard_map/all_to_all | solution.py:388
  18.3 7.4 %collective-permute-start = (bf16[128,1024]{1,0:T(8,128)(2,1)S(1)}, bf16[128,1024]{1,0:T(8,128)(2,1)S(1)}, u32[]{:S(2)}, u32[]{:S(2)}) collective-permute-start(bf16[128,1024]{1,0:T(8,128)(2,1)S(1)} %bitcast.28), channel_id=1, source_target_pairs={{0,0},{1,32},{2,64},{3,96},{4,128},{5,160},{6,192},{7,224},{32,33}... | collective-permute-start | bytes 786440 | tf_op jit(solution)/shard_map/ppermute | solution.py:393
  25.7 12.1 %collective-permute-done.refs_1_ = bf16[128,1024]{1,0:T(8,128)(2,1)S(1)} collective-permute-done((bf16[128,1024]{1,0:T(8,128)(2,1)S(1)}, bf16[128,1024]{1,0:T(8,128)(2,1)S(1)}, u32[]{:S(2)}, u32[]{:S(2)}) %collective-permute-start) | collective-permute-done | bytes 262176 | tf_op jit(solution)/shard_map/ppermute | solution.py:393
  37.8 1.7 collective-permute-start.1
  39.5 1.6 collective-permute-start.2
  41.1 38.4 %collective-permute-start.8 = (f32[1,1024]{1,0:T(1,128)S(1)}, f32[1,1024]{1,0:T(1,128)S(1)}, u32[]{:S(2)}, u32[]{:S(2)}) collective-permute-start(f32[1,1024]{1,0:T(1,128)S(1)} %copy-done.17), channel_id=1, source_target_pairs={{0,0},{1,32},{2,64},{3,96},{4,128},{5,160},{6,192},{7,224},{32,33}... | collective-permute-start | bytes 12296 | tf_op jit(solution)/shard_map/ppermute | solution.py:397
  80.3 3.0 %collective-permute-start.5 = (bf16[128,1024]{1,0:T(8,128)(2,1)S(1)}, bf16[128,1024]{1,0:T(8,128)(2,1)S(1)}, u32[]{:S(2)}, u32[]{:S(2)}) collective-permute-start(bf16[128,1024]{1,0:T(8,128)(2,1)S(1)} %collective-permute-done.refs_1_), channel_id=1, source_target_pairs={{0,160},{32,128},{64,224},{96,192},{128,32},{160,0},{192,96},{224,... | collective-permute-start | bytes 786440 | tf_op jit(solution)/shard_map/ppermute | solution.py:391
  83.3 8.3 %collective-permute-start.6 = (bf16[128,1024]{1,0:T(8,128)(2,1)S(1)}, bf16[128,1024]{1,0:T(8,128)(2,1)S(1)}, u32[]{:S(2)}, u32[]{:S(2)}) collective-permute-start(bf16[128,1024]{1,0:T(8,128)(2,1)S(1)} %collective-permute-done.refs_1_), channel_id=1, source_target_pairs={{0,192},{32,224},{64,128},{96,160},{128,64},{160,96},{192,0},{224,... | collective-permute-start | bytes 786440 | tf_op jit(solution)/shard_map/ppermute | solution.py:391
  91.6 15.0 %collective-permute-start.7 = (bf16[128,1024]{1,0:T(8,128)(2,1)S(1)}, bf16[128,1024]{1,0:T(8,128)(2,1)S(1)}, u32[]{:S(2)}, u32[]{:S(2)}) collective-permute-start(bf16[128,1024]{1,0:T(8,128)(2,1)S(1)} %collective-permute-done.refs_1_), channel_id=1, source_target_pairs={{0,224},{32,192},{64,160},{96,128},{128,96},{160,64},{192,32},{224... | collective-permute-start | bytes 786440 | tf_op jit(solution)/shard_map/ppermute | solution.py:391
  106.6 3.4 %collective-permute-done.4.refs_5_ = bf16[128,1024]{1,0:T(8,128)(2,1)S(1)} collective-permute-done((bf16[128,1024]{1,0:T(8,128)(2,1)S(1)}, bf16[128,1024]{1,0:T(8,128)(2,1)S(1)}, u32[]{:S(2)}, u32[]{:S(2)}) %collective-permute-start.4) | collective-permute-done | bytes 262176 | tf_op jit(solution)/shard_map/ppermute | solution.py:391
  110.0 7.6 %collective-permute-done.5.refs_6_ = bf16[128,1024]{1,0:T(8,128)(2,1)S(1)} collective-permute-done((bf16[128,1024]{1,0:T(8,128)(2,1)S(1)}, bf16[128,1024]{1,0:T(8,128)(2,1)S(1)}, u32[]{:S(2)}, u32[]{:S(2)}) %collective-permute-start.5) | collective-permute-done | bytes 262176 | tf_op jit(solution)/shard_map/ppermute | solution.py:391
  117.6 7.1 %collective-permute-done.7.refs_8_ = bf16[128,1024]{1,0:T(8,128)(2,1)S(1)} collective-permute-done((bf16[128,1024]{1,0:T(8,128)(2,1)S(1)}, bf16[128,1024]{1,0:T(8,128)(2,1)S(1)}, u32[]{:S(2)}, u32[]{:S(2)}) %collective-permute-start.7) | collective-permute-done | bytes 262176 | tf_op jit(solution)/shard_map/ppermute | solution.py:391
  124.7 1.0 broadcast_in_dim.19.refs_9_
  125.7 12.0 %mix.1 = (bf16[8,4,2,256,128]{4,3,2,1,0:T(8,128)(2,1)}, f32[1,1152]{1,0:T(1,128)}) custom-call(bf16[32,2,256,128]{3,2,1,0:T(8,128)(2,1)} %all-to-all-done.refs_0_.recv_ref, bf16[128,1024]{1,0:T(8,128)(2,1)} %copy-done.9, bf16[128,1024]{1,0:T(8,128)(2,1)} %copy-done.10, bf16[128,1024]{1,0:T(8,128)(2,1)} %copy-done.11, bf16[128,1024]{1,0:T(8,128)(2,1)} %copy-done.12, ...), custom_call_target="tpu_custom_call" | custom-call | flops 4294967296 | bytes 10485760 | tf_op jit(solution)/shard_map/mix/pallas_call | solution.py:198
  137.7 11.6 %psum.7.sums_ref = f32[1,1152]{1,0:T(1,128)} all-reduce(f32[1,1152]{1,0:T(1,128)} %get-tuple-element.38), channel_id=1, replica_groups=mesh['sp_0'=8,'sp_1'=4,'dp_0'=4,'dp_1'=2] {'sp_0'}, use_global_device_ids=true, to_apply=%region_0.0 | all-reduce | flops 1152 | bytes 9216 | tf_op jit(solution)/shard_map/psum | solution.py:405
  149.3 1.4 pack.1
  150.7 33.7 %all_to_all.15 = f32[32,8,128]{2,1,0:T(8,128)S(1)} all-to-all(f32[32,8,128]{2,1,0:T(8,128)} %pack.1), channel_id=1, replica_groups=mesh['sp_0'=8,'sp_1'=4,'dp_0'=4,'dp_1'=2] {'dp_0','dp_1','sp_1'}, dimensions={0} | all-to-all | bytes 262144 | tf_op jit(solution)/shard_map/all_to_all | solution.py:388
  184.3 6.8 %all-to-all-start.1 = ((bf16[32,2,256,128]{3,2,1,0:T(8,128)(2,1)}), bf16[32,2,256,128]{3,2,1,0:T(8,128)(2,1)}, u32[]{:S(2)}, u32[]{:S(2)}) async-start(bf16[32,2,256,128]{3,2,1,0:T(8,128)(2,1)} %bitcast.21), calls=%async_computation.1 | async-start | bytes 8388608 | tf_op jit(solution)/shard_map/all_to_all | solution.py:388
  191.1 6.0 %weight_grads.1 = (bf16[128,1024]{1,0:T(8,128)(2,1)}, bf16[128,1024]{1,0:T(8,128)(2,1)}, bf16[128,1024]{1,0:T(8,128)(2,1)}, bf16[128,1024]{1,0:T(8,128)(2,1)}, b...) custom-call(bf16[32,2,256,128]{3,2,1,0:T(8,128)(2,1)} %all-to-all-do, ...), custom_call_target="tpu_custom_call" | custom-call | flops 2147483648 | bytes 6291456 | tf_op jit(solution)/shard_map/weight_grads/pallas_call | solution.py:260
  197.1 1.3 collective-permute-start.10
  198.8 3.4 %collective-permute-start.12 = (bf16[128,1024]{1,0:T(8,128)(2,1)}, bf16[128,1024]{1,0:T(8,128)(2,1)S(1)}, u32[]{:S(2)}, u32[]{:S(2)}) collective-permute-start(bf16[128,1024]{1,0:T(8,128)(2,1)} %get-tuple-element.34), channel_id=1, source_target_pairs={{0,128},{32,160},{64,192},{96,224},{128,0},{160,32},{192,64},{224,... | collective-permute-start | bytes 786440 | tf_op jit(solution)/shard_map/ppermute | solution.py:391
  202.2 1.8 collective-permute-start.13
  204.0 3.4 %collective-permute-start.14 = (bf16[128,1024]{1,0:T(8,128)(2,1)}, bf16[128,1024]{1,0:T(8,128)(2,1)S(1)}, u32[]{:S(2)}, u32[]{:S(2)}) collective-permute-start(bf16[128,1024]{1,0:T(8,128)(2,1)} %get-tuple-element.36), channel_id=1, source_target_pairs={{0,192},{32,224},{64,128},{96,160},{128,64},{160,96},{192,0},{224,... | collective-permute-start | bytes 786440 | tf_op jit(solution)/shard_map/ppermute | solution.py:391
  207.4 26.5 %collective-permute-done.10.refs_2_ = bf16[128,1024]{1,0:T(8,128)(2,1)S(1)} collective-permute-done((bf16[128,1024]{1,0:T(8,128)(2,1)}, bf16[128,1024]{1,0:T(8,128)(2,1)S(1)}, u32[]{:S(2)}, u32[]{:S(2)}) %collective-permute-start.10) | collective-permute-done | bytes 262176 | tf_op jit(solution)/shard_map/ppermute | solution.py:391
  234.0 5.9 %collective-permute-start.9 = (bf16[128,1024]{1,0:T(8,128)(2,1)}, bf16[128,1024]{1,0:T(8,128)(2,1)S(1)}, u32[]{:S(2)}, u32[]{:S(2)}) collective-permute-start(bf16[128,1024]{1,0:T(8,128)(2,1)} %get-tuple-element.31), channel_id=1, source_target_pairs={{0,32},{32,0},{64,96},{96,64},{128,160},{160,128},{192,224},{224,1... | collective-permute-start | bytes 786440 | tf_op jit(solution)/shard_map/ppermute | solution.py:391
  239.9 9.2 %slopes.1 = (bf16[256,4096]{1,0:T(8,128)(2,1)}, bf16[256,4096]{1,0:T(8,128)(2,1)}, bf16[256,4096]{1,0:T(8,128)(2,1)}) custom-call(bf16[256,4096]{1,0:T(8,128)(2,1)} %bitcast.18, bf16[256,4096]{1,0:T(8,128)(2,1)} %bitcast.20), custom_call_target="tpu_custom_call" | custom-call | flops 104857600 | bytes 16777216 | tf_op jit(solution)/shard_map/slopes/pallas_call | solution.py:109
  249.2 4.5 %collective-permute-done.15.refs_7_ = bf16[128,1024]{1,0:T(8,128)(2,1)S(1)} collective-permute-done((bf16[128,1024]{1,0:T(8,128)(2,1)}, bf16[128,1024]{1,0:T(8,128)(2,1)S(1)}, u32[]{:S(2)}, u32[]{:S(2)}) %collective-permute-start.15) | collective-permute-done | bytes 262176 | tf_op jit(solution)/shard_map/ppermute | solution.py:391
  254.5 3.5 %add.11 = bf16[128,1024]{1,0:T(8,128)(2,1)} custom-call(bf16[128,1024]{1,0:T(8,128)(2,1)} %get-tuple-element.30.refs_0_, bf16[128,1024]{1,0:T(8,128)(2,1)} %copy-done.6, bf16[128,1024]{1,0:T(8,128)(2,1)} %copy-done, bf16[128,1024]{1,0:T(8,128)(2,1)} %copy-done.1, bf16[128,1024]{1,0:T(8,128)(2,1)} %copy-done.2, bf16[128,1024]{1,0:T(8,128)(2,1)} %copy-done.3, ...), custom_call_target="tpu_custom_call" | custom-call | flops 1179648 | bytes 2359296 | tf_op jit(solution)/shard_map/add/pallas_call | solution.py:287
  258.0 2.5 collective-permute-start.16
  261.7 20.3 %collective-permute-done.16 = bf16[128,1024]{1,0:T(8,128)(2,1)S(1)} collective-permute-done((bf16[128,1024]{1,0:T(8,128)(2,1)}, bf16[128,1024]{1,0:T(8,128)(2,1)S(1)}, u32[]{:S(2)}, u32[]{:S(2)}) %collective-permute-start.16) | collective-permute-done | bytes 262176 | tf_op jit(solution)/shard_map/ppermute | solution.py:406
  282.9 10.3 %epilogue.1 = (bf16[256,4096]{1,0:T(8,128)(2,1)}, bf16[256,4096]{1,0:T(8,128)(2,1)}) custom-call(bf16[32,2,256,128]{3,2,1,0:T(8,128)(2,1)} %all-to-all-done.1.recv_ref, bf16[256,4096]{1,0:T(8,128)(2,1)} %bitcast.16, bf16[256,4096]{1,0:T(8,128)(2,1)} %get-tuple-element.24.up_slope_ref, bf16[256,4096]{1,0:T(8,128)(2,1)} %get-tuple-element.25.val_slope_ref, ...), custom_call_target="tpu_custom_call" | custom-call | flops 20971520 | bytes 23068672 | tf_op jit(solution)/shard_map/epilogue/pallas_call | solution.py:333
  (57 shorter events, 4.0 us)
Async XLA Ops:
  10.1 8.1 %copy-start.8 = (bf16[1,128,1024]{2,1,0:T(8,128)(2,1)S(1)}, bf16[1,128,1024]{2,1,0:T(8,128)(2,1)}, u32[]{:S(2)}) copy-start(bf16[1,128,1024]{2,1,0:T(8,128)(2,1)} %param.9) | copy-start | bytes 786436
  10.1 31.0 %copy-start.17 = (f32[1,1024]{1,0:T(1,128)S(1)}, f32[1,1024]{1,0:T(1,128)}, u32[]{:S(2)}) copy-start(f32[1,1024]{1,0:T(1,128)} %param.10) | copy-start | bytes 12292
  10.1 114.5 %all-to-all-start = ((bf16[32,2,256,128]{3,2,1,0:T(8,128)(2,1)}), bf16[32,2,256,128]{3,2,1,0:T(8,128)(2,1)}, u32[]{:S(2)}, u32[]{:S(2)}) async-start(bf16[32,2,256,128]{3,2,1,0:T(8,128)(2,1)} %get-tuple-element.22), calls=%async_computation | async-start | bytes 8388608 | tf_op jit(solution)/shard_map/all_to_all | solution.py:388
  18.3 19.5 %collective-permute-start = (bf16[128,1024]{1,0:T(8,128)(2,1)S(1)}, bf16[128,1024]{1,0:T(8,128)(2,1)S(1)}, u32[]{:S(2)}, u32[]{:S(2)}) collective-permute-start(bf16[128,1024]{1,0:T(8,128)(2,1)S(1)} %bitcast.28), channel_id=1, source_target_pairs={{0,0},{1,32},{2,64},{3,96},{4,128},{5,160},{6,192},{7,224},{32,33}... | collective-permute-start | bytes 786440 | tf_op jit(solution)/shard_map/ppermute | solution.py:393
  37.8 87.9 %copy-start.9 = (bf16[128,1024]{1,0:T(8,128)(2,1)}, bf16[128,1024]{1,0:T(8,128)(2,1)S(1)}, u32[]{:S(2)}) copy-start(bf16[128,1024]{1,0:T(8,128)(2,1)S(1)} %collective-permute-done.refs_1_) | copy-start | bytes 786436
  37.8 45.4 %collective-permute-start.1 = (bf16[128,1024]{1,0:T(8,128)(2,1)S(1)}, bf16[128,1024]{1,0:T(8,128)(2,1)S(1)}, u32[]{:S(2)}, u32[]{:S(2)}) collective-permute-start(bf16[128,1024]{1,0:T(8,128)(2,1)S(1)} %collective-permute-done.refs_1_), channel_id=1, source_target_pairs={{0,32},{32,0},{64,96},{96,64},{128,160},{160,128},{192,224},{224,1... | collective-permute-start | bytes 786440 | tf_op jit(solution)/shard_map/ppermute | solution.py:391
  39.5 52.1 %collective-permute-start.2 = (bf16[128,1024]{1,0:T(8,128)(2,1)S(1)}, bf16[128,1024]{1,0:T(8,128)(2,1)S(1)}, u32[]{:S(2)}, u32[]{:S(2)}) collective-permute-start(bf16[128,1024]{1,0:T(8,128)(2,1)S(1)} %collective-permute-done.refs_1_), channel_id=1, source_target_pairs={{0,64},{32,96},{64,0},{96,32},{128,192},{160,224},{192,128},{224,1... | collective-permute-start | bytes 786440 | tf_op jit(solution)/shard_map/ppermute | solution.py:391
  41.1 39.2 %collective-permute-start.8 = (f32[1,1024]{1,0:T(1,128)S(1)}, f32[1,1024]{1,0:T(1,128)S(1)}, u32[]{:S(2)}, u32[]{:S(2)}) collective-permute-start(f32[1,1024]{1,0:T(1,128)S(1)} %copy-done.17), channel_id=1, source_target_pairs={{0,0},{1,32},{2,64},{3,96},{4,128},{5,160},{6,192},{7,224},{32,33}... | collective-permute-start | bytes 12296 | tf_op jit(solution)/shard_map/ppermute | solution.py:397
  79.6 27.1 %collective-permute-start.3 = (bf16[128,1024]{1,0:T(8,128)(2,1)S(1)}, bf16[128,1024]{1,0:T(8,128)(2,1)S(1)}, u32[]{:S(2)}, u32[]{:S(2)}) collective-permute-start(bf16[128,1024]{1,0:T(8,128)(2,1)S(1)} %collective-permute-done.refs_1_), channel_id=1, source_target_pairs={{0,96},{32,64},{64,32},{96,0},{128,224},{160,192},{192,160},{224,1... | collective-permute-start | bytes 786440 | tf_op jit(solution)/shard_map/ppermute | solution.py:391
  79.7 30.3 %collective-permute-start.4 = (bf16[128,1024]{1,0:T(8,128)(2,1)S(1)}, bf16[128,1024]{1,0:T(8,128)(2,1)S(1)}, u32[]{:S(2)}, u32[]{:S(2)}) collective-permute-start(bf16[128,1024]{1,0:T(8,128)(2,1)S(1)} %collective-permute-done.refs_1_), channel_id=1, source_target_pairs={{0,128},{32,160},{64,192},{96,224},{128,0},{160,32},{192,64},{224,... | collective-permute-start | bytes 786440 | tf_op jit(solution)/shard_map/ppermute | solution.py:391
  80.3 37.3 %collective-permute-start.5 = (bf16[128,1024]{1,0:T(8,128)(2,1)S(1)}, bf16[128,1024]{1,0:T(8,128)(2,1)S(1)}, u32[]{:S(2)}, u32[]{:S(2)}) collective-permute-start(bf16[128,1024]{1,0:T(8,128)(2,1)S(1)} %collective-permute-done.refs_1_), channel_id=1, source_target_pairs={{0,160},{32,128},{64,224},{96,192},{128,32},{160,0},{192,96},{224,... | collective-permute-start | bytes 786440 | tf_op jit(solution)/shard_map/ppermute | solution.py:391
  83.3 42.4 %copy-start.10 = (bf16[128,1024]{1,0:T(8,128)(2,1)}, bf16[128,1024]{1,0:T(8,128)(2,1)S(1)}, u32[]{:S(2)}) copy-start(bf16[128,1024]{1,0:T(8,128)(2,1)S(1)} %collective-permute-done.1.refs_2_) | copy-start | bytes 786436
  83.3 34.3 %collective-permute-start.6 = (bf16[128,1024]{1,0:T(8,128)(2,1)S(1)}, bf16[128,1024]{1,0:T(8,128)(2,1)S(1)}, u32[]{:S(2)}, u32[]{:S(2)}) collective-permute-start(bf16[128,1024]{1,0:T(8,128)(2,1)S(1)} %collective-permute-done.refs_1_), channel_id=1, source_target_pairs={{0,192},{32,224},{64,128},{96,160},{128,64},{160,96},{192,0},{224,... | collective-permute-start | bytes 786440 | tf_op jit(solution)/shard_map/ppermute | solution.py:391
  91.6 34.1 %copy-start.11 = (bf16[128,1024]{1,0:T(8,128)(2,1)}, bf16[128,1024]{1,0:T(8,128)(2,1)S(1)}, u32[]{:S(2)}) copy-start(bf16[128,1024]{1,0:T(8,128)(2,1)S(1)} %collective-permute-done.2.refs_3_) | copy-start | bytes 786436
  91.6 33.1 %collective-permute-start.7 = (bf16[128,1024]{1,0:T(8,128)(2,1)S(1)}, bf16[128,1024]{1,0:T(8,128)(2,1)S(1)}, u32[]{:S(2)}, u32[]{:S(2)}) collective-permute-start(bf16[128,1024]{1,0:T(8,128)(2,1)S(1)} %collective-permute-done.refs_1_), channel_id=1, source_target_pairs={{0,224},{32,192},{64,160},{96,128},{128,96},{160,64},{192,32},{224... | collective-permute-start | bytes 786440 | tf_op jit(solution)/shard_map/ppermute | solution.py:391
  106.6 19.0 %copy-start.12 = (bf16[128,1024]{1,0:T(8,128)(2,1)}, bf16[128,1024]{1,0:T(8,128)(2,1)S(1)}, u32[]{:S(2)}) copy-start(bf16[128,1024]{1,0:T(8,128)(2,1)S(1)} %collective-permute-done.3.refs_4_) | copy-start | bytes 786436
  110.0 15.7 %copy-start.13 = (bf16[128,1024]{1,0:T(8,128)(2,1)}, bf16[128,1024]{1,0:T(8,128)(2,1)S(1)}, u32[]{:S(2)}) copy-start(bf16[128,1024]{1,0:T(8,128)(2,1)S(1)} %collective-permute-done.4.refs_5_) | copy-start | bytes 786436
  117.6 8.1 %copy-start.14 = (bf16[128,1024]{1,0:T(8,128)(2,1)}, bf16[128,1024]{1,0:T(8,128)(2,1)S(1)}, u32[]{:S(2)}) copy-start(bf16[128,1024]{1,0:T(8,128)(2,1)S(1)} %collective-permute-done.5.refs_6_) | copy-start | bytes 786436
  117.6 8.1 %copy-start.15 = (bf16[128,1024]{1,0:T(8,128)(2,1)}, bf16[128,1024]{1,0:T(8,128)(2,1)S(1)}, u32[]{:S(2)}) copy-start(bf16[128,1024]{1,0:T(8,128)(2,1)S(1)} %collective-permute-done.6.refs_7_) | copy-start | bytes 786436
  184.3 98.5 %all-to-all-start.1 = ((bf16[32,2,256,128]{3,2,1,0:T(8,128)(2,1)}), bf16[32,2,256,128]{3,2,1,0:T(8,128)(2,1)}, u32[]{:S(2)}, u32[]{:S(2)}) async-start(bf16[32,2,256,128]{3,2,1,0:T(8,128)(2,1)} %bitcast.21), calls=%async_computation.1 | async-start | bytes 8388608 | tf_op jit(solution)/shard_map/all_to_all | solution.py:388
  197.1 36.9 %collective-permute-start.10 = (bf16[128,1024]{1,0:T(8,128)(2,1)}, bf16[128,1024]{1,0:T(8,128)(2,1)S(1)}, u32[]{:S(2)}, u32[]{:S(2)}) collective-permute-start(bf16[128,1024]{1,0:T(8,128)(2,1)} %get-tuple-element.32), channel_id=1, source_target_pairs={{0,64},{32,96},{64,0},{96,32},{128,192},{160,224},{192,128},{224,1... | collective-permute-start | bytes 786440 | tf_op jit(solution)/shard_map/ppermute | solution.py:391
  198.3 35.6 %collective-permute-start.11 = (bf16[128,1024]{1,0:T(8,128)(2,1)}, bf16[128,1024]{1,0:T(8,128)(2,1)S(1)}, u32[]{:S(2)}, u32[]{:S(2)}) collective-permute-start(bf16[128,1024]{1,0:T(8,128)(2,1)} %get-tuple-element.33), channel_id=1, source_target_pairs={{0,96},{32,64},{64,32},{96,0},{128,224},{160,192},{192,160},{224,1... | collective-permute-start | bytes 786440 | tf_op jit(solution)/shard_map/ppermute | solution.py:391
  198.8 50.3 %collective-permute-start.12 = (bf16[128,1024]{1,0:T(8,128)(2,1)}, bf16[128,1024]{1,0:T(8,128)(2,1)S(1)}, u32[]{:S(2)}, u32[]{:S(2)}) collective-permute-start(bf16[128,1024]{1,0:T(8,128)(2,1)} %get-tuple-element.34), channel_id=1, source_target_pairs={{0,128},{32,160},{64,192},{96,224},{128,0},{160,32},{192,64},{224,... | collective-permute-start | bytes 786440 | tf_op jit(solution)/shard_map/ppermute | solution.py:391
  202.2 46.9 %collective-permute-start.13 = (bf16[128,1024]{1,0:T(8,128)(2,1)}, bf16[128,1024]{1,0:T(8,128)(2,1)S(1)}, u32[]{:S(2)}, u32[]{:S(2)}) collective-permute-start(bf16[128,1024]{1,0:T(8,128)(2,1)} %get-tuple-element.35), channel_id=1, source_target_pairs={{0,160},{32,128},{64,224},{96,192},{128,32},{160,0},{192,96},{224,... | collective-permute-start | bytes 786440 | tf_op jit(solution)/shard_map/ppermute | solution.py:391
  204.0 45.2 %collective-permute-start.14 = (bf16[128,1024]{1,0:T(8,128)(2,1)}, bf16[128,1024]{1,0:T(8,128)(2,1)S(1)}, u32[]{:S(2)}, u32[]{:S(2)}) collective-permute-start(bf16[128,1024]{1,0:T(8,128)(2,1)} %get-tuple-element.36), channel_id=1, source_target_pairs={{0,192},{32,224},{64,128},{96,160},{128,64},{160,96},{192,0},{224,... | collective-permute-start | bytes 786440 | tf_op jit(solution)/shard_map/ppermute | solution.py:391
  234.0 15.2 %copy-start = (bf16[128,1024]{1,0:T(8,128)(2,1)}, bf16[128,1024]{1,0:T(8,128)(2,1)S(1)}, u32[]{:S(2)}) copy-start(bf16[128,1024]{1,0:T(8,128)(2,1)S(1)} %collective-permute-done.10.refs_2_) | copy-start | bytes 786436
  234.0 19.8 %collective-permute-start.15 = (bf16[128,1024]{1,0:T(8,128)(2,1)}, bf16[128,1024]{1,0:T(8,128)(2,1)S(1)}, u32[]{:S(2)}, u32[]{:S(2)}) collective-permute-start(bf16[128,1024]{1,0:T(8,128)(2,1)} %get-tuple-element.37), channel_id=1, source_target_pairs={{0,224},{32,192},{64,160},{96,128},{128,96},{160,64},{192,32},{224... | collective-permute-start | bytes 786440 | tf_op jit(solution)/shard_map/ppermute | solution.py:391
  234.0 15.1 %copy-start.1 = (bf16[128,1024]{1,0:T(8,128)(2,1)}, bf16[128,1024]{1,0:T(8,128)(2,1)S(1)}, u32[]{:S(2)}) copy-start(bf16[128,1024]{1,0:T(8,128)(2,1)S(1)} %collective-permute-done.11.refs_3_) | copy-start | bytes 786436
  234.0 19.8 %collective-permute-start.9 = (bf16[128,1024]{1,0:T(8,128)(2,1)}, bf16[128,1024]{1,0:T(8,128)(2,1)S(1)}, u32[]{:S(2)}, u32[]{:S(2)}) collective-permute-start(bf16[128,1024]{1,0:T(8,128)(2,1)} %get-tuple-element.31), channel_id=1, source_target_pairs={{0,32},{32,0},{64,96},{96,64},{128,160},{160,128},{192,224},{224,1... | collective-permute-start | bytes 786440 | tf_op jit(solution)/shard_map/ppermute | solution.py:391
  249.1 11.4 %copy-start.7 = (f32[4096]{0:T(1024)S(1)}, f32[4096]{0:T(1024)}, u32[]{:S(2)}) copy-start(f32[4096]{0:T(1024)} %param.11) | copy-start | bytes 49156
  249.1 4.6 %copy-start.2 = (bf16[128,1024]{1,0:T(8,128)(2,1)}, bf16[128,1024]{1,0:T(8,128)(2,1)S(1)}, u32[]{:S(2)}) copy-start(bf16[128,1024]{1,0:T(8,128)(2,1)S(1)} %collective-permute-done.12.refs_4_) | copy-start | bytes 786436
  258.0 24.0 %collective-permute-start.16 = (bf16[128,1024]{1,0:T(8,128)(2,1)}, bf16[128,1024]{1,0:T(8,128)(2,1)S(1)}, u32[]{:S(2)}, u32[]{:S(2)}) collective-permute-start(bf16[128,1024]{1,0:T(8,128)(2,1)} %add.11), channel_id=1, source_target_pairs={{0,0},{32,1},{64,2},{96,3},{128,4},{160,5},{192,6},{224,7},{33,32}... | collective-permute-start | bytes 786440 | tf_op jit(solution)/shard_map/ppermute | solution.py:406
  (5 other events, 11.7 us)

commit v4 on v3

--- a/solution.py
+++ b/solution.py
@@ -120,75 +120,84 @@
     )(up, val)
 
 
+def slab_of(z_offset):
+    z = (lax.axis_index(Z) + z_offset + 8) % 8
+    return z ^ (lax.axis_index("dp_0") * 2 + lax.axis_index("dp_1"))
+
+
+ANY = pl.BlockSpec(memory_space=pl.ANY)
+VMEM = pl.BlockSpec(memory_space=pltpu.VMEM)
+OFFSETS = (0, -1, -2, -3, 1, 2, 3, 4)
+PAD = 8
+
+
 def mix_kernel(seqs, parts, *refs):
     recv_ref, *w_refs = refs[: 1 + seqs]
     bias_ref, out_ref, sums_ref, gate_ref, value_ref, w_ref, mixed_ref, back_ref, sems = refs[1 + seqs :]
     toks = recv_ref.shape[2]
     block = parts * toks
     slab = block // seqs
-    key = order_key()
-    gate_sem, value_sem, w_sem, back_sem, mixed_sem = (sems.at[k] for k in range(5))
-    for b in range(seqs):
-        cols = slice(b * LANES, (b + 1) * LANES)
-        pieces = slice(b * parts, (b + 1) * parts)
-        pltpu.make_async_copy(recv_ref.at[pieces, 0], gate_ref.at[:, :, cols], gate_sem).start()
+    pair = 2 * LANES
+    steps = seqs // 2
+
+    def columns(j):
+        return slice(j * pair, (j + 1) * pair)
+
+    def fetch(which, to_ref, j):
+        for b in (2 * j, 2 * j + 1):
+            pltpu.make_async_copy(
+                recv_ref.at[b * parts : (b + 1) * parts, which],
+                to_ref.at[:, :, b * LANES : (b + 1) * LANES],
+                sems.at[which, j],
+            ).start()
+
+    def fetched(which, to_ref, j):
+        part = to_ref.at[:, :, columns(j)]
+        pltpu.make_async_copy(part, part, sems.at[which, j]).wait()
+
+    def put(which, from_ref, j):
+        for b in (2 * j, 2 * j + 1):
+            pltpu.make_async_copy(
+                from_ref.at[:, :, b * LANES : (b + 1) * LANES],
+                out_ref.at[b, :, which],
+                sems.at[2 + which, j],
+            ).start()
+
     for d in range(seqs):
-        rows = pl.ds(pl.multiple_of((d ^ key) * slab, slab), slab)
-        pltpu.make_async_copy(w_refs[d], w_ref.at[rows], w_sem).start()
-    for b in range(seqs):
-        cols = slice(b * LANES, (b + 1) * LANES)
-        pieces = slice(b * parts, (b + 1) * parts)
-        pltpu.make_async_copy(recv_ref.at[pieces, 1], value_ref.at[:, :, cols], value_sem).start()
-    pltpu.make_async_copy(gate_ref, gate_ref, gate_sem).wait()
-    pltpu.make_async_copy(w_ref, w_ref, w_sem).wait()
-
-    gate = gate_ref[...].reshape(block, seqs * LANES)
-    across = (((1,), (1,)), ((), ()))
-    ones = jnp.ones((8, seqs * LANES), BF16)
-    bias_sums = lax.dot_general(ones, gate, across, preferred_element_type=F32)
-    sums_ref[:, LANES:] = bias_sums[:1]
-
-    def back_step(y, carry):
-        at = pl.ds(pl.multiple_of(y * toks, toks), toks)
-        back_ref[y] = lax.dot_general(
-            w_ref[:, at],
-            gate_ref[...].reshape(block, seqs * LANES),
-            (((0,), (0,)), ((), ())),
-            preferred_element_type=F32,
+        rows = pl.ds(pl.multiple_of(slab_of(OFFSETS[d]) * slab, slab), slab)
+        pltpu.make_async_copy(w_refs[d], w_ref.at[rows], sems.at[4, 0]).start()
+    for j in range(steps):
+        fetch(0, gate_ref, j)
+        fetch(1, value_ref, j)
+    bias_col = jnp.transpose(jnp.broadcast_to(bias_ref[...], (8, block)))[:, :1]
+    pltpu.make_async_copy(w_ref, w_ref, sems.at[4, 0]).wait()
+    sums = jnp.zeros((8, block), F32)
+    total = jnp.zeros((8, LANES), F32)
+    for j in range(steps):
+        fetched(0, gate_ref, j)
+        gate = gate_ref[:, :, columns(j)].reshape(block, pair)
+        back = lax.dot_general(
+            w_ref[...], gate, (((0,), (0,)), ((), ())), preferred_element_type=F32
         ).astype(BF16)
-        for b in range(seqs):
-            cols = slice(b * LANES, (b + 1) * LANES)
-            pltpu.make_async_copy(back_ref.at[y, :, cols], out_ref.at[b, y, 1], back_sem).start()
-        return carry
-
-    lax.fori_loop(0, parts, back_step, 0)
-    pltpu.make_async_copy(value_ref, value_ref, value_sem).wait()
-
-    def mixed_step(y, total):
-        at = pl.ds(pl.multiple_of(y * toks, toks), toks)
-        mixed = jnp.dot(
-            w_ref[at], value_ref[...].reshape(block, seqs * LANES), preferred_element_type=F32
+        back_ref[:, :, columns(j)] = back.reshape(parts, toks, pair)
+        put(1, back_ref, j)
+        sums += lax.dot_general(
+            jnp.ones((8, pair), BF16), gate, (((1,), (1,)), ((), ())), preferred_element_type=F32
         )
-        mixed_ref[y] = (mixed + bias_ref[at, :1]).astype(BF16)
-        for b in range(seqs):
-            cols = slice(b * LANES, (b + 1) * LANES)
-            pltpu.make_async_copy(mixed_ref.at[y, :, cols], out_ref.at[b, y, 0], mixed_sem).start()
-            terms = back_ref[y, :, cols].astype(F32) * value_ref[y, :, cols].astype(F32)
-            total += jnp.sum(terms.reshape(toks // 8, 8, LANES), axis=0)
-        return total
-
-    total = lax.fori_loop(0, parts, mixed_step, jnp.zeros((8, LANES), F32))
+        fetched(1, value_ref, j)
+        value = value_ref[:, :, columns(j)].reshape(block, pair)
+        mixed = jnp.dot(w_ref[...], value, preferred_element_type=F32)
+        mixed_ref[:, :, columns(j)] = (mixed + bias_col).astype(BF16).reshape(parts, toks, pair)
+        put(0, mixed_ref, j)
+        terms = back.astype(F32) * value.astype(F32)
+        terms = jnp.sum(terms.reshape(block // 8, 8, pair), axis=0)
+        total += terms[:, :LANES] + terms[:, LANES:]
+    sums_ref[:, LANES:] = sums[:1]
     sums_ref[:, :LANES] = jnp.sum(total, axis=0, keepdims=True)
-    pltpu.make_async_copy(back_ref, back_ref, back_sem).wait()
-    pltpu.make_async_copy(mixed_ref, mixed_ref, mixed_sem).wait()
-
-
-def order_key():
-    return lax.axis_index(Z) ^ (lax.axis_index("dp_0") * 2 + lax.axis_index("dp_1"))
-
-
-ANY = pl.BlockSpec(memory_space=pl.ANY)
-VMEM = pl.BlockSpec(memory_space=pltpu.VMEM)
+    for which, from_ref in ((1, back_ref), (0, mixed_ref)):
+        for j in range(steps):
+            part = from_ref.at[:, :, columns(j)]
+            pltpu.make_async_copy(part, part, sems.at[2 + which, j]).wait()
 
 
 def mix(recv, pieces, bias, seqs, parts):
@@ -209,7 +218,7 @@
             pltpu.VMEM((block, block), BF16),
             flat,
             flat,
-            pltpu.SemaphoreType.DMA((5,)),
+            pltpu.SemaphoreType.DMA((5, seqs // 2)),
         ],
         compiler_params=pltpu.CompilerParams(vmem_limit_bytes=60 * 1024 * 1024),
         cost_estimate=pl.CostEstimate(
@@ -220,20 +229,44 @@
     return out.reshape(recv.shape), sums
 
 
-def grads_kernel(seqs, parts, recv_ref, *refs):
+def split(x):
+    high = x.astype(BF16)
+    middle = (x - high.astype(F32)).astype(BF16)
+    low = (x - high.astype(F32) - middle.astype(F32)).astype(BF16)
+    return high, middle, low
+
+
+def pack_sums(sums):
+    bias = split(sums[:, LANES:])
+    wide = jnp.concatenate([sums[:, :LANES], jnp.zeros_like(sums[:, 2 * LANES :])], axis=1)
+    gain = split(wide)
+    zeros = jnp.zeros_like(bias[0])
+    return jnp.concatenate([*bias, *gain, zeros, zeros], axis=0)
+
+
+def unpack_sums(rows):
+    rows = rows.astype(F32)
+    bias = rows[0:1] + rows[1:2] + rows[2:3]
+    gain = rows[3:4] + rows[4:5] + rows[5:6]
+    return jnp.concatenate([gain[:, :LANES], bias], axis=1)
+
+
+def grads_kernel(seqs, parts, recv_ref, sums_ref, *refs):
     outs = refs[:seqs]
-    gate_ref, value_ref, grad_ref, sems = refs[seqs:]
+    gate_ref, value_ref, grad_ref, rows_ref, sems = refs[seqs:]
     toks = recv_ref.shape[2]
     block = parts * toks
     slab = block // seqs
-    key = order_key()
     for b in range(seqs):
         cols = slice(b * LANES, (b + 1) * LANES)
         pieces = slice(b * parts, (b + 1) * parts)
-        pltpu.make_async_copy(recv_ref.at[pieces, 0], gate_ref.at[:, :, cols], sems.at[0]).start()
-        pltpu.make_async_copy(recv_ref.at[pieces, 1], value_ref.at[:, :, cols], sems.at[1]).start()
-    pltpu.make_async_copy(gate_ref, gate_ref, sems.at[0]).wait()
-    pltpu.make_async_copy(value_ref, value_ref, sems.at[1]).wait()
+        pltpu.make_async_copy(recv_ref.at[pieces, 0], gate_ref.at[:, :, cols], sems.at[0, 0]).start()
+        pltpu.make_async_copy(recv_ref.at[pieces, 1], value_ref.at[:, :, cols], sems.at[1, 0]).start()
+    rows_ref[...] = pack_sums(sums_ref[...])
+    for d in range(seqs):
+        pltpu.make_async_copy(rows_ref, outs[d].at[slab:], sems.at[3, d]).start()
+    pltpu.make_async_copy(gate_ref, gate_ref, sems.at[0, 0]).wait()
+    pltpu.make_async_copy(value_ref, value_ref, sems.at[1, 0]).wait()
 
     def step(y, carry):
         grad = lax.dot_general(
@@ -245,56 +278,102 @@
         grad_ref[y] = grad.astype(BF16)
         at = pl.ds(pl.multiple_of(y * toks, toks), toks)
         for d in range(seqs):
-            rows = pl.ds(pl.multiple_of((d ^ key) * slab, slab), slab)
-            pltpu.make_async_copy(grad_ref.at[y, rows], outs[d].at[:, at], sems.at[2]).start()
+            rows = pl.ds(pl.multiple_of(slab_of(-OFFSETS[d]) * slab, slab), slab)
+            pltpu.make_async_copy(grad_ref.at[y, rows], outs[d].at[:slab, at], sems.at[2, 0]).start()
         return carry
 
     lax.fori_loop(0, parts, step, 0)
-    pltpu.make_async_copy(grad_ref, grad_ref, sems.at[2]).wait()
-
-
-def weight_grads(recv, seqs, parts):
+    pltpu.make_async_copy(grad_ref, grad_ref, sems.at[2, 0]).wait()
+    for d in range(seqs):
+        pltpu.make_async_copy(rows_ref, outs[d].at[slab:], sems.at[3, d]).wait()
+
+
+def weight_grads(recv, sums, seqs, parts):
     toks = recv.shape[2]
     block = parts * toks
     flat = pltpu.VMEM((parts, toks, seqs * LANES), BF16)
     return pl.pallas_call(
         functools.partial(grads_kernel, seqs, parts),
-        in_specs=[ANY],
+        in_specs=[ANY, VMEM],
         out_specs=[ANY] * seqs,
-        out_shape=[jax.ShapeDtypeStruct((block // seqs, block), BF16)] * seqs,
+        out_shape=[jax.ShapeDtypeStruct((block // seqs + PAD, block), BF16)] * seqs,
         scratch_shapes=[
             flat,
             flat,
             pltpu.VMEM((parts, block, toks), BF16),
-            pltpu.SemaphoreType.DMA((3,)),
+            pltpu.VMEM((PAD, block), BF16),
+            pltpu.SemaphoreType.DMA((4, seqs)),
         ],
         compiler_params=pltpu.CompilerParams(vmem_limit_bytes=60 * 1024 * 1024),
         cost_estimate=pl.CostEstimate(
             flops=2 * block * block * seqs * LANES, bytes_accessed=6 * block * block, transcendentals=0
         ),
         name="weight_grads",
-    )(recv)
-
-
-def add_kernel(*refs):
-    *ins, out_ref = refs
-    out_ref[...] = sum(r[...].astype(F32) for r in ins).astype(BF16)
-
-
-def add(pieces, rows=32):
+    )(recv, sums)
+
+
+def hop_kernel(slab, *refs):
+    n = len(refs) // 3
+    for here, there, out in zip(refs[:n], refs[n : 2 * n], refs[2 * n :]):
+        out[:slab] = (here[:slab].astype(F32) + there[:slab].astype(F32)).astype(BF16)
+        out[slab:] = pack_sums(unpack_sums(here[slab:]) + unpack_sums(there[slab:]))
+
+
+def hop(here, there):
+    height, width = here[0].shape
+    return pl.pallas_call(
+        functools.partial(hop_kernel, height - PAD),
+        in_specs=[VMEM] * (2 * len(here)),
+        out_specs=[VMEM] * len(here),
+        out_shape=[jax.ShapeDtypeStruct((height, width), BF16)] * len(here),
+        compiler_params=pltpu.CompilerParams(vmem_limit_bytes=8 * 1024 * 1024),
+        cost_estimate=pl.CostEstimate(
+            flops=2 * height * width, bytes_accessed=12 * height * width, transcendentals=0
+        ),
+        name="hop",
+    )(*here, *there)
+
+
+def last_kernel(slab, *refs):
+    *ins, grad_ref = refs
+    grad_ref[...] = sum(r[:slab].astype(F32) for r in ins).astype(BF16)
+
+
+def last(pieces):
     height, width = pieces[0].shape
-    row = pl.BlockSpec((rows, width), lambda i: (i, 0))
-    return pl.pallas_call(
-        add_kernel,
-        grid=(height // rows,),
-        in_specs=[row] * len(pieces),
-        out_specs=row,
-        out_shape=jax.ShapeDtypeStruct((height, width), BF16),
-        compiler_params=params(60),
-        cost_estimate=pl.CostEstimate(
-            flops=9 * height * width, bytes_accessed=18 * height * width, transcendentals=0
-        ),
-        name="add",
+    return pl.pallas_call(
+        functools.partial(last_kernel, height - PAD),
+        in_specs=[VMEM] * 3,
+        out_specs=VMEM,
+        out_shape=jax.ShapeDtypeStruct((height - PAD, width), BF16),
+        compiler_params=pltpu.CompilerParams(vmem_limit_bytes=8 * 1024 * 1024),
+        cost_estimate=pl.CostEstimate(
+            flops=4 * height * width, bytes_accessed=8 * height * width, transcendentals=0
+        ),
+        name="last",
+    )(*pieces)
+
+
+def pack_kernel(slab, seqs, parts, *refs):
+    *ins, small_ref = refs
+    sums = sum(unpack_sums(r[slab:]) for r in ins)
+    small_ref[...] = jnp.zeros_like(small_ref)
+    for a in range(seqs):
+        at = slice((a + 1) * LANES, (a + 2) * LANES)
+        for y in range(parts):
+            small_ref[a * parts + y, :1] = sums[:, :LANES]
+            small_ref[a * parts + y, 1:2] = sums[:, at]
+
+
+def pack(pieces, seqs, parts):
+    slab = pieces[0].shape[0] - PAD
+    return pl.pallas_call(
+        functools.partial(pack_kernel, slab, seqs, parts),
+        in_specs=[VMEM] * 3,
+        out_specs=VMEM,
+        out_shape=jax.ShapeDtypeStruct((seqs * parts, 8, LANES), F32),
+        compiler_params=pltpu.CompilerParams(vmem_limit_bytes=8 * 1024 * 1024),
+        name="pack",
     )(*pieces)
 
 
@@ -352,33 +431,10 @@
     )(recv, cot, up_slope, val_slope, act, inv, gain)
 
 
-def pack_kernel(seqs, parts, sums_ref, out_ref):
-    out_ref[...] = jnp.zeros_like(out_ref)
-    for a in range(seqs):
-        at = slice((a + 1) * LANES, (a + 2) * LANES)
-        for y in range(parts):
-            out_ref[a * parts + y, :1] = sums_ref[:, :LANES]
-            out_ref[a * parts + y, 1:2] = sums_ref[:, at]
-
-
-def pack(sums, seqs, parts):
-    shape = (seqs * parts, 8, LANES)
-    return pl.pallas_call(
-        functools.partial(pack_kernel, seqs, parts),
-        grid=(1,),
-        in_specs=[pl.BlockSpec(sums.shape, lambda i: (0, 0))],
-        out_specs=pl.BlockSpec(shape, lambda i: (0, 0, 0)),
-        out_shape=jax.ShapeDtypeStruct(shape, F32),
-        compiler_params=params(60),
-        name="pack",
-    )(sums)
-
-
 def shards(cotangent, up_pre, value_pre, spatial_weight, spatial_bias, value_gain):
     planes = lax.axis_size(Z)
     seqs = lax.axis_size(DP)
     parts = lax.axis_size("sp_1")
-    block = spatial_weight.shape[2]
     cot, up, val = cotangent[0], up_pre[0], value_pre[0]
     gain = value_gain[None]
     away = [(z * seqs + a, (z ^ a) * seqs + z) for z in range(planes) for a in range(seqs)]
@@ -387,24 +443,33 @@
     def exchange(x):
         return lax.all_to_all(x, PLANE, split_axis=0, concat_axis=0, tiled=True)
 
-    def across(x, d):
-        return lax.ppermute(x, Z, [(z, z ^ d) for z in range(planes)])
+    def shifted(x, by):
+        return lax.ppermute(x, Z, [(z, (z + by) % planes) for z in range(planes)])
 
     weights = lax.ppermute(spatial_weight[0], Z_DP, away)
+    bias = lax.ppermute(spatial_bias, Z_DP, away)
     sent, inv = prologue(cot, up, val, gain)
     recv = exchange(sent)
-    pieces = [weights] + [across(weights, d) for d in range(1, planes)]
-    bias = lax.ppermute(spatial_bias, Z_DP, away)
-    bias = jnp.broadcast_to(bias.reshape(block, 1), (block, LANES))
+    before, after = [weights], [weights]
+    for _ in range(3):
+        before.append(shifted(before[-1], 1))
+        after.append(shifted(after[-1], -1))
+    after.append(shifted(after[-1], -1))
+    pieces = before + after[1:]
     up_slope, val_slope, act = slopes(up, val)
     back, sums = mix(recv, pieces, bias, seqs, parts)
     back = exchange(back)
-    grads = weight_grads(recv, seqs, parts)
-    grads = [grads[0]] + [across(grads[d], d) for d in range(1, planes)]
-    grads = add(grads)
-    sums = lax.psum(sums, Z)
+    own, p1, p2, p3, m1, m2, m3, m4 = weight_grads(recv, sums, seqs, parts)
+    plus, minus = shifted(p3, 1), shifted(m4, -1)
+    plus, minus = hop((p2, m3), (plus, minus))
+    plus, minus = shifted(plus, 1), shifted(minus, -1)
+    plus, minus = hop((p1, m2), (plus, minus))
+    plus, minus = shifted(plus, 1), shifted(minus, -1)
+    (minus,) = hop((m1,), (minus,))
+    minus = shifted(minus, -1)
+    grads = last((own, plus, minus))
     grads = lax.ppermute(grads, Z_DP, home)
-    small = pack(sums, seqs, parts)
+    small = pack((own, plus, minus), seqs, parts)
     small = exchange(small)
     gain_grad = small[:, 0].reshape(-1) / value_gain
     mine = lax.axis_index(Z) * parts + lax.axis_index("sp_1")

time: 294 us -> 264 us (0.90)
  the two profiles are of different devices: /device:TPU:7 before, /device:TPU:1 now
where the time goes in v4:
time: 264 us; the launch traced here: 260 us
  starting transfers between devices  98.4 us (37%)
  waiting for transfers between devices  79 us (30%)
  Pallas kernels  50.1 us (19%)
  blocking collectives  25.1 us (10%)
  local copies, waits for them, and re-layouts  5.13 us (2%)
    ppermute x14, starting transfers between devices, shifted(): return lax.ppermute(x, Z, [(z, (z + by) % planes) for z in range(planes)])  43.4 us
    all_to_all x2, waiting for transfers between devices, exchange(): return lax.all_to_all(x, PLANE, split_axis=0, concat_axis=0, tiled=True)  40.6 us
    ppermute x1, starting transfers between devices, shards(): bias = lax.ppermute(spatial_bias, Z_DP, away)  35.6 us
    ppermute x14, waiting for transfers between devices, shifted(): return lax.ppermute(x, Z, [(z, (z + by) % planes) for z in range(planes)])  29 us
    all_to_all x1, blocking collectives, exchange(): return lax.all_to_all(x, PLANE, split_axis=0, concat_axis=0, tiled=True)  25.1 us
    all_to_all x2, starting transfers between devices, exchange(): return lax.all_to_all(x, PLANE, split_axis=0, concat_axis=0, tiled=True)  13.7 us
    pallas_call x1, Pallas kernels, mix(): pl.pallas_call(functools.partial(mix_kernel, seqs, parts), in_specs=[ANY]...  13.4 us
    pallas_call x1, Pallas kernels, epilogue(): pl.pallas_call(functools.partial(epilogue_kernel, groups), grid=(toks //...  10.3 us
  transfers between devices with their start and end apart: 19, of which 11 were waited for; matrix products, arithmetic and copies ran while one was open for 1% of the time, Pallas kernels for 4%

profile of v4, /device:TPU:1, one launch (start us, length us, event | category | flops | bytes accessed | tf_op | source)
XLA Modules:
  0.0 260.0 jit_solution(5515818188333500457)
XLA Ops:
  0.6 9.5 %prologue.1 = (bf16[32,2,256,128]{3,2,1,0:T(8,128)(2,1)}, f32[256,128]{1,0:T(8,128)}) custom-call(bf16[256,4096]{1,0:T(8,128)(2,1)} %bitcast.14, bf16[256,4096]{1,0:T(8,128)(2,1)} %bitcast.16, bf16[256,4096]{1,0:T(8,128)(2,1)} %bitcast.18, f32[1,4096]{1,0:T(1,128)} %bitcast.21), custom_call_target="tpu_custom_call" | custom-call | flops 104857600 | bytes 10485760 | tf_op jit(solution)/shard_map/prologue/pallas_call | solution.py:66
  10.1 8.8 %all-to-all-start = ((bf16[32,2,256,128]{3,2,1,0:T(8,128)(2,1)}), bf16[32,2,256,128]{3,2,1,0:T(8,128)(2,1)}, u32[]{:S(2)}, u32[]{:S(2)}) async-start(bf16[32,2,256,128]{3,2,1,0:T(8,128)(2,1)} %get-tuple-element.26), calls=%async_computation | async-start | bytes 8388608 | tf_op jit(solution)/shard_map/all_to_all | solution.py:444
  18.9 3.7 %collective-permute-start = (bf16[128,1024]{1,0:T(8,128)(2,1)S(1)}, bf16[128,1024]{1,0:T(8,128)(2,1)S(1)}, u32[]{:S(2)}, u32[]{:S(2)}) collective-permute-start(bf16[128,1024]{1,0:T(8,128)(2,1)S(1)} %bitcast.26), channel_id=1, source_target_pairs={{0,0},{1,32},{2,64},{3,96},{4,128},{5,160},{6,192},{7,224},{32,33}... | collective-permute-start | bytes 786440 | tf_op jit(solution)/shard_map/ppermute | solution.py:449
  22.7 4.0 %collective-permute-done.refs_1_ = bf16[128,1024]{1,0:T(8,128)(2,1)S(1)} collective-permute-done((bf16[128,1024]{1,0:T(8,128)(2,1)S(1)}, bf16[128,1024]{1,0:T(8,128)(2,1)S(1)}, u32[]{:S(2)}, u32[]{:S(2)}) %collective-permute-start) | collective-permute-done | bytes 262176 | tf_op jit(solution)/shard_map/ppermute | solution.py:449
  26.6 13.4 %collective-permute-start.4 = (bf16[128,1024]{1,0:T(8,128)(2,1)S(1)}, bf16[128,1024]{1,0:T(8,128)(2,1)S(1)}, u32[]{:S(2)}, u32[]{:S(2)}) collective-permute-start(bf16[128,1024]{1,0:T(8,128)(2,1)S(1)} %collective-permute-done.refs_1_), channel_id=1, source_target_pairs={{0,224},{32,0},{64,32},{96,64},{128,96},{160,128},{192,160},{224,1... | collective-permute-start | bytes 786440 | tf_op jit(solution)/shard_map/ppermute | solution.py:447
  40.1 3.3 %collective-permute-done.4.refs_5_ = bf16[128,1024]{1,0:T(8,128)(2,1)S(1)} collective-permute-done((bf16[128,1024]{1,0:T(8,128)(2,1)S(1)}, bf16[128,1024]{1,0:T(8,128)(2,1)S(1)}, u32[]{:S(2)}, u32[]{:S(2)}) %collective-permute-start.4) | collective-permute-done | bytes 262176 | tf_op jit(solution)/shard_map/ppermute | solution.py:447
  43.4 3.5 %collective-permute-start.5 = (bf16[128,1024]{1,0:T(8,128)(2,1)S(1)}, bf16[128,1024]{1,0:T(8,128)(2,1)S(1)}, u32[]{:S(2)}, u32[]{:S(2)}) collective-permute-start(bf16[128,1024]{1,0:T(8,128)(2,1)S(1)} %collective-permute-done.4.refs_5_), channel_id=1, source_target_pairs={{0,224},{32,0},{64,32},{96,64},{128,96},{160,128},{192,160},{224,1... | collective-permute-start | bytes 786440 | tf_op jit(solution)/shard_map/ppermute | solution.py:447
  46.9 3.3 %collective-permute-done.5.refs_6_ = bf16[128,1024]{1,0:T(8,128)(2,1)S(1)} collective-permute-done((bf16[128,1024]{1,0:T(8,128)(2,1)S(1)}, bf16[128,1024]{1,0:T(8,128)(2,1)S(1)}, u32[]{:S(2)}, u32[]{:S(2)}) %collective-permute-start.5) | collective-permute-done | bytes 262176 | tf_op jit(solution)/shard_map/ppermute | solution.py:447
  50.2 3.5 %collective-permute-start.6 = (bf16[128,1024]{1,0:T(8,128)(2,1)S(1)}, bf16[128,1024]{1,0:T(8,128)(2,1)S(1)}, u32[]{:S(2)}, u32[]{:S(2)}) collective-permute-start(bf16[128,1024]{1,0:T(8,128)(2,1)S(1)} %collective-permute-done.5.refs_6_), channel_id=1, source_target_pairs={{0,224},{32,0},{64,32},{96,64},{128,96},{160,128},{192,160},{224,1... | collective-permute-start | bytes 786440 | tf_op jit(solution)/shard_map/ppermute | solution.py:447
  53.7 3.3 %collective-permute-done.6.refs_7_ = bf16[128,1024]{1,0:T(8,128)(2,1)S(1)} collective-permute-done((bf16[128,1024]{1,0:T(8,128)(2,1)S(1)}, bf16[128,1024]{1,0:T(8,128)(2,1)S(1)}, u32[]{:S(2)}, u32[]{:S(2)}) %collective-permute-start.6) | collective-permute-done | bytes 262176 | tf_op jit(solution)/shard_map/ppermute | solution.py:447
  57.0 3.5 %collective-permute-start.7 = (bf16[128,1024]{1,0:T(8,128)(2,1)S(1)}, bf16[128,1024]{1,0:T(8,128)(2,1)S(1)}, u32[]{:S(2)}, u32[]{:S(2)}) collective-permute-start(bf16[128,1024]{1,0:T(8,128)(2,1)S(1)} %collective-permute-done.6.refs_7_), channel_id=1, source_target_pairs={{0,224},{32,0},{64,32},{96,64},{128,96},{160,128},{192,160},{224,1... | collective-permute-start | bytes 786440 | tf_op jit(solution)/shard_map/ppermute | solution.py:447
  60.6 35.6 %collective-permute-start.8 = (f32[1,1024]{1,0:T(1,128)S(1)}, f32[1,1024]{1,0:T(1,128)S(1)}, u32[]{:S(2)}, u32[]{:S(2)}) collective-permute-start(f32[1,1024]{1,0:T(1,128)S(1)} %copy-done.16), channel_id=1, source_target_pairs={{0,0},{1,32},{2,64},{3,96},{4,128},{5,160},{6,192},{7,224},{32,33}... | collective-permute-start | bytes 12296 | tf_op jit(solution)/shard_map/ppermute | solution.py:450
  97.5 13.4 %mix.1 = (bf16[8,4,2,256,128]{4,3,2,1,0:T(8,128)(2,1)}, f32[1,1152]{1,0:T(1,128)}) custom-call(bf16[32,2,256,128]{3,2,1,0:T(8,128)(2,1)} %all-to-all-done.refs_0_.recv_ref, bf16[128,1024]{1,0:T(8,128)(2,1)} %copy-done.8, bf16[128,1024]{1,0:T(8,128)(2,1)} %copy-done.10, bf16[128,1024]{1,0:T(8,128)(2,1)} %copy-done.12, bf16[128,1024]{1,0:T(8,128)(2,1)} %copy-done.14, ...), custom_call_target="tpu_custom_call" | custom-call | flops 4294967296 | bytes 10485760 | tf_op jit(solution)/shard_map/mix/pallas_call | solution.py:207
  111.0 7.0 %weight_grads.1 = (bf16[136,1024]{1,0:T(8,128)(2,1)}, bf16[136,1024]{1,0:T(8,128)(2,1)}, bf16[136,1024]{1,0:T(8,128)(2,1)}, bf16[136,1024]{1,0:T(8,128)(2,1)}, b...) custom-call(bf16[32,2,256,128]{3,2,1,0:T(8,128)(2,1)} %all-to-all-do, ...), custom_call_target="tpu_custom_call" | custom-call | flops 2147483648 | bytes 6291456 | tf_op jit(solution)/shard_map/weight_grads/pallas_call | solution.py:295
  118.1 10.9 %collective-permute-start.10 = (bf16[136,1024]{1,0:T(8,128)(2,1)}, bf16[136,1024]{1,0:T(8,128)(2,1)S(1)}, u32[]{:S(2)}, u32[]{:S(2)}) collective-permute-start(bf16[136,1024]{1,0:T(8,128)(2,1)} %get-tuple-element.41), channel_id=1, source_target_pairs={{0,224},{32,0},{64,32},{96,64},{128,96},{160,128},{192,160},{224,1... | collective-permute-start | bytes 835592 | tf_op jit(solution)/shard_map/ppermute | solution.py:447
  129.0 6.2 %collective-permute-done.9.refs_2_ = bf16[136,1024]{1,0:T(8,128)(2,1)S(1)} collective-permute-done((bf16[136,1024]{1,0:T(8,128)(2,1)}, bf16[136,1024]{1,0:T(8,128)(2,1)S(1)}, u32[]{:S(2)}, u32[]{:S(2)}) %collective-permute-start.9) | collective-permute-done | bytes 278560 | tf_op jit(solution)/shard_map/ppermute | solution.py:447
  135.2 1.0 copy-done.4
  136.1 1.0 copy-done.5
  137.4 2.7 %collective-permute-start.12 = (bf16[136,1024]{1,0:T(8,128)(2,1)S(1)}, bf16[136,1024]{1,0:T(8,128)(2,1)S(1)}, u32[]{:S(2)}, u32[]{:S(2)}) collective-permute-start(bf16[136,1024]{1,0:T(8,128)(2,1)S(1)} %get-tuple-element.43), channel_id=1, source_target_pairs={{0,224},{32,0},{64,32},{96,64},{128,96},{160,128},{192,160},{224,1... | collective-permute-start | bytes 835592 | tf_op jit(solution)/shard_map/ppermute | solution.py:447
  140.0 5.2 %collective-permute-done.11.refs_2_ = bf16[136,1024]{1,0:T(8,128)(2,1)S(1)} collective-permute-done((bf16[136,1024]{1,0:T(8,128)(2,1)S(1)}, bf16[136,1024]{1,0:T(8,128)(2,1)S(1)}, u32[]{:S(2)}, u32[]{:S(2)}) %collective-permute-start.11) | collective-permute-done | bytes 278560 | tf_op jit(solution)/shard_map/ppermute | solution.py:447
  145.2 1.0 copy-done.2
  147.4 2.5 collective-permute-start.14
  149.8 3.5 %collective-permute-done.14.refs_1_ = bf16[136,1024]{1,0:T(8,128)(2,1)S(1)} collective-permute-done((bf16[136,1024]{1,0:T(8,128)(2,1)S(1)}, bf16[136,1024]{1,0:T(8,128)(2,1)S(1)}, u32[]{:S(2)}, u32[]{:S(2)}) %collective-permute-start.14) | collective-permute-done | bytes 278560 | tf_op jit(solution)/shard_map/ppermute | solution.py:447
  153.4 3.2 %collective-permute-start.15 = (bf16[136,1024]{1,0:T(8,128)(2,1)S(1)}, bf16[136,1024]{1,0:T(8,128)(2,1)S(1)}, u32[]{:S(2)}, u32[]{:S(2)}) collective-permute-start(bf16[136,1024]{1,0:T(8,128)(2,1)S(1)} %hop.5), channel_id=1, source_target_pairs={{0,224},{32,0},{64,32},{96,64},{128,96},{160,128},{192,160},{224,1... | collective-permute-start | bytes 835592 | tf_op jit(solution)/shard_map/ppermute | solution.py:447
  156.6 4.2 %collective-permute-done.15.refs_2_ = bf16[136,1024]{1,0:T(8,128)(2,1)S(1)} collective-permute-done((bf16[136,1024]{1,0:T(8,128)(2,1)S(1)}, bf16[136,1024]{1,0:T(8,128)(2,1)S(1)}, u32[]{:S(2)}, u32[]{:S(2)}) %collective-permute-start.15) | collective-permute-done | bytes 278560 | tf_op jit(solution)/shard_map/ppermute | solution.py:447
  160.8 25.1 %all_to_all.15 = f32[32,8,128]{2,1,0:T(8,128)S(1)} all-to-all(f32[32,8,128]{2,1,0:T(8,128)S(1)} %pack.1), channel_id=1, replica_groups=mesh['sp_0'=8,'sp_1'=4,'dp_0'=4,'dp_1'=2] {'dp_0','dp_1','sp_1'}, dimensions={0} | all-to-all | bytes 262144 | tf_op jit(solution)/shard_map/all_to_all | solution.py:444
  185.9 5.0 %all-to-all-start.1 = ((bf16[32,2,256,128]{3,2,1,0:T(8,128)(2,1)}), bf16[32,2,256,128]{3,2,1,0:T(8,128)(2,1)}, u32[]{:S(2)}, u32[]{:S(2)}) async-start(bf16[32,2,256,128]{3,2,1,0:T(8,128)(2,1)} %bitcast.20), calls=%async_computation.1 | async-start | bytes 8388608 | tf_op jit(solution)/shard_map/all_to_all | solution.py:444
  190.9 9.3 %slopes.1 = (bf16[256,4096]{1,0:T(8,128)(2,1)}, bf16[256,4096]{1,0:T(8,128)(2,1)}, bf16[256,4096]{1,0:T(8,128)(2,1)}) custom-call(bf16[256,4096]{1,0:T(8,128)(2,1)} %bitcast.17, bf16[256,4096]{1,0:T(8,128)(2,1)} %bitcast.19), custom_call_target="tpu_custom_call" | custom-call | flops 104857600 | bytes 16777216 | tf_op jit(solution)/shard_map/slopes/pallas_call | solution.py:109
  200.2 1.9 collective-permute-start.16
  203.4 5.0 %collective-permute-done.16 = bf16[128,1024]{1,0:T(8,128)(2,1)S(1)} collective-permute-done((bf16[128,1024]{1,0:T(8,128)(2,1)S(1)}, bf16[128,1024]{1,0:T(8,128)(2,1)S(1)}, u32[]{:S(2)}, u32[]{:S(2)}) %collective-permute-start.16) | collective-permute-done | bytes 262176 | tf_op jit(solution)/shard_map/ppermute | solution.py:471
  209.2 40.6 %all-to-all-done.1.recv_ref = bf16[32,2,256,128]{3,2,1,0:T(8,128)(2,1)} async-done(((bf16[32,2,256,128]{3,2,1,0:T(8,128)(2,1)}), bf16[32,2,256,128]{3,2,1,0:T(8,128)(2,1)}, u32[]{:S(2)}, u32[]{:S(2)}) %all-to-all-start.1) | async-done | bytes 4194336 | tf_op jit(solution)/shard_map/all_to_all | solution.py:444
  249.7 10.3 %epilogue.1 = (bf16[256,4096]{1,0:T(8,128)(2,1)}, bf16[256,4096]{1,0:T(8,128)(2,1)}) custom-call(bf16[32,2,256,128]{3,2,1,0:T(8,128)(2,1)} %all-to-all-done.1.recv_ref, bf16[256,4096]{1,0:T(8,128)(2,1)} %bitcast.15, bf16[256,4096]{1,0:T(8,128)(2,1)} %get-tuple-element.28.up_slope_ref, bf16[256,4096]{1,0:T(8,128)(2,1)} %get-tuple-element.29.val_slope_ref, ...), custom_call_target="tpu_custom_call" | custom-call | flops 20971520 | bytes 23068672 | tf_op jit(solution)/shard_map/epilogue/pallas_call | solution.py:412
  (58 shorter events, 5.1 us)
Async XLA Ops:
  10.1 8.8 %copy-start.7 = (bf16[1,128,1024]{2,1,0:T(8,128)(2,1)S(1)}, bf16[1,128,1024]{2,1,0:T(8,128)(2,1)}, u32[]{:S(2)}) copy-start(bf16[1,128,1024]{2,1,0:T(8,128)(2,1)} %param.9) | copy-start | bytes 786436
  10.1 50.4 %copy-start.16 = (f32[1,1024]{1,0:T(1,128)S(1)}, f32[1,1024]{1,0:T(1,128)}, u32[]{:S(2)}) copy-start(f32[1,1024]{1,0:T(1,128)} %param.10) | copy-start | bytes 12292
  10.1 86.6 %all-to-all-start = ((bf16[32,2,256,128]{3,2,1,0:T(8,128)(2,1)}), bf16[32,2,256,128]{3,2,1,0:T(8,128)(2,1)}, u32[]{:S(2)}, u32[]{:S(2)}) async-start(bf16[32,2,256,128]{3,2,1,0:T(8,128)(2,1)} %get-tuple-element.26), calls=%async_computation | async-start | bytes 8388608 | tf_op jit(solution)/shard_map/all_to_all | solution.py:444
  18.9 7.7 %collective-permute-start = (bf16[128,1024]{1,0:T(8,128)(2,1)S(1)}, bf16[128,1024]{1,0:T(8,128)(2,1)S(1)}, u32[]{:S(2)}, u32[]{:S(2)}) collective-permute-start(bf16[128,1024]{1,0:T(8,128)(2,1)S(1)} %bitcast.26), channel_id=1, source_target_pairs={{0,0},{1,32},{2,64},{3,96},{4,128},{5,160},{6,192},{7,224},{32,33}... | collective-permute-start | bytes 786440 | tf_op jit(solution)/shard_map/ppermute | solution.py:449
  26.6 70.1 %copy-start.8 = (bf16[128,1024]{1,0:T(8,128)(2,1)}, bf16[128,1024]{1,0:T(8,128)(2,1)S(1)}, u32[]{:S(2)}) copy-start(bf16[128,1024]{1,0:T(8,128)(2,1)S(1)} %collective-permute-done.refs_1_) | copy-start | bytes 786436
  26.6 16.7 %collective-permute-start.4 = (bf16[128,1024]{1,0:T(8,128)(2,1)S(1)}, bf16[128,1024]{1,0:T(8,128)(2,1)S(1)}, u32[]{:S(2)}, u32[]{:S(2)}) collective-permute-start(bf16[128,1024]{1,0:T(8,128)(2,1)S(1)} %collective-permute-done.refs_1_), channel_id=1, source_target_pairs={{0,224},{32,0},{64,32},{96,64},{128,96},{160,128},{192,160},{224,1... | collective-permute-start | bytes 786440 | tf_op jit(solution)/shard_map/ppermute | solution.py:447
  40.1 6.8 %collective-permute-start.1 = (bf16[128,1024]{1,0:T(8,128)(2,1)S(1)}, bf16[128,1024]{1,0:T(8,128)(2,1)S(1)}, u32[]{:S(2)}, u32[]{:S(2)}) collective-permute-start(bf16[128,1024]{1,0:T(8,128)(2,1)S(1)} %collective-permute-done.refs_1_), channel_id=1, source_target_pairs={{0,32},{32,64},{64,96},{96,128},{128,160},{160,192},{192,224},{224... | collective-permute-start | bytes 786440 | tf_op jit(solution)/shard_map/ppermute | solution.py:447
  43.4 53.4 %copy-start.9 = (bf16[128,1024]{1,0:T(8,128)(2,1)}, bf16[128,1024]{1,0:T(8,128)(2,1)S(1)}, u32[]{:S(2)}) copy-start(bf16[128,1024]{1,0:T(8,128)(2,1)S(1)} %collective-permute-done.4.refs_5_) | copy-start | bytes 786436
  43.4 6.8 %collective-permute-start.5 = (bf16[128,1024]{1,0:T(8,128)(2,1)S(1)}, bf16[128,1024]{1,0:T(8,128)(2,1)S(1)}, u32[]{:S(2)}, u32[]{:S(2)}) collective-permute-start(bf16[128,1024]{1,0:T(8,128)(2,1)S(1)} %collective-permute-done.4.refs_5_), channel_id=1, source_target_pairs={{0,224},{32,0},{64,32},{96,64},{128,96},{160,128},{192,160},{224,1... | collective-permute-start | bytes 786440 | tf_op jit(solution)/shard_map/ppermute | solution.py:447
  46.9 49.9 %copy-start.10 = (bf16[128,1024]{1,0:T(8,128)(2,1)}, bf16[128,1024]{1,0:T(8,128)(2,1)S(1)}, u32[]{:S(2)}) copy-start(bf16[128,1024]{1,0:T(8,128)(2,1)S(1)} %collective-permute-done.1.refs_2_) | copy-start | bytes 786436
  46.9 6.8 %collective-permute-start.2 = (bf16[128,1024]{1,0:T(8,128)(2,1)S(1)}, bf16[128,1024]{1,0:T(8,128)(2,1)S(1)}, u32[]{:S(2)}, u32[]{:S(2)}) collective-permute-start(bf16[128,1024]{1,0:T(8,128)(2,1)S(1)} %collective-permute-done.1.refs_2_), channel_id=1, source_target_pairs={{0,32},{32,64},{64,96},{96,128},{128,160},{160,192},{192,224},{224... | collective-permute-start | bytes 786440 | tf_op jit(solution)/shard_map/ppermute | solution.py:447
  50.2 46.6 %copy-start.11 = (bf16[128,1024]{1,0:T(8,128)(2,1)}, bf16[128,1024]{1,0:T(8,128)(2,1)S(1)}, u32[]{:S(2)}) copy-start(bf16[128,1024]{1,0:T(8,128)(2,1)S(1)} %collective-permute-done.5.refs_6_) | copy-start | bytes 786436
  50.2 6.8 %collective-permute-start.6 = (bf16[128,1024]{1,0:T(8,128)(2,1)S(1)}, bf16[128,1024]{1,0:T(8,128)(2,1)S(1)}, u32[]{:S(2)}, u32[]{:S(2)}) collective-permute-start(bf16[128,1024]{1,0:T(8,128)(2,1)S(1)} %collective-permute-done.5.refs_6_), channel_id=1, source_target_pairs={{0,224},{32,0},{64,32},{96,64},{128,96},{160,128},{192,160},{224,1... | collective-permute-start | bytes 786440 | tf_op jit(solution)/shard_map/ppermute | solution.py:447
  53.7 43.1 %copy-start.12 = (bf16[128,1024]{1,0:T(8,128)(2,1)}, bf16[128,1024]{1,0:T(8,128)(2,1)S(1)}, u32[]{:S(2)}) copy-start(bf16[128,1024]{1,0:T(8,128)(2,1)S(1)} %collective-permute-done.2.refs_3_) | copy-start | bytes 786436
  53.7 43.0 %collective-permute-start.3 = (bf16[128,1024]{1,0:T(8,128)(2,1)S(1)}, bf16[128,1024]{1,0:T(8,128)(2,1)S(1)}, u32[]{:S(2)}, u32[]{:S(2)}) collective-permute-start(bf16[128,1024]{1,0:T(8,128)(2,1)S(1)} %collective-permute-done.2.refs_3_), channel_id=1, source_target_pairs={{0,32},{32,64},{64,96},{96,128},{128,160},{160,192},{192,224},{224... | collective-permute-start | bytes 786440 | tf_op jit(solution)/shard_map/ppermute | solution.py:447
  57.0 39.8 %copy-start.13 = (bf16[128,1024]{1,0:T(8,128)(2,1)}, bf16[128,1024]{1,0:T(8,128)(2,1)S(1)}, u32[]{:S(2)}) copy-start(bf16[128,1024]{1,0:T(8,128)(2,1)S(1)} %collective-permute-done.6.refs_7_) | copy-start | bytes 786436
  57.0 39.7 %collective-permute-start.7 = (bf16[128,1024]{1,0:T(8,128)(2,1)S(1)}, bf16[128,1024]{1,0:T(8,128)(2,1)S(1)}, u32[]{:S(2)}, u32[]{:S(2)}) collective-permute-start(bf16[128,1024]{1,0:T(8,128)(2,1)S(1)} %collective-permute-done.6.refs_7_), channel_id=1, source_target_pairs={{0,224},{32,0},{64,32},{96,64},{128,96},{160,128},{192,160},{224,1... | collective-permute-start | bytes 786440 | tf_op jit(solution)/shard_map/ppermute | solution.py:447
  60.6 36.2 %collective-permute-start.8 = (f32[1,1024]{1,0:T(1,128)S(1)}, f32[1,1024]{1,0:T(1,128)S(1)}, u32[]{:S(2)}, u32[]{:S(2)}) collective-permute-start(f32[1,1024]{1,0:T(1,128)S(1)} %copy-done.16), channel_id=1, source_target_pairs={{0,0},{1,32},{2,64},{3,96},{4,128},{5,160},{6,192},{7,224},{32,33}... | collective-permute-start | bytes 12296 | tf_op jit(solution)/shard_map/ppermute | solution.py:450
  117.9 35.4 %copy-start.1 = (bf16[136,1024]{1,0:T(8,128)(2,1)S(1)}, bf16[136,1024]{1,0:T(8,128)(2,1)}, u32[]{:S(2)}) copy-start(bf16[136,1024]{1,0:T(8,128)(2,1)} %get-tuple-element.45.refs_0_) | copy-start | bytes 835588
  118.0 42.8 %copy-start = (bf16[136,1024]{1,0:T(8,128)(2,1)S(1)}, bf16[136,1024]{1,0:T(8,128)(2,1)}, u32[]{:S(2)}) copy-start(bf16[136,1024]{1,0:T(8,128)(2,1)} %get-tuple-element.35.refs_0_) | copy-start | bytes 835588
  118.0 17.2 %collective-permute-start.9 = (bf16[136,1024]{1,0:T(8,128)(2,1)}, bf16[136,1024]{1,0:T(8,128)(2,1)S(1)}, u32[]{:S(2)}, u32[]{:S(2)}) collective-permute-start(bf16[136,1024]{1,0:T(8,128)(2,1)} %get-tuple-element.40), channel_id=1, source_target_pairs={{0,32},{32,64},{64,96},{96,128},{128,160},{160,192},{192,224},{224... | collective-permute-start | bytes 835592 | tf_op jit(solution)/shard_map/ppermute | solution.py:447
  118.1 17.1 %collective-permute-start.10 = (bf16[136,1024]{1,0:T(8,128)(2,1)}, bf16[136,1024]{1,0:T(8,128)(2,1)S(1)}, u32[]{:S(2)}, u32[]{:S(2)}) collective-permute-start(bf16[136,1024]{1,0:T(8,128)(2,1)} %get-tuple-element.41), channel_id=1, source_target_pairs={{0,224},{32,0},{64,32},{96,64},{128,96},{160,128},{192,160},{224,1... | collective-permute-start | bytes 835592 | tf_op jit(solution)/shard_map/ppermute | solution.py:447
  135.2 1.0 copy-start.4
  137.3 8.0 %collective-permute-start.11 = (bf16[136,1024]{1,0:T(8,128)(2,1)S(1)}, bf16[136,1024]{1,0:T(8,128)(2,1)S(1)}, u32[]{:S(2)}, u32[]{:S(2)}) collective-permute-start(bf16[136,1024]{1,0:T(8,128)(2,1)S(1)} %get-tuple-element.42), channel_id=1, source_target_pairs={{0,32},{32,64},{64,96},{96,128},{128,160},{160,192},{192,224},{224... | collective-permute-start | bytes 835592 | tf_op jit(solution)/shard_map/ppermute | solution.py:447
  137.4 7.9 %collective-permute-start.12 = (bf16[136,1024]{1,0:T(8,128)(2,1)S(1)}, bf16[136,1024]{1,0:T(8,128)(2,1)S(1)}, u32[]{:S(2)}, u32[]{:S(2)}) collective-permute-start(bf16[136,1024]{1,0:T(8,128)(2,1)S(1)} %get-tuple-element.43), channel_id=1, source_target_pairs={{0,224},{32,0},{64,32},{96,64},{128,96},{160,128},{192,160},{224,1... | collective-permute-start | bytes 835592 | tf_op jit(solution)/shard_map/ppermute | solution.py:447
  145.2 1.0 copy-start.2
  147.4 6.0 %collective-permute-start.14 = (bf16[136,1024]{1,0:T(8,128)(2,1)S(1)}, bf16[136,1024]{1,0:T(8,128)(2,1)S(1)}, u32[]{:S(2)}, u32[]{:S(2)}) collective-permute-start(bf16[136,1024]{1,0:T(8,128)(2,1)S(1)} %get-tuple-element.46), channel_id=1, source_target_pairs={{0,224},{32,0},{64,32},{96,64},{128,96},{160,128},{192,160},{224,1... | collective-permute-start | bytes 835592 | tf_op jit(solution)/shard_map/ppermute | solution.py:447
  149.8 6.8 %collective-permute-start.13 = (bf16[136,1024]{1,0:T(8,128)(2,1)S(1)}, bf16[136,1024]{1,0:T(8,128)(2,1)S(1)}, u32[]{:S(2)}, u32[]{:S(2)}) collective-permute-start(bf16[136,1024]{1,0:T(8,128)(2,1)S(1)} %get-tuple-element.44), channel_id=1, source_target_pairs={{0,32},{32,64},{64,96},{96,128},{128,160},{160,192},{192,224},{224... | collective-permute-start | bytes 835592 | tf_op jit(solution)/shard_map/ppermute | solution.py:447
  153.4 7.4 %collective-permute-start.15 = (bf16[136,1024]{1,0:T(8,128)(2,1)S(1)}, bf16[136,1024]{1,0:T(8,128)(2,1)S(1)}, u32[]{:S(2)}, u32[]{:S(2)}) collective-permute-start(bf16[136,1024]{1,0:T(8,128)(2,1)S(1)} %hop.5), channel_id=1, source_target_pairs={{0,224},{32,0},{64,32},{96,64},{128,96},{160,128},{192,160},{224,1... | collective-permute-start | bytes 835592 | tf_op jit(solution)/shard_map/ppermute | solution.py:447
  185.9 63.8 %all-to-all-start.1 = ((bf16[32,2,256,128]{3,2,1,0:T(8,128)(2,1)}), bf16[32,2,256,128]{3,2,1,0:T(8,128)(2,1)}, u32[]{:S(2)}, u32[]{:S(2)}) async-start(bf16[32,2,256,128]{3,2,1,0:T(8,128)(2,1)} %bitcast.20), calls=%async_computation.1 | async-start | bytes 8388608 | tf_op jit(solution)/shard_map/all_to_all | solution.py:444
  190.9 11.3 %copy-start.6 = (f32[4096]{0:T(1024)S(1)}, f32[4096]{0:T(1024)}, u32[]{:S(2)}) copy-start(f32[4096]{0:T(1024)} %param.11) | copy-start | bytes 49156
  200.2 8.1 %collective-permute-start.16 = (bf16[128,1024]{1,0:T(8,128)(2,1)S(1)}, bf16[128,1024]{1,0:T(8,128)(2,1)S(1)}, u32[]{:S(2)}, u32[]{:S(2)}) collective-permute-start(bf16[128,1024]{1,0:T(8,128)(2,1)S(1)} %last.1), channel_id=1, source_target_pairs={{0,0},{32,1},{64,2},{96,3},{128,4},{160,5},{192,6},{224,7},{33,32}... | collective-permute-start | bytes 786440 | tf_op jit(solution)/shard_map/ppermute | solution.py:471
  (5 other events, 4.0 us)

commit v5 on v4

v5 whole, which is shorter than its diff:
```python
import functools
import math

import jax
import jax.numpy as jnp
from jax import lax
from jax.experimental import pallas as pl
from jax.experimental.pallas import tpu as pltpu
from jax.sharding import Mesh
from jax.sharding import PartitionSpec as P

Z = "sp_0"
SP = ("sp_0", "sp_1")
DP = ("dp_0", "dp_1")
PLANE = ("dp_0", "dp_1", "sp_1")
Z_DP = ("sp_0", "dp_0", "dp_1")

norm_floor = 0.5
root_half = 1.0 / math.sqrt(2.0)
inv_root_tau = 1.0 / math.sqrt(2.0 * math.pi)
LANES = 128
F32 = jnp.float32
BF16 = jnp.bfloat16


def normal_cdf(x):
    return 0.5 * (1.0 + lax.erf(x * root_half))


HBM = pl.BlockSpec(memory_space=pltpu.HBM)
VMEM = pl.BlockSpec(memory_space=pltpu.VMEM)


def limit(mib):
    return pltpu.CompilerParams(vmem_limit_bytes=mib * 1024 * 1024)


def params(mib):
    return pltpu.CompilerParams(
        dimension_semantics=("arbitrary",), vmem_limit_bytes=mib * 1024 * 1024
    )


def prologue_kernel(
    groups, rows, cot_hbm, up_hbm, val_hbm, gain_ref, out_hbm, inv_ref, cot_ref, up_ref, val_ref, out_ref, act_ref, sems
):
    toks = cot_ref.shape[0]
    steps = toks // rows

    def loads(i):
        at = pl.ds(pl.multiple_of(i * rows, rows), rows)
        pairs = ((cot_hbm, cot_ref), (up_hbm, up_ref), (val_hbm, val_ref))
        return [
            pltpu.make_async_copy(src.at[at], dst.at[at], sems.at[k, i])
            for k, (src, dst) in enumerate(pairs)
        ]

    def store(i):
        at = pl.ds(pl.multiple_of(i * rows, rows), rows)
        return pltpu.make_async_copy(out_ref.at[:, :, at], out_hbm.at[:, :, at], sems.at[3, i])

    for i in range(AHEAD):
        for copy in loads(i):
            copy.start()

    def step(i, carry):
        for copy in loads(i):
            copy.wait()

        @pl.when(i + AHEAD < steps)
        def _():
            for copy in loads(i + AHEAD):
                copy.start()

        at = pl.ds(pl.multiple_of(i * rows, rows), rows)

        def first(g, squares):
            cols = pl.ds(pl.multiple_of(g * LANES, LANES), LANES)
            up = up_ref[at, cols].astype(F32)
            up_act = (up * normal_cdf(up)).astype(BF16).astype(F32)
            out_ref[g, 0, at] = (cot_ref[at, cols].astype(F32) * up_act).astype(BF16)
            val = val_ref[at, cols].astype(F32)
            act = val * normal_cdf(val)
            act_ref[:, cols] = act
            return squares + act * act

        squares = lax.fori_loop(0, groups, first, jnp.zeros((rows, LANES), F32), unroll=UNROLL)
        mean = jnp.sum(squares, axis=1, keepdims=True) * (1.0 / (groups * LANES))
        inv = lax.rsqrt(mean + norm_floor)
        inv_ref[at] = jnp.broadcast_to(inv, (rows, LANES))

        def second(g, carry):
            cols = pl.ds(pl.multiple_of(g * LANES, LANES), LANES)
            out_ref[g, 1, at] = (act_ref[:, cols] * inv * gain_ref[:, cols]).astype(BF16)
            return carry

        lax.fori_loop(0, groups, second, 0, unroll=4)
        store(i).start()
        return carry

    lax.fori_loop(0, steps, step, 0)
    for i in range(steps):
        store(i).wait()


UNROLL = 4
AHEAD = 4


def prologue(cot, up, val, gain, rows=64):
    toks, width = cot.shape
    groups = width // LANES
    whole = pltpu.VMEM((toks, width), BF16)
    return pl.pallas_call(
        functools.partial(prologue_kernel, groups, rows),
        in_specs=[HBM, HBM, HBM, VMEM],
        out_specs=[HBM, VMEM],
        out_shape=[
            jax.ShapeDtypeStruct((groups, 2, toks, LANES), BF16),
            jax.ShapeDtypeStruct((toks, LANES), F32),
        ],
        scratch_shapes=[
            whole,
            whole,
            whole,
            pltpu.VMEM((groups, 2, toks, LANES), BF16),
            pltpu.VMEM((rows, width), F32),
            pltpu.SemaphoreType.DMA((4, toks // rows)),
        ],
        compiler_params=limit(60),
        cost_estimate=pl.CostEstimate(
            flops=100 * toks * width, bytes_accessed=10 * toks * width, transcendentals=0
        ),
        name="prologue",
    )(cot, up, val, gain)


def slopes_kernel(up_ref, val_ref, up_slope_ref, val_slope_ref, act_ref):
    groups = up_ref.shape[1] // LANES

    def step(g, carry):
        at = pl.ds(pl.multiple_of(g * LANES, LANES), LANES)
        up = up_ref[:, at].astype(F32)
        up_slope = normal_cdf(up) + up * (jnp.exp(-0.5 * up * up) * inv_root_tau)
        up_slope_ref[:, at] = up_slope.astype(BF16)
        val = val_ref[:, at].astype(F32)
        phi = normal_cdf(val)
        act_ref[:, at] = (val * phi).astype(BF16)
        val_slope = phi + val * (jnp.exp(-0.5 * val * val) * inv_root_tau)
        val_slope_ref[:, at] = val_slope.astype(BF16)
        return carry

    lax.fori_loop(0, groups, step, 0, unroll=2)


def slopes(up, val, rows=64):
    toks, width = up.shape
    row = pl.BlockSpec((rows, width), lambda i: (i, 0))
    out = jax.ShapeDtypeStruct((toks, width), BF16)
    return pl.pallas_call(
        slopes_kernel,
        grid=(toks // rows,),
        in_specs=[row, row],
        out_specs=[row, row, row],
        out_shape=[out, out, out],
        compiler_params=params(60),
        cost_estimate=pl.CostEstimate(
            flops=100 * toks * width, bytes_accessed=16 * toks * width, transcendentals=0
        ),
        name="slopes",
    )(up, val)


def slab_of(z_offset):
    z = (lax.axis_index(Z) + z_offset + 8) % 8
    return z ^ (lax.axis_index("dp_0") * 2 + lax.axis_index("dp_1"))


OFFSETS = (0, -1, -2, -3, 1, 2, 3, 4)
PAD = 8


def arrange_kernel(*refs):
    *pieces, w_ref, wt_ref = refs
    slab = pieces[0].shape[0]
    for d, piece in enumerate(pieces):
        at = pl.ds(pl.multiple_of(slab_of(OFFSETS[d]) * slab, slab), slab)
        rows = piece[...]
        w_ref[at] = rows
        wt_ref[:, at] = jnp.transpose(rows)


def arrange(pieces):
    _, block = pieces[0].shape
    return pl.pallas_call(
        arrange_kernel,
        in_specs=[VMEM] * len(pieces),
        out_specs=[VMEM] * 2,
        out_shape=[
            jax.ShapeDtypeStruct((block, block), BF16),
            jax.ShapeDtypeStruct((block, block), BF16),
        ],
        compiler_params=limit(8),
        cost_estimate=pl.CostEstimate(
            flops=4 * block * block, bytes_accessed=6 * block * block, transcendentals=0
        ),
        name="arrange",
    )(*pieces)


def mix_kernel(
    seqs, parts, per, recv_hbm, w_hbm, wt_hbm, bias_row_ref, out_hbm, sums_ref,
    recv_ref, out_ref, w_ref, wt_ref, bias_ref, sems, fixed_sems
):
    toks = recv_ref.shape[2]
    block = parts * toks
    steps = seqs // per

    def load(j):
        at = pl.ds(j * (per * parts), per * parts)
        return pltpu.make_async_copy(recv_hbm.at[at], recv_ref.at[at], sems.at[0, j])

    def store(j):
        at = pl.ds(j * per, per)
        return pltpu.make_async_copy(out_ref.at[at], out_hbm.at[at], sems.at[1, j])

    def side_by_side(j, which):
        return jnp.concatenate(
            [
                recv_ref[pl.ds((j * per + b) * parts, parts), which].reshape(block, LANES)
                for b in range(per)
            ],
            axis=1,
        )

    fixed = [
        pltpu.make_async_copy(src, dst, fixed_sems.at[k])
        for k, (src, dst) in enumerate(((wt_hbm, wt_ref), (w_hbm, w_ref)))
    ]
    fixed[0].start()
    load(0).start()
    fixed[1].start()
    for j in range(1, steps):
        load(j).start()
    bias_ref[...] = jnp.transpose(jnp.broadcast_to(bias_row_ref[...], (LANES, block)))
    fixed[0].wait()

    def step(j, total):
        load(j).wait()
        gate = side_by_side(j, 0)
        back = jnp.dot(wt_ref[...], gate, preferred_element_type=F32).astype(BF16)
        value = side_by_side(j, 1)
        for b in range(per):
            cols = slice(b * LANES, (b + 1) * LANES)
            out_ref[j * per + b, :, 1] = back[:, cols].reshape(parts, toks, LANES)
            terms = back[:, cols].astype(F32) * value[:, cols].astype(F32)
            total += jnp.sum(terms.reshape(block // 8, 8, LANES), axis=0)

        @pl.when(j == 0)
        def _():
            fixed[1].wait()

        mixed = jnp.dot(w_ref[...], value, preferred_element_type=F32)
        for b in range(per):
            cols = slice(b * LANES, (b + 1) * LANES)
            part = (mixed[:, cols] + bias_ref[...]).astype(BF16)
            out_ref[j * per + b, :, 0] = part.reshape(parts, toks, LANES)
        store(j).start()
        return total

    total = lax.fori_loop(0, steps, step, jnp.zeros((8, LANES), F32))
    sums_ref[...] = jnp.sum(total, axis=0, keepdims=True)
    for j in range(steps):
        store(j).wait()


PER = 4


def mix(recv, w, wt, bias, seqs, parts):
    toks = recv.shape[2]
    block = parts * toks
    whole = (seqs, parts, 2, toks, LANES)
    out, sums = pl.pallas_call(
        functools.partial(mix_kernel, seqs, parts, PER),
        in_specs=[HBM] * 3 + [VMEM],
        out_specs=[HBM, VMEM],
        out_shape=[jax.ShapeDtypeStruct(whole, BF16), jax.ShapeDtypeStruct((1, LANES), F32)],
        scratch_shapes=[
            pltpu.VMEM(recv.shape, BF16),
            pltpu.VMEM(whole, BF16),
            pltpu.VMEM((block, block), BF16),
            pltpu.VMEM((block, block), BF16),
            pltpu.VMEM((block, LANES), F32),
            pltpu.SemaphoreType.DMA((2, seqs // PER)),
            pltpu.SemaphoreType.DMA((2,)),
        ],
        compiler_params=limit(60),
        cost_estimate=pl.CostEstimate(
            flops=4 * block * block * seqs * LANES, bytes_accessed=10 * block * block, transcendentals=0
        ),
        name="mix",
    )(recv, w, wt, bias)
    return out.reshape(recv.shape), sums


def split(x):
    high = x.astype(BF16)
    middle = (x - high.astype(F32)).astype(BF16)
    low = (x - high.astype(F32) - middle.astype(F32)).astype(BF16)
    return high, middle, low


def pack_sums(sums):
    bias = split(sums[:, LANES:])
    wide = jnp.concatenate([sums[:, :LANES], jnp.zeros_like(sums[:, 2 * LANES :])], axis=1)
    gain = split(wide)
    zeros = jnp.zeros_like(bias[0])
    return jnp.concatenate([*bias, *gain, zeros, zeros], axis=0)


def unpack_sums(rows):
    rows = rows.astype(F32)
    bias = rows[0:1] + rows[1:2] + rows[2:3]
    gain = rows[3:4] + rows[4:5] + rows[5:6]
    return jnp.concatenate([gain[:, :LANES], bias], axis=1)


def grads_kernel(seqs, parts, recv_ref, sums_ref, *refs):
    outs = refs[:seqs]
    gate_ref, value_ref, grad_ref, rows_ref, sems = refs[seqs:]
    toks = recv_ref.shape[2]
    block = parts * toks
    slab = block // seqs
    for b in range(seqs):
        cols = slice(b * LANES, (b + 1) * LANES)
        pieces = slice(b * parts, (b + 1) * parts)
        pltpu.make_async_copy(recv_ref.at[pieces, 0], gate_ref.at[:, :, cols], sems.at[0, 0]).start()
        pltpu.make_async_copy(recv_ref.at[pieces, 1], value_ref.at[:, :, cols], sems.at[1, 0]).start()
    pltpu.make_async_copy(gate_ref, gate_ref, sems.at[0, 0]).wait()
    bias_sums = []
    for y in range(parts):
        gate = gate_ref[y].astype(F32)
        gate = sum(gate[:, b * LANES : (b + 1) * LANES] for b in range(seqs))
        bias_sums.append(jnp.sum(jnp.transpose(gate), axis=0, keepdims=True))
    rows_ref[...] = pack_sums(jnp.concatenate([sums_ref[...], *bias_sums], axis=1))
    for d in range(seqs):
        pltpu.make_async_copy(rows_ref, outs[d].at[slab:], sems.at[3, d]).start()
    pltpu.make_async_copy(value_ref, value_ref, sems.at[1, 0]).wait()

    def step(y, carry):
        grad = lax.dot_general(
            gate_ref[...].reshape(block, seqs * LANES),
            value_ref[y],
            (((1,), (1,)), ((), ())),
            preferred_element_type=F32,
        )
        grad_ref[y] = grad.astype(BF16)
        at = pl.ds(pl.multiple_of(y * toks, toks), toks)
        for d in range(seqs):
            rows = pl.ds(pl.multiple_of(slab_of(-OFFSETS[d]) * slab, slab), slab)
            pltpu.make_async_copy(grad_ref.at[y, rows], outs[d].at[:slab, at], sems.at[2, 0]).start()
        return carry

    lax.fori_loop(0, parts, step, 0)
    pltpu.make_async_copy(grad_ref, grad_ref, sems.at[2, 0]).wait()
    for d in range(seqs):
        pltpu.make_async_copy(rows_ref, outs[d].at[slab:], sems.at[3, d]).wait()


def weight_grads(recv, sums, seqs, parts):
    toks = recv.shape[2]
    block = parts * toks
    flat = pltpu.VMEM((parts, toks, seqs * LANES), BF16)
    return pl.pallas_call(
        functools.partial(grads_kernel, seqs, parts),
        in_specs=[HBM, VMEM],
        out_specs=[HBM] * seqs,
        out_shape=[jax.ShapeDtypeStruct((block // seqs + PAD, block), BF16)] * seqs,
        scratch_shapes=[
            flat,
            flat,
            pltpu.VMEM((parts, block, toks), BF16),
            pltpu.VMEM((PAD, block), BF16),
            pltpu.SemaphoreType.DMA((4, seqs)),
        ],
        compiler_params=limit(28),
        cost_estimate=pl.CostEstimate(
            flops=2 * block * block * seqs * LANES, bytes_accessed=6 * block * block, transcendentals=0
        ),
        name="weight_grads",
    )(recv, sums)


def hop_kernel(slab, *refs):
    n = len(refs) // 3
    for here, there, out in zip(refs[:n], refs[n : 2 * n], refs[2 * n :]):
        out[:slab] = (here[:slab].astype(F32) + there[:slab].astype(F32)).astype(BF16)
        out[slab:] = pack_sums(unpack_sums(here[slab:]) + unpack_sums(there[slab:]))


def hop(here, there):
    height, width = here[0].shape
    return pl.pallas_call(
        functools.partial(hop_kernel, height - PAD),
        in_specs=[VMEM] * (2 * len(here)),
        out_specs=[VMEM] * len(here),
        out_shape=[jax.ShapeDtypeStruct((height, width), BF16)] * len(here),
        compiler_params=limit(8),
        cost_estimate=pl.CostEstimate(
            flops=2 * height * width, bytes_accessed=12 * height * width, transcendentals=0
        ),
        name="hop",
    )(*here, *there)


def last_kernel(slab, *refs):
    *ins, grad_ref = refs
    grad_ref[...] = sum(r[:slab].astype(F32) for r in ins).astype(BF16)


def last(pieces):
    height, width = pieces[0].shape
    return pl.pallas_call(
        functools.partial(last_kernel, height - PAD),
        in_specs=[VMEM] * 3,
        out_specs=VMEM,
        out_shape=jax.ShapeDtypeStruct((height - PAD, width), BF16),
        compiler_params=limit(8),
        cost_estimate=pl.CostEstimate(
            flops=4 * height * width, bytes_accessed=8 * height * width, transcendentals=0
        ),
        name="last",
    )(*pieces)


def pack_kernel(slab, seqs, parts, *refs):
    *ins, small_ref = refs
    sums = sum(unpack_sums(r[slab:]) for r in ins)
    small_ref[...] = jnp.zeros_like(small_ref)
    for a in range(seqs):
        at = slice((a + 1) * LANES, (a + 2) * LANES)
        for y in range(parts):
            small_ref[a * parts + y, :1] = sums[:, :LANES]
            small_ref[a * parts + y, 1:2] = sums[:, at]


def pack(pieces, seqs, parts):
    slab = pieces[0].shape[0] - PAD
    return pl.pallas_call(
        functools.partial(pack_kernel, slab, seqs, parts),
        in_specs=[VMEM] * 3,
        out_specs=VMEM,
        out_shape=jax.ShapeDtypeStruct((seqs * parts, 8, LANES), F32),
        compiler_params=limit(8),
        name="pack",
    )(*pieces)


def epilogue_kernel(
    groups, rows, recv_hbm, cot_hbm, up_slope_hbm, val_slope_hbm, act_hbm, inv_ref, gain_ref, up_hbm, val_hbm,
    recv_ref, cot_ref, up_slope_ref, val_slope_ref, act_ref, up_ref, val_ref, sems
):
    toks = cot_ref.shape[0]
    steps = toks // rows

    def loads(i):
        at = pl.ds(pl.multiple_of(i * rows, rows), rows)
        pairs = (
            (cot_hbm, cot_ref),
            (up_slope_hbm, up_slope_ref),
            (val_slope_hbm, val_slope_ref),
            (act_hbm, act_ref),
        )
        return [pltpu.make_async_copy(recv_hbm.at[:, :, at], recv_ref.at[:, :, at], sems.at[0, i])] + [
            pltpu.make_async_copy(src.at[at], dst.at[at], sems.at[3 + k, i])
            for k, (src, dst) in enumerate(pairs)
        ]

    def stores(i):
        at = pl.ds(pl.multiple_of(i * rows, rows), rows)
        return [
            pltpu.make_async_copy(up_ref.at[at], up_hbm.at[at], sems.at[1, i]),
            pltpu.make_async_copy(val_ref.at[at], val_hbm.at[at], sems.at[2, i]),
        ]

    for i in range(AHEAD):
        for copy in loads(i):
            copy.start()

    def step(i, carry):
        for copy in loads(i):
            copy.wait()

        @pl.when(i + AHEAD < steps)
        def _():
            for copy in loads(i + AHEAD):
                copy.start()

        at = pl.ds(pl.multiple_of(i * rows, rows), rows)

        def first(g, dots):
            cols = pl.ds(pl.multiple_of(g * LANES, LANES), LANES)
            mid = (cot_ref[at, cols].astype(F32) * recv_ref[g, 0, at].astype(F32)).astype(BF16)
            up_ref[at, cols] = (mid.astype(F32) * up_slope_ref[at, cols].astype(F32)).astype(BF16)
            scaled = recv_ref[g, 1, at].astype(F32) * gain_ref[:, cols]
            return dots + scaled * act_ref[at, cols].astype(F32)

        dots = lax.fori_loop(0, groups, first, jnp.zeros((rows, LANES), F32), unroll=4)
        mean = jnp.sum(dots, axis=1, keepdims=True) * (1.0 / (groups * LANES))
        inv = inv_ref[at]
        pull = inv * inv * inv * mean

        def second(g, carry):
            cols = pl.ds(pl.multiple_of(g * LANES, LANES), LANES)
            scaled = recv_ref[g, 1, at].astype(F32) * gain_ref[:, cols]
            slope = inv * scaled - pull * act_ref[at, cols].astype(F32)
            val_ref[at, cols] = (slope * val_slope_ref[at, cols].astype(F32)).astype(BF16)
            return carry

        lax.fori_loop(0, groups, second, 0, unroll=4)
        for copy in stores(i):
            copy.start()
        return carry

    lax.fori_loop(0, steps, step, 0)
    for i in range(steps):
        for copy in stores(i):
            copy.wait()


def epilogue(recv, cot, up_slope, val_slope, act, inv, gain, rows=64):
    toks, width = cot.shape
    groups = width // LANES
    out = jax.ShapeDtypeStruct((toks, width), BF16)
    whole = pltpu.VMEM((toks, width), BF16)
    return pl.pallas_call(
        functools.partial(epilogue_kernel, groups, rows),
        in_specs=[HBM] * 5 + [VMEM] * 2,
        out_specs=[HBM, HBM],
        out_shape=[out, out],
        scratch_shapes=[
            pltpu.VMEM(recv.shape, BF16),
            whole,
            whole,
            whole,
            whole,
            whole,
            whole,
            pltpu.SemaphoreType.DMA((7, toks // rows)),
        ],
        compiler_params=limit(EPI_MIB),
        cost_estimate=pl.CostEstimate(
            flops=20 * toks * width, bytes_accessed=22 * toks * width, transcendentals=0
        ),
        name="epilogue",
    )(recv, cot, up_slope, val_slope, act, inv, gain)


EPI_MIB = 60


def shards(cotangent, up_pre, value_pre, spatial_weight, spatial_bias, value_gain):
    planes = lax.axis_size(Z)
    seqs = lax.axis_size(DP)
    parts = lax.axis_size("sp_1")
    cot, up, val = cotangent[0], up_pre[0], value_pre[0]
    gain = value_gain[None]
    away = [(z * seqs + a, (z ^ a) * seqs + z) for z in range(planes) for a in range(seqs)]
    home = [(there, here) for here, there in away]

    def exchange(x):
        return lax.all_to_all(x, PLANE, split_axis=0, concat_axis=0, tiled=True)

    def shifted(x, by):
        return lax.ppermute(x, Z, [(z, (z + by) % planes) for z in range(planes)])

    weights = lax.ppermute(spatial_weight[0], Z_DP, away)
    bias = lax.ppermute(spatial_bias, Z_DP, away)
    sent, inv = prologue(cot, up, val, gain)
    recv = exchange(sent)
    before, after = [weights], [weights]
    for _ in range(3):
        before.append(shifted(before[-1], 1))
        after.append(shifted(after[-1], -1))
    after.append(shifted(after[-1], -1))
    pieces = before + after[1:]
    up_slope, val_slope, act = slopes(up, val)
    w, wt = arrange(pieces)
    back, sums = mix(recv, w, wt, bias, seqs, parts)
    back = exchange(back)
    own, p1, p2, p3, m1, m2, m3, m4 = weight_grads(recv, sums, seqs, parts)
    plus, minus = shifted(p3, 1), shifted(m4, -1)
    plus, minus = hop((p2, m3), (plus, minus))
    plus, minus = shifted(plus, 1), shifted(minus, -1)
    plus, minus = hop((p1, m2), (plus, minus))
    plus, minus = shifted(plus, 1), shifted(minus, -1)
    (minus,) = hop((m1,), (minus,))
    minus = shifted(minus, -1)
    grads = last((own, plus, minus))
    grads = lax.ppermute(grads, Z_DP, home)
    small = pack((own, plus, minus), seqs, parts)
    small = exchange(small)
    gain_grad = small[:, 0].reshape(-1) / value_gain
    mine = lax.axis_index(Z) * parts + lax.axis_index("sp_1")
    bias_grad = lax.dynamic_slice_in_dim(small, mine, 1, axis=0)[:, 1]
    up_grad, value_grad = epilogue(back, cot, up_slope, val_slope, act, inv, gain)
    return (up_grad[None], value_grad[None], grads[None].astype(F32), bias_grad, gain_grad)


def solution(mesh):
    torus = Mesh(mesh.devices.reshape(8, 4, 4, 2), ("sp_0", "sp_1", "dp_0", "dp_1"))
    in_specs = (
        P(DP, SP, None),
        P(DP, SP, None),
        P(DP, SP, None),
        P(SP, DP, None),
        P(SP, None),
        P(),
    )
    out_specs = (P(DP, SP, None), P(DP, SP, None), P(SP, DP, None), P(SP, DP), P())
    return jax.shard_map(
        shards, mesh=torus, in_specs=in_specs, out_specs=out_specs, check_vma=False
    )
```

time: 264 us -> 254 us (0.962)
  Pallas kernels: 50.1 us -> 41.5 us
    pallas_call x4 -> x5, Pallas kernels: 40.2 us -> 33.3 us  [the longest x1 9.96 us: mix(): pl.pallas_call(functools.partial(mix_kernel, seqs, parts, PER), in_specs=...]
  transfers between devices with their start and end apart: 19 -> 19, of which waited for: 11 -> 11; matrix products, arithmetic and copies ran while one was open for 1% -> 1% of each run, Pallas kernels for 4% -> 3%
where the time goes in v5:
time: 254 us; the launch traced here: 249 us
  starting transfers between devices  96.8 us (38%)
  waiting for transfers between devices  80.6 us (32%)
  Pallas kernels  41.5 us (16%)
  blocking collectives  23.2 us (9%)
  local copies, waits for them, and re-layouts  4.42 us (2%)
    all_to_all x2, waiting for transfers between devices, exchange(): return lax.all_to_all(x, PLANE, split_axis=0, concat_axis=0, tiled=True)  41.7 us
    ppermute x14, starting transfers between devices, shifted(): return lax.ppermute(x, Z, [(z, (z + by) % planes) for z in range(planes)])  41.2 us
    ppermute x1, starting transfers between devices, shards(): bias = lax.ppermute(spatial_bias, Z_DP, away)  35.4 us
    ppermute x14, waiting for transfers between devices, shifted(): return lax.ppermute(x, Z, [(z, (z + by) % planes) for z in range(planes)])  30.3 us
    all_to_all x1, blocking collectives, exchange(): return lax.all_to_all(x, PLANE, split_axis=0, concat_axis=0, tiled=True)  23.2 us
    all_to_all x2, starting transfers between devices, exchange(): return lax.all_to_all(x, PLANE, split_axis=0, concat_axis=0, tiled=True)  13.7 us
    pallas_call x1, Pallas kernels, mix(): pl.pallas_call(functools.partial(mix_kernel, seqs, parts, PER), in_specs=...  9.96 us
    pallas_call x1, Pallas kernels, epilogue(): pl.pallas_call(functools.partial(epilogue_kernel, groups, rows), in_specs...  8.45 us
  transfers between devices with their start and end apart: 19, of which 11 were waited for; matrix products, arithmetic and copies ran while one was open for 1% of the time, Pallas kernels for 3%

profile of v5, /device:TPU:1, one launch (start us, length us, event | category | flops | bytes accessed | tf_op | source)
XLA Modules:
  0.0 248.9 jit_solution(6775109292525390521)
XLA Ops:
  0.6 7.8 %prologue.1 = (bf16[32,2,256,128]{3,2,1,0:T(8,128)(2,1)}, f32[256,128]{1,0:T(8,128)}) custom-call(bf16[256,4096]{1,0:T(8,128)(2,1)} %bitcast.14, bf16[256,4096]{1,0:T(8,128)(2,1)} %bitcast.16, bf16[256,4096]{1,0:T(8,128)(2,1)} %bitcast.18, f32[1,4096]{1,0:T(1,128)} %bitcast.21), custom_call_target="tpu_custom_call" | custom-call | flops 104857600 | bytes 10485760 | tf_op jit(solution)/shard_map/prologue/pallas_call | solution.py:114
  8.5 8.8 %all-to-all-start = ((bf16[32,2,256,128]{3,2,1,0:T(8,128)(2,1)}), bf16[32,2,256,128]{3,2,1,0:T(8,128)(2,1)}, u32[]{:S(2)}, u32[]{:S(2)}) async-start(bf16[32,2,256,128]{3,2,1,0:T(8,128)(2,1)} %get-tuple-element.28), calls=%async_computation | async-start | bytes 8388608 | tf_op jit(solution)/shard_map/all_to_all | solution.py:573
  17.3 3.7 %collective-permute-start = (bf16[128,1024]{1,0:T(8,128)(2,1)S(1)}, bf16[128,1024]{1,0:T(8,128)(2,1)S(1)}, u32[]{:S(2)}, u32[]{:S(2)}) collective-permute-start(bf16[128,1024]{1,0:T(8,128)(2,1)S(1)} %bitcast.26), channel_id=1, source_target_pairs={{0,0},{1,32},{2,64},{3,96},{4,128},{5,160},{6,192},{7,224},{32,33}... | collective-permute-start | bytes 786440 | tf_op jit(solution)/shard_map/ppermute | solution.py:578
  21.0 4.0 %collective-permute-done.refs_0_ = bf16[128,1024]{1,0:T(8,128)(2,1)S(1)} collective-permute-done((bf16[128,1024]{1,0:T(8,128)(2,1)S(1)}, bf16[128,1024]{1,0:T(8,128)(2,1)S(1)}, u32[]{:S(2)}, u32[]{:S(2)}) %collective-permute-start) | collective-permute-done | bytes 262176 | tf_op jit(solution)/shard_map/ppermute | solution.py:578
  25.0 13.4 %collective-permute-start.4 = (bf16[128,1024]{1,0:T(8,128)(2,1)S(1)}, bf16[128,1024]{1,0:T(8,128)(2,1)S(1)}, u32[]{:S(2)}, u32[]{:S(2)}) collective-permute-start(bf16[128,1024]{1,0:T(8,128)(2,1)S(1)} %collective-permute-done.refs_0_), channel_id=1, source_target_pairs={{0,224},{32,0},{64,32},{96,64},{128,96},{160,128},{192,160},{224,1... | collective-permute-start | bytes 786440 | tf_op jit(solution)/shard_map/ppermute | solution.py:576
  38.4 3.3 %collective-permute-done.4.refs_4_ = bf16[128,1024]{1,0:T(8,128)(2,1)S(1)} collective-permute-done((bf16[128,1024]{1,0:T(8,128)(2,1)S(1)}, bf16[128,1024]{1,0:T(8,128)(2,1)S(1)}, u32[]{:S(2)}, u32[]{:S(2)}) %collective-permute-start.4) | collective-permute-done | bytes 262176 | tf_op jit(solution)/shard_map/ppermute | solution.py:576
  41.7 3.5 %collective-permute-start.5 = (bf16[128,1024]{1,0:T(8,128)(2,1)S(1)}, bf16[128,1024]{1,0:T(8,128)(2,1)S(1)}, u32[]{:S(2)}, u32[]{:S(2)}) collective-permute-start(bf16[128,1024]{1,0:T(8,128)(2,1)S(1)} %collective-permute-done.4.refs_4_), channel_id=1, source_target_pairs={{0,224},{32,0},{64,32},{96,64},{128,96},{160,128},{192,160},{224,1... | collective-permute-start | bytes 786440 | tf_op jit(solution)/shard_map/ppermute | solution.py:576
  45.2 3.3 %collective-permute-done.5.refs_5_ = bf16[128,1024]{1,0:T(8,128)(2,1)S(1)} collective-permute-done((bf16[128,1024]{1,0:T(8,128)(2,1)S(1)}, bf16[128,1024]{1,0:T(8,128)(2,1)S(1)}, u32[]{:S(2)}, u32[]{:S(2)}) %collective-permute-start.5) | collective-permute-done | bytes 262176 | tf_op jit(solution)/shard_map/ppermute | solution.py:576
  48.5 3.5 %collective-permute-start.6 = (bf16[128,1024]{1,0:T(8,128)(2,1)S(1)}, bf16[128,1024]{1,0:T(8,128)(2,1)S(1)}, u32[]{:S(2)}, u32[]{:S(2)}) collective-permute-start(bf16[128,1024]{1,0:T(8,128)(2,1)S(1)} %collective-permute-done.5.refs_5_), channel_id=1, source_target_pairs={{0,224},{32,0},{64,32},{96,64},{128,96},{160,128},{192,160},{224,1... | collective-permute-start | bytes 786440 | tf_op jit(solution)/shard_map/ppermute | solution.py:576
  52.1 3.3 %collective-permute-done.6.refs_6_ = bf16[128,1024]{1,0:T(8,128)(2,1)S(1)} collective-permute-done((bf16[128,1024]{1,0:T(8,128)(2,1)S(1)}, bf16[128,1024]{1,0:T(8,128)(2,1)S(1)}, u32[]{:S(2)}, u32[]{:S(2)}) %collective-permute-start.6) | collective-permute-done | bytes 262176 | tf_op jit(solution)/shard_map/ppermute | solution.py:576
  55.4 3.5 %collective-permute-start.7 = (bf16[128,1024]{1,0:T(8,128)(2,1)S(1)}, bf16[128,1024]{1,0:T(8,128)(2,1)S(1)}, u32[]{:S(2)}, u32[]{:S(2)}) collective-permute-start(bf16[128,1024]{1,0:T(8,128)(2,1)S(1)} %collective-permute-done.6.refs_6_), channel_id=1, source_target_pairs={{0,224},{32,0},{64,32},{96,64},{128,96},{160,128},{192,160},{224,1... | collective-permute-start | bytes 786440 | tf_op jit(solution)/shard_map/ppermute | solution.py:576
  58.9 35.4 %collective-permute-start.8 = (f32[1,1024]{1,0:T(1,128)S(1)}, f32[1,1024]{1,0:T(1,128)S(1)}, u32[]{:S(2)}, u32[]{:S(2)}) collective-permute-start(f32[1,1024]{1,0:T(1,128)S(1)} %copy-done.5), channel_id=1, source_target_pairs={{0,0},{1,32},{2,64},{3,96},{4,128},{5,160},{6,192},{7,224},{32,33}... | collective-permute-start | bytes 12296 | tf_op jit(solution)/shard_map/ppermute | solution.py:579
  95.1 1.3 copy-done
  96.5 1.3 copy-done.1
  98.4 10.0 %mix.1 = (bf16[8,4,2,256,128]{4,3,2,1,0:T(8,128)(2,1)}, f32[1,128]{1,0:T(1,128)}) custom-call(bf16[32,2,256,128]{3,2,1,0:T(8,128)(2,1)} %all-to-all-done.recv_hbm.recv_ref, bf16[1024,1024]{1,0:T(8,128)(2,1)} %copy-done, bf16[1024,1024]{1,0:T(8,128)(2,1)} %copy-done.1, f32[1,1024]{1,0:T(1,128)} %copy-done.6), custom_call_target="tpu_custom_call" | custom-call | flops 4294967296 | bytes 10485760 | tf_op jit(solution)/shard_map/mix/pallas_call | solution.py:284
  109.0 6.3 %weight_grads.1 = (bf16[136,1024]{1,0:T(8,128)(2,1)S(1)}, bf16[136,1024]{1,0:T(8,128)(2,1)S(1)}, bf16[136,1024]{1,0:T(8,128)(2,1)S(1)}, bf16[136,1024]{1,0:T(8,1...) custom-call(bf16[32,2,256,128]{3,2,1,0:T(8,128)(2,1)} %all-to-all-do, ...), custom_call_target="tpu_custom_call" | custom-call | flops 2147483648 | bytes 6291456 | tf_op jit(solution)/shard_map/weight_grads/pallas_call | solution.py:375
  115.3 8.2 %collective-permute-start.10 = (bf16[136,1024]{1,0:T(8,128)(2,1)S(1)}, bf16[136,1024]{1,0:T(8,128)(2,1)S(1)}, u32[]{:S(2)}, u32[]{:S(2)}) collective-permute-start(bf16[136,1024]{1,0:T(8,128)(2,1)S(1)} %get-tuple-element.45), channel_id=1, source_target_pairs={{0,224},{32,0},{64,32},{96,64},{128,96},{160,128},{192,160},{224,1... | collective-permute-start | bytes 835592 | tf_op jit(solution)/shard_map/ppermute | solution.py:576
  123.6 6.0 %collective-permute-done.9.refs_2_ = bf16[136,1024]{1,0:T(8,128)(2,1)S(1)} collective-permute-done((bf16[136,1024]{1,0:T(8,128)(2,1)S(1)}, bf16[136,1024]{1,0:T(8,128)(2,1)S(1)}, u32[]{:S(2)}, u32[]{:S(2)}) %collective-permute-start.9) | collective-permute-done | bytes 278560 | tf_op jit(solution)/shard_map/ppermute | solution.py:576
  130.5 1.3 collective-permute-start.11
  131.8 1.7 collective-permute-start.12
  133.4 6.0 %collective-permute-done.11.refs_2_ = bf16[136,1024]{1,0:T(8,128)(2,1)S(1)} collective-permute-done((bf16[136,1024]{1,0:T(8,128)(2,1)S(1)}, bf16[136,1024]{1,0:T(8,128)(2,1)S(1)}, u32[]{:S(2)}, u32[]{:S(2)}) %collective-permute-start.11) | collective-permute-done | bytes 278560 | tf_op jit(solution)/shard_map/ppermute | solution.py:576
  139.6 2.5 collective-permute-start.14
  142.1 4.1 %collective-permute-done.14.refs_1_ = bf16[136,1024]{1,0:T(8,128)(2,1)S(1)} collective-permute-done((bf16[136,1024]{1,0:T(8,128)(2,1)S(1)}, bf16[136,1024]{1,0:T(8,128)(2,1)S(1)}, u32[]{:S(2)}, u32[]{:S(2)}) %collective-permute-start.14) | collective-permute-done | bytes 278560 | tf_op jit(solution)/shard_map/ppermute | solution.py:576
  146.3 3.5 %collective-permute-start.15 = (bf16[136,1024]{1,0:T(8,128)(2,1)S(1)}, bf16[136,1024]{1,0:T(8,128)(2,1)S(1)}, u32[]{:S(2)}, u32[]{:S(2)}) collective-permute-start(bf16[136,1024]{1,0:T(8,128)(2,1)S(1)} %hop.5), channel_id=1, source_target_pairs={{0,224},{32,0},{64,32},{96,64},{128,96},{160,128},{192,160},{224,1... | collective-permute-start | bytes 835592 | tf_op jit(solution)/shard_map/ppermute | solution.py:576
  149.8 3.5 %collective-permute-done.15.refs_2_ = bf16[136,1024]{1,0:T(8,128)(2,1)S(1)} collective-permute-done((bf16[136,1024]{1,0:T(8,128)(2,1)S(1)}, bf16[136,1024]{1,0:T(8,128)(2,1)S(1)}, u32[]{:S(2)}, u32[]{:S(2)}) %collective-permute-start.15) | collective-permute-done | bytes 278560 | tf_op jit(solution)/shard_map/ppermute | solution.py:576
  153.3 23.2 %all_to_all.15 = f32[32,8,128]{2,1,0:T(8,128)S(1)} all-to-all(f32[32,8,128]{2,1,0:T(8,128)S(1)} %pack.1), channel_id=1, replica_groups=mesh['sp_0'=8,'sp_1'=4,'dp_0'=4,'dp_1'=2] {'dp_0','dp_1','sp_1'}, dimensions={0} | all-to-all | bytes 262144 | tf_op jit(solution)/shard_map/all_to_all | solution.py:573
  176.5 4.9 %all-to-all-start.1 = ((bf16[32,2,256,128]{3,2,1,0:T(8,128)(2,1)}), bf16[32,2,256,128]{3,2,1,0:T(8,128)(2,1)}, u32[]{:S(2)}, u32[]{:S(2)}) async-start(bf16[32,2,256,128]{3,2,1,0:T(8,128)(2,1)} %bitcast.20), calls=%async_computation.1 | async-start | bytes 8388608 | tf_op jit(solution)/shard_map/all_to_all | solution.py:573
  181.5 7.6 %slopes.1 = (bf16[256,4096]{1,0:T(8,128)(2,1)}, bf16[256,4096]{1,0:T(8,128)(2,1)}, bf16[256,4096]{1,0:T(8,128)(2,1)}) custom-call(bf16[256,4096]{1,0:T(8,128)(2,1)} %bitcast.17, bf16[256,4096]{1,0:T(8,128)(2,1)} %bitcast.19), custom_call_target="tpu_custom_call" | custom-call | flops 104857600 | bytes 16777216 | tf_op jit(solution)/shard_map/slopes/pallas_call | solution.py:160
  189.2 2.8 %collective-permute-start.16 = (bf16[128,1024]{1,0:T(8,128)(2,1)S(1)}, bf16[128,1024]{1,0:T(8,128)(2,1)S(1)}, u32[]{:S(2)}, u32[]{:S(2)}) collective-permute-start(bf16[128,1024]{1,0:T(8,128)(2,1)S(1)} %last.1), channel_id=1, source_target_pairs={{0,0},{32,1},{64,2},{96,3},{128,4},{160,5},{192,6},{224,7},{33,32}... | collective-permute-start | bytes 786440 | tf_op jit(solution)/shard_map/ppermute | solution.py:601
  193.1 4.6 %collective-permute-done.16 = bf16[128,1024]{1,0:T(8,128)(2,1)S(1)} collective-permute-done((bf16[128,1024]{1,0:T(8,128)(2,1)S(1)}, bf16[128,1024]{1,0:T(8,128)(2,1)S(1)}, u32[]{:S(2)}, u32[]{:S(2)}) %collective-permute-start.16) | collective-permute-done | bytes 262176 | tf_op jit(solution)/shard_map/ppermute | solution.py:601
  198.6 41.7 %all-to-all-done.1.recv_hbm = bf16[32,2,256,128]{3,2,1,0:T(8,128)(2,1)} async-done(((bf16[32,2,256,128]{3,2,1,0:T(8,128)(2,1)}), bf16[32,2,256,128]{3,2,1,0:T(8,128)(2,1)}, u32[]{:S(2)}, u32[]{:S(2)}) %all-to-all-start.1) | async-done | bytes 4194336 | tf_op jit(solution)/shard_map/all_to_all | solution.py:573
  240.3 8.4 %epilogue.1 = (bf16[256,4096]{1,0:T(8,128)(2,1)}, bf16[256,4096]{1,0:T(8,128)(2,1)}) custom-call(bf16[32,2,256,128]{3,2,1,0:T(8,128)(2,1)} %all-to-all-done.1.recv_hbm, bf16[256,4096]{1,0:T(8,128)(2,1)} %bitcast.15, bf16[256,4096]{1,0:T(8,128)(2,1)} %get-tuple-element.32.up_slope_hbm, bf16[256,4096]{1,0:T(8,128)(2,1)} %get-tuple-element.33.val_slope_hbm, ...), custom_call_target="tpu_custom_call" | custom-call | flops 20971520 | bytes 23068672 | tf_op jit(solution)/shard_map/epilogue/pallas_call | solution.py:537
  (37 shorter events, 5.5 us)
Async XLA Ops:
  8.5 8.8 %copy-start.4 = (bf16[1,128,1024]{2,1,0:T(8,128)(2,1)S(1)}, bf16[1,128,1024]{2,1,0:T(8,128)(2,1)}, u32[]{:S(2)}) copy-start(bf16[1,128,1024]{2,1,0:T(8,128)(2,1)} %param.9) | copy-start | bytes 786436
  8.5 50.4 %copy-start.5 = (f32[1,1024]{1,0:T(1,128)S(1)}, f32[1,1024]{1,0:T(1,128)}, u32[]{:S(2)}) copy-start(f32[1,1024]{1,0:T(1,128)} %param.10) | copy-start | bytes 12292
  8.5 89.3 %all-to-all-start = ((bf16[32,2,256,128]{3,2,1,0:T(8,128)(2,1)}), bf16[32,2,256,128]{3,2,1,0:T(8,128)(2,1)}, u32[]{:S(2)}, u32[]{:S(2)}) async-start(bf16[32,2,256,128]{3,2,1,0:T(8,128)(2,1)} %get-tuple-element.28), calls=%async_computation | async-start | bytes 8388608 | tf_op jit(solution)/shard_map/all_to_all | solution.py:573
  17.3 7.7 %collective-permute-start = (bf16[128,1024]{1,0:T(8,128)(2,1)S(1)}, bf16[128,1024]{1,0:T(8,128)(2,1)S(1)}, u32[]{:S(2)}, u32[]{:S(2)}) collective-permute-start(bf16[128,1024]{1,0:T(8,128)(2,1)S(1)} %bitcast.26), channel_id=1, source_target_pairs={{0,0},{1,32},{2,64},{3,96},{4,128},{5,160},{6,192},{7,224},{32,33}... | collective-permute-start | bytes 786440 | tf_op jit(solution)/shard_map/ppermute | solution.py:578
  25.0 16.7 %collective-permute-start.4 = (bf16[128,1024]{1,0:T(8,128)(2,1)S(1)}, bf16[128,1024]{1,0:T(8,128)(2,1)S(1)}, u32[]{:S(2)}, u32[]{:S(2)}) collective-permute-start(bf16[128,1024]{1,0:T(8,128)(2,1)S(1)} %collective-permute-done.refs_0_), channel_id=1, source_target_pairs={{0,224},{32,0},{64,32},{96,64},{128,96},{160,128},{192,160},{224,1... | collective-permute-start | bytes 786440 | tf_op jit(solution)/shard_map/ppermute | solution.py:576
  38.4 6.8 %collective-permute-start.1 = (bf16[128,1024]{1,0:T(8,128)(2,1)S(1)}, bf16[128,1024]{1,0:T(8,128)(2,1)S(1)}, u32[]{:S(2)}, u32[]{:S(2)}) collective-permute-start(bf16[128,1024]{1,0:T(8,128)(2,1)S(1)} %collective-permute-done.refs_0_), channel_id=1, source_target_pairs={{0,32},{32,64},{64,96},{96,128},{128,160},{160,192},{192,224},{224... | collective-permute-start | bytes 786440 | tf_op jit(solution)/shard_map/ppermute | solution.py:576
  41.7 6.8 %collective-permute-start.5 = (bf16[128,1024]{1,0:T(8,128)(2,1)S(1)}, bf16[128,1024]{1,0:T(8,128)(2,1)S(1)}, u32[]{:S(2)}, u32[]{:S(2)}) collective-permute-start(bf16[128,1024]{1,0:T(8,128)(2,1)S(1)} %collective-permute-done.4.refs_4_), channel_id=1, source_target_pairs={{0,224},{32,0},{64,32},{96,64},{128,96},{160,128},{192,160},{224,1... | collective-permute-start | bytes 786440 | tf_op jit(solution)/shard_map/ppermute | solution.py:576
  45.2 6.8 %collective-permute-start.2 = (bf16[128,1024]{1,0:T(8,128)(2,1)S(1)}, bf16[128,1024]{1,0:T(8,128)(2,1)S(1)}, u32[]{:S(2)}, u32[]{:S(2)}) collective-permute-start(bf16[128,1024]{1,0:T(8,128)(2,1)S(1)} %collective-permute-done.1.refs_1_), channel_id=1, source_target_pairs={{0,32},{32,64},{64,96},{96,128},{128,160},{160,192},{192,224},{224... | collective-permute-start | bytes 786440 | tf_op jit(solution)/shard_map/ppermute | solution.py:576
  48.5 6.8 %collective-permute-start.6 = (bf16[128,1024]{1,0:T(8,128)(2,1)S(1)}, bf16[128,1024]{1,0:T(8,128)(2,1)S(1)}, u32[]{:S(2)}, u32[]{:S(2)}) collective-permute-start(bf16[128,1024]{1,0:T(8,128)(2,1)S(1)} %collective-permute-done.5.refs_5_), channel_id=1, source_target_pairs={{0,224},{32,0},{64,32},{96,64},{128,96},{160,128},{192,160},{224,1... | collective-permute-start | bytes 786440 | tf_op jit(solution)/shard_map/ppermute | solution.py:576
  52.1 42.3 %collective-permute-start.3 = (bf16[128,1024]{1,0:T(8,128)(2,1)S(1)}, bf16[128,1024]{1,0:T(8,128)(2,1)S(1)}, u32[]{:S(2)}, u32[]{:S(2)}) collective-permute-start(bf16[128,1024]{1,0:T(8,128)(2,1)S(1)} %collective-permute-done.2.refs_2_), channel_id=1, source_target_pairs={{0,32},{32,64},{64,96},{96,128},{128,160},{160,192},{192,224},{224... | collective-permute-start | bytes 786440 | tf_op jit(solution)/shard_map/ppermute | solution.py:576
  55.4 39.0 %collective-permute-start.7 = (bf16[128,1024]{1,0:T(8,128)(2,1)S(1)}, bf16[128,1024]{1,0:T(8,128)(2,1)S(1)}, u32[]{:S(2)}, u32[]{:S(2)}) collective-permute-start(bf16[128,1024]{1,0:T(8,128)(2,1)S(1)} %collective-permute-done.6.refs_6_), channel_id=1, source_target_pairs={{0,224},{32,0},{64,32},{96,64},{128,96},{160,128},{192,160},{224,1... | collective-permute-start | bytes 786440 | tf_op jit(solution)/shard_map/ppermute | solution.py:576
  58.9 38.9 %collective-permute-start.8 = (f32[1,1024]{1,0:T(1,128)S(1)}, f32[1,1024]{1,0:T(1,128)S(1)}, u32[]{:S(2)}, u32[]{:S(2)}) collective-permute-start(f32[1,1024]{1,0:T(1,128)S(1)} %copy-done.5), channel_id=1, source_target_pairs={{0,0},{1,32},{2,64},{3,96},{4,128},{5,160},{6,192},{7,224},{32,33}... | collective-permute-start | bytes 12296 | tf_op jit(solution)/shard_map/ppermute | solution.py:579
  95.1 1.3 copy-start
  96.5 1.3 copy-start.1
  97.8 0.6 copy-start.6
  108.3 0.7 copy-start.2
  115.3 14.3 %collective-permute-start.9 = (bf16[136,1024]{1,0:T(8,128)(2,1)S(1)}, bf16[136,1024]{1,0:T(8,128)(2,1)S(1)}, u32[]{:S(2)}, u32[]{:S(2)}) collective-permute-start(bf16[136,1024]{1,0:T(8,128)(2,1)S(1)} %get-tuple-element.44), channel_id=1, source_target_pairs={{0,32},{32,64},{64,96},{96,128},{128,160},{160,192},{192,224},{224... | collective-permute-start | bytes 835592 | tf_op jit(solution)/shard_map/ppermute | solution.py:576
  115.3 15.0 %collective-permute-start.10 = (bf16[136,1024]{1,0:T(8,128)(2,1)S(1)}, bf16[136,1024]{1,0:T(8,128)(2,1)S(1)}, u32[]{:S(2)}, u32[]{:S(2)}) collective-permute-start(bf16[136,1024]{1,0:T(8,128)(2,1)S(1)} %get-tuple-element.45), channel_id=1, source_target_pairs={{0,224},{32,0},{64,32},{96,64},{128,96},{160,128},{192,160},{224,1... | collective-permute-start | bytes 835592 | tf_op jit(solution)/shard_map/ppermute | solution.py:576
  130.5 8.9 %collective-permute-start.11 = (bf16[136,1024]{1,0:T(8,128)(2,1)S(1)}, bf16[136,1024]{1,0:T(8,128)(2,1)S(1)}, u32[]{:S(2)}, u32[]{:S(2)}) collective-permute-start(bf16[136,1024]{1,0:T(8,128)(2,1)S(1)} %get-tuple-element.46), channel_id=1, source_target_pairs={{0,32},{32,64},{64,96},{96,128},{128,160},{160,192},{192,224},{224... | collective-permute-start | bytes 835592 | tf_op jit(solution)/shard_map/ppermute | solution.py:576
  131.8 7.6 %collective-permute-start.12 = (bf16[136,1024]{1,0:T(8,128)(2,1)S(1)}, bf16[136,1024]{1,0:T(8,128)(2,1)S(1)}, u32[]{:S(2)}, u32[]{:S(2)}) collective-permute-start(bf16[136,1024]{1,0:T(8,128)(2,1)S(1)} %get-tuple-element.47), channel_id=1, source_target_pairs={{0,224},{32,0},{64,32},{96,64},{128,96},{160,128},{192,160},{224,1... | collective-permute-start | bytes 835592 | tf_op jit(solution)/shard_map/ppermute | solution.py:576
  139.6 6.6 %collective-permute-start.14 = (bf16[136,1024]{1,0:T(8,128)(2,1)S(1)}, bf16[136,1024]{1,0:T(8,128)(2,1)S(1)}, u32[]{:S(2)}, u32[]{:S(2)}) collective-permute-start(bf16[136,1024]{1,0:T(8,128)(2,1)S(1)} %get-tuple-element.50), channel_id=1, source_target_pairs={{0,224},{32,0},{64,32},{96,64},{128,96},{160,128},{192,160},{224,1... | collective-permute-start | bytes 835592 | tf_op jit(solution)/shard_map/ppermute | solution.py:576
  142.1 7.7 %collective-permute-start.13 = (bf16[136,1024]{1,0:T(8,128)(2,1)S(1)}, bf16[136,1024]{1,0:T(8,128)(2,1)S(1)}, u32[]{:S(2)}, u32[]{:S(2)}) collective-permute-start(bf16[136,1024]{1,0:T(8,128)(2,1)S(1)} %get-tuple-element.48), channel_id=1, source_target_pairs={{0,32},{32,64},{64,96},{96,128},{128,160},{160,192},{192,224},{224... | collective-permute-start | bytes 835592 | tf_op jit(solution)/shard_map/ppermute | solution.py:576
  146.3 7.0 %collective-permute-start.15 = (bf16[136,1024]{1,0:T(8,128)(2,1)S(1)}, bf16[136,1024]{1,0:T(8,128)(2,1)S(1)}, u32[]{:S(2)}, u32[]{:S(2)}) collective-permute-start(bf16[136,1024]{1,0:T(8,128)(2,1)S(1)} %hop.5), channel_id=1, source_target_pairs={{0,224},{32,0},{64,32},{96,64},{128,96},{160,128},{192,160},{224,1... | collective-permute-start | bytes 835592 | tf_op jit(solution)/shard_map/ppermute | solution.py:576
  176.5 63.8 %all-to-all-start.1 = ((bf16[32,2,256,128]{3,2,1,0:T(8,128)(2,1)}), bf16[32,2,256,128]{3,2,1,0:T(8,128)(2,1)}, u32[]{:S(2)}, u32[]{:S(2)}) async-start(bf16[32,2,256,128]{3,2,1,0:T(8,128)(2,1)} %bitcast.20), calls=%async_computation.1 | async-start | bytes 8388608 | tf_op jit(solution)/shard_map/all_to_all | solution.py:573
  181.4 10.5 %copy-start.3 = (f32[4096]{0:T(1024)S(1)}, f32[4096]{0:T(1024)}, u32[]{:S(2)}) copy-start(f32[4096]{0:T(1024)} %param.11) | copy-start | bytes 49156
  189.2 8.6 %collective-permute-start.16 = (bf16[128,1024]{1,0:T(8,128)(2,1)S(1)}, bf16[128,1024]{1,0:T(8,128)(2,1)S(1)}, u32[]{:S(2)}, u32[]{:S(2)}) collective-permute-start(bf16[128,1024]{1,0:T(8,128)(2,1)S(1)} %last.1), channel_id=1, source_target_pairs={{0,0},{32,1},{64,2},{96,3},{128,4},{160,5},{192,6},{224,7},{33,32}... | collective-permute-start | bytes 786440 | tf_op jit(solution)/shard_map/ppermute | solution.py:601

commit v6 on v5

--- a/solution.py
+++ b/solution.py
@@ -435,26 +435,29 @@
 
 
 def pack_kernel(slab, seqs, parts, *refs):
-    *ins, small_ref = refs
+    *ins, gain_ref, small_ref = refs
     sums = sum(unpack_sums(r[slab:]) for r in ins)
+    group = (lax.axis_index("dp_0") * 2 + lax.axis_index("dp_1")) * parts + lax.axis_index("sp_1")
+    gain = gain_ref[:, pl.ds(pl.multiple_of(group * LANES, LANES), LANES)]
+    gain_sum = sums[:, :LANES] / gain
     small_ref[...] = jnp.zeros_like(small_ref)
     for a in range(seqs):
         at = slice((a + 1) * LANES, (a + 2) * LANES)
         for y in range(parts):
-            small_ref[a * parts + y, :1] = sums[:, :LANES]
+            small_ref[a * parts + y, :1] = gain_sum
             small_ref[a * parts + y, 1:2] = sums[:, at]
 
 
-def pack(pieces, seqs, parts):
+def pack(pieces, gain, seqs, parts):
     slab = pieces[0].shape[0] - PAD
     return pl.pallas_call(
         functools.partial(pack_kernel, slab, seqs, parts),
-        in_specs=[VMEM] * 3,
+        in_specs=[VMEM] * 4,
         out_specs=VMEM,
         out_shape=jax.ShapeDtypeStruct((seqs * parts, 8, LANES), F32),
         compiler_params=limit(8),
         name="pack",
-    )(*pieces)
+    )(*pieces, gain)
 
 
 def epilogue_kernel(
@@ -598,10 +601,11 @@
     (minus,) = hop((m1,), (minus,))
     minus = shifted(minus, -1)
     grads = last((own, plus, minus))
+    small = pack((own, plus, minus), gain, seqs, parts)
+    grads, back = lax.optimization_barrier((grads, back))
     grads = lax.ppermute(grads, Z_DP, home)
-    small = pack((own, plus, minus), seqs, parts)
     small = exchange(small)
-    gain_grad = small[:, 0].reshape(-1) / value_gain
+    gain_grad = small[:, 0].reshape(-1)
     mine = lax.axis_index(Z) * parts + lax.axis_index("sp_1")
     bias_grad = lax.dynamic_slice_in_dim(small, mine, 1, axis=0)[:, 1]
     up_grad, value_grad = epilogue(back, cot, up_slope, val_slope, act, inv, gain)

time: 254 us -> 218 us (0.86)
  the two profiles are of different devices: /device:TPU:1 before, /device:TPU:15 now
where the time goes in v6:
time: 218 us
  starting transfers between devices  105 us (48%)
  waiting for transfers between devices  64.5 us (30%)
  Pallas kernels  42.2 us (19%)
  local copies, waits for them, and re-layouts  4.38 us (2%)
    ppermute x14, starting transfers between devices, shifted(): return lax.ppermute(x, Z, [(z, (z + by) % planes) for z in range(planes)])  56.9 us
    ppermute x14, waiting for transfers between devices, shifted(): return lax.ppermute(x, Z, [(z, (z + by) % planes) for z in range(planes)])  37 us
    all_to_all x3, starting transfers between devices, exchange(): return lax.all_to_all(x, PLANE, split_axis=0, concat_axis=0, tiled=True)  32.9 us
    ppermute x1, waiting for transfers between devices, shards(): weights = lax.ppermute(spatial_weight[0], Z_DP, away)  11.8 us
    pallas_call x1, Pallas kernels, mix(): pl.pallas_call(functools.partial(mix_kernel, seqs, parts, PER), in_specs=...  9.93 us
    pallas_call x1, Pallas kernels, epilogue(): pl.pallas_call(functools.partial(epilogue_kernel, groups, rows), in_specs...  8.45 us
    ppermute x1, waiting for transfers between devices, shards(): grads = lax.ppermute(grads, Z_DP, home)  8.1 us
    pallas_call x1, Pallas kernels, prologue(): pl.pallas_call(functools.partial(prologue_kernel, groups, rows), in_specs...  7.82 us
  transfers between devices with their start and end apart: 20, of which 15 were waited for; matrix products, arithmetic and copies ran while one was open for 1% of the time, Pallas kernels for 11%

profile of v6, /device:TPU:15, one launch (start us, length us, event | category | flops | bytes accessed | tf_op | source)
XLA Modules:
  0.0 217.5 jit_solution(3057388681431574888)
XLA Ops:
  0.6 7.8 %prologue.1 = (bf16[32,2,256,128]{3,2,1,0:T(8,128)(2,1)}, f32[256,128]{1,0:T(8,128)}) custom-call(bf16[256,4096]{1,0:T(8,128)(2,1)} %bitcast.17, bf16[256,4096]{1,0:T(8,128)(2,1)} %bitcast.19, bf16[256,4096]{1,0:T(8,128)(2,1)} %bitcast.21, f32[1,4096]{1,0:T(1,128)} %bitcast.14), custom_call_target="tpu_custom_call" | custom-call | flops 104857600 | bytes 10485760 | tf_op jit(solution)/shard_map/prologue/pallas_call | solution.py:114
  8.5 8.0 %all-to-all-start = ((bf16[32,2,256,128]{3,2,1,0:T(8,128)(2,1)}), bf16[32,2,256,128]{3,2,1,0:T(8,128)(2,1)}, u32[]{:S(2)}, u32[]{:S(2)}) async-start(bf16[32,2,256,128]{3,2,1,0:T(8,128)(2,1)} %get-tuple-element.30), calls=%async_computation | async-start | bytes 8388608 | tf_op jit(solution)/shard_map/all_to_all | solution.py:576
  16.5 7.7 %collective-permute-start = (bf16[128,1024]{1,0:T(8,128)(2,1)S(1)}, bf16[128,1024]{1,0:T(8,128)(2,1)S(1)}, u32[]{:S(2)}, u32[]{:S(2)}) collective-permute-start(bf16[128,1024]{1,0:T(8,128)(2,1)S(1)} %bitcast.27), channel_id=1, source_target_pairs={{0,0},{1,32},{2,64},{3,96},{4,128},{5,160},{6,192},{7,224},{32,33}... | collective-permute-start | bytes 786440 | tf_op jit(solution)/shard_map/ppermute | solution.py:581
  24.2 11.8 %collective-permute-done.refs_0_ = bf16[128,1024]{1,0:T(8,128)(2,1)S(1)} collective-permute-done((bf16[128,1024]{1,0:T(8,128)(2,1)S(1)}, bf16[128,1024]{1,0:T(8,128)(2,1)S(1)}, u32[]{:S(2)}, u32[]{:S(2)}) %collective-permute-start) | collective-permute-done | bytes 262176 | tf_op jit(solution)/shard_map/ppermute | solution.py:581
  36.0 34.5 %collective-permute-start.4 = (bf16[128,1024]{1,0:T(8,128)(2,1)S(1)}, bf16[128,1024]{1,0:T(8,128)(2,1)S(1)}, u32[]{:S(2)}, u32[]{:S(2)}) collective-permute-start(bf16[128,1024]{1,0:T(8,128)(2,1)S(1)} %collective-permute-done.refs_0_), channel_id=1, source_target_pairs={{0,224},{32,0},{64,32},{96,64},{128,96},{160,128},{192,160},{224,1... | collective-permute-start | bytes 786440 | tf_op jit(solution)/shard_map/ppermute | solution.py:579
  70.5 3.3 %collective-permute-done.4.refs_4_ = bf16[128,1024]{1,0:T(8,128)(2,1)S(1)} collective-permute-done((bf16[128,1024]{1,0:T(8,128)(2,1)S(1)}, bf16[128,1024]{1,0:T(8,128)(2,1)S(1)}, u32[]{:S(2)}, u32[]{:S(2)}) %collective-permute-start.4) | collective-permute-done | bytes 262176 | tf_op jit(solution)/shard_map/ppermute | solution.py:579
  73.8 3.1 %collective-permute-start.5 = (bf16[128,1024]{1,0:T(8,128)(2,1)S(1)}, bf16[128,1024]{1,0:T(8,128)(2,1)S(1)}, u32[]{:S(2)}, u32[]{:S(2)}) collective-permute-start(bf16[128,1024]{1,0:T(8,128)(2,1)S(1)} %collective-permute-done.4.refs_4_), channel_id=1, source_target_pairs={{0,224},{32,0},{64,32},{96,64},{128,96},{160,128},{192,160},{224,1... | collective-permute-start | bytes 786440 | tf_op jit(solution)/shard_map/ppermute | solution.py:579
  76.9 2.4 %collective-permute-done.1.refs_1_ = bf16[128,1024]{1,0:T(8,128)(2,1)S(1)} collective-permute-done((bf16[128,1024]{1,0:T(8,128)(2,1)S(1)}, bf16[128,1024]{1,0:T(8,128)(2,1)S(1)}, u32[]{:S(2)}, u32[]{:S(2)}) %collective-permute-start.1) | collective-permute-done | bytes 262176 | tf_op jit(solution)/shard_map/ppermute | solution.py:579
  79.3 3.2 %collective-permute-done.5.refs_5_ = bf16[128,1024]{1,0:T(8,128)(2,1)S(1)} collective-permute-done((bf16[128,1024]{1,0:T(8,128)(2,1)S(1)}, bf16[128,1024]{1,0:T(8,128)(2,1)S(1)}, u32[]{:S(2)}, u32[]{:S(2)}) %collective-permute-start.5) | collective-permute-done | bytes 262176 | tf_op jit(solution)/shard_map/ppermute | solution.py:579
  82.5 3.4 %collective-permute-start.6 = (bf16[128,1024]{1,0:T(8,128)(2,1)S(1)}, bf16[128,1024]{1,0:T(8,128)(2,1)S(1)}, u32[]{:S(2)}, u32[]{:S(2)}) collective-permute-start(bf16[128,1024]{1,0:T(8,128)(2,1)S(1)} %collective-permute-done.5.refs_5_), channel_id=1, source_target_pairs={{0,224},{32,0},{64,32},{96,64},{128,96},{160,128},{192,160},{224,1... | collective-permute-start | bytes 786440 | tf_op jit(solution)/shard_map/ppermute | solution.py:579
  85.9 2.2 %collective-permute-done.2.refs_2_ = bf16[128,1024]{1,0:T(8,128)(2,1)S(1)} collective-permute-done((bf16[128,1024]{1,0:T(8,128)(2,1)S(1)}, bf16[128,1024]{1,0:T(8,128)(2,1)S(1)}, u32[]{:S(2)}, u32[]{:S(2)}) %collective-permute-start.2) | collective-permute-done | bytes 262176 | tf_op jit(solution)/shard_map/ppermute | solution.py:579
  88.1 2.5 %collective-permute-done.6.refs_6_ = bf16[128,1024]{1,0:T(8,128)(2,1)S(1)} collective-permute-done((bf16[128,1024]{1,0:T(8,128)(2,1)S(1)}, bf16[128,1024]{1,0:T(8,128)(2,1)S(1)}, u32[]{:S(2)}, u32[]{:S(2)}) %collective-permute-start.6) | collective-permute-done | bytes 262176 | tf_op jit(solution)/shard_map/ppermute | solution.py:579
  90.6 3.4 %collective-permute-start.7 = (bf16[128,1024]{1,0:T(8,128)(2,1)S(1)}, bf16[128,1024]{1,0:T(8,128)(2,1)S(1)}, u32[]{:S(2)}, u32[]{:S(2)}) collective-permute-start(bf16[128,1024]{1,0:T(8,128)(2,1)S(1)} %collective-permute-done.6.refs_6_), channel_id=1, source_target_pairs={{0,224},{32,0},{64,32},{96,64},{128,96},{160,128},{192,160},{224,1... | collective-permute-start | bytes 786440 | tf_op jit(solution)/shard_map/ppermute | solution.py:579
  94.0 1.9 collective-permute-start.8
  102.0 9.9 %mix.1 = (bf16[8,4,2,256,128]{4,3,2,1,0:T(8,128)(2,1)}, f32[1,128]{1,0:T(1,128)}) custom-call(bf16[32,2,256,128]{3,2,1,0:T(8,128)(2,1)} %all-to-all-done.recv_hbm.recv_ref, bf16[1024,1024]{1,0:T(8,128)(2,1)} %copy-done.1, bf16[1024,1024]{1,0:T(8,128)(2,1)} %copy-done.2, f32[1,1024]{1,0:T(1,128)} %copy-done.6), custom_call_target="tpu_custom_call" | custom-call | flops 4294967296 | bytes 10485760 | tf_op jit(solution)/shard_map/mix/pallas_call | solution.py:284
  111.9 15.5 %all-to-all-start.1 = ((bf16[32,2,256,128]{3,2,1,0:T(8,128)(2,1)}), bf16[32,2,256,128]{3,2,1,0:T(8,128)(2,1)}, u32[]{:S(2)}, u32[]{:S(2)}) async-start(bf16[32,2,256,128]{3,2,1,0:T(8,128)(2,1)} %bitcast.23), calls=%async_computation.1 | async-start | bytes 8388608 | tf_op jit(solution)/shard_map/all_to_all | solution.py:576
  127.5 6.3 %weight_grads.1 = (bf16[136,1024]{1,0:T(8,128)(2,1)S(1)}, bf16[136,1024]{1,0:T(8,128)(2,1)S(1)}, bf16[136,1024]{1,0:T(8,128)(2,1)S(1)}, bf16[136,1024]{1,0:T(8,1...) custom-call(bf16[32,2,256,128]{3,2,1,0:T(8,128)(2,1)} %all-to-all-do, ...), custom_call_target="tpu_custom_call" | custom-call | flops 2147483648 | bytes 6291456 | tf_op jit(solution)/shard_map/weight_grads/pallas_call | solution.py:375
  133.8 3.5 %collective-permute-start.10 = (bf16[136,1024]{1,0:T(8,128)(2,1)S(1)}, bf16[136,1024]{1,0:T(8,128)(2,1)S(1)}, u32[]{:S(2)}, u32[]{:S(2)}) collective-permute-start(bf16[136,1024]{1,0:T(8,128)(2,1)S(1)} %get-tuple-element.40), channel_id=1, source_target_pairs={{0,224},{32,0},{64,32},{96,64},{128,96},{160,128},{192,160},{224,1... | collective-permute-start | bytes 835592 | tf_op jit(solution)/shard_map/ppermute | solution.py:579
  137.3 5.7 %collective-permute-done.10.refs_3_ = bf16[136,1024]{1,0:T(8,128)(2,1)S(1)} collective-permute-done((bf16[136,1024]{1,0:T(8,128)(2,1)S(1)}, bf16[136,1024]{1,0:T(8,128)(2,1)S(1)}, u32[]{:S(2)}, u32[]{:S(2)}) %collective-permute-start.10) | collective-permute-done | bytes 278560 | tf_op jit(solution)/shard_map/ppermute | solution.py:579
  143.0 3.2 %collective-permute-done.9.refs_2_ = bf16[136,1024]{1,0:T(8,128)(2,1)S(1)} collective-permute-done((bf16[136,1024]{1,0:T(8,128)(2,1)S(1)}, bf16[136,1024]{1,0:T(8,128)(2,1)S(1)}, u32[]{:S(2)}, u32[]{:S(2)}) %collective-permute-start.9) | collective-permute-done | bytes 278560 | tf_op jit(solution)/shard_map/ppermute | solution.py:579
  146.7 2.7 %collective-permute-start.12 = (bf16[136,1024]{1,0:T(8,128)(2,1)S(1)}, bf16[136,1024]{1,0:T(8,128)(2,1)S(1)}, u32[]{:S(2)}, u32[]{:S(2)}) collective-permute-start(bf16[136,1024]{1,0:T(8,128)(2,1)S(1)} %get-tuple-element.42), channel_id=1, source_target_pairs={{0,224},{32,0},{64,32},{96,64},{128,96},{160,128},{192,160},{224,1... | collective-permute-start | bytes 835592 | tf_op jit(solution)/shard_map/ppermute | solution.py:579
  149.3 5.4 %collective-permute-done.11.refs_2_ = bf16[136,1024]{1,0:T(8,128)(2,1)S(1)} collective-permute-done((bf16[136,1024]{1,0:T(8,128)(2,1)S(1)}, bf16[136,1024]{1,0:T(8,128)(2,1)S(1)}, u32[]{:S(2)}, u32[]{:S(2)}) %collective-permute-start.11) | collective-permute-done | bytes 278560 | tf_op jit(solution)/shard_map/ppermute | solution.py:579
  154.9 2.6 %collective-permute-start.14 = (bf16[136,1024]{1,0:T(8,128)(2,1)S(1)}, bf16[136,1024]{1,0:T(8,128)(2,1)S(1)}, u32[]{:S(2)}, u32[]{:S(2)}) collective-permute-start(bf16[136,1024]{1,0:T(8,128)(2,1)S(1)} %get-tuple-element.45), channel_id=1, source_target_pairs={{0,224},{32,0},{64,32},{96,64},{128,96},{160,128},{192,160},{224,1... | collective-permute-start | bytes 835592 | tf_op jit(solution)/shard_map/ppermute | solution.py:579
  157.5 3.6 %collective-permute-done.14.refs_1_ = bf16[136,1024]{1,0:T(8,128)(2,1)S(1)} collective-permute-done((bf16[136,1024]{1,0:T(8,128)(2,1)S(1)}, bf16[136,1024]{1,0:T(8,128)(2,1)S(1)}, u32[]{:S(2)}, u32[]{:S(2)}) %collective-permute-start.14) | collective-permute-done | bytes 278560 | tf_op jit(solution)/shard_map/ppermute | solution.py:579
  161.2 3.5 %collective-permute-start.15 = (bf16[136,1024]{1,0:T(8,128)(2,1)S(1)}, bf16[136,1024]{1,0:T(8,128)(2,1)S(1)}, u32[]{:S(2)}, u32[]{:S(2)}) collective-permute-start(bf16[136,1024]{1,0:T(8,128)(2,1)S(1)} %hop.5), channel_id=1, source_target_pairs={{0,224},{32,0},{64,32},{96,64},{128,96},{160,128},{192,160},{224,1... | collective-permute-start | bytes 835592 | tf_op jit(solution)/shard_map/ppermute | solution.py:579
  164.7 3.5 %collective-permute-done.15.refs_2_ = bf16[136,1024]{1,0:T(8,128)(2,1)S(1)} collective-permute-done((bf16[136,1024]{1,0:T(8,128)(2,1)S(1)}, bf16[136,1024]{1,0:T(8,128)(2,1)S(1)}, u32[]{:S(2)}, u32[]{:S(2)}) %collective-permute-start.15) | collective-permute-done | bytes 278560 | tf_op jit(solution)/shard_map/ppermute | solution.py:579
  168.9 7.6 %all-to-all-done.1.recv_hbm = bf16[32,2,256,128]{3,2,1,0:T(8,128)(2,1)} async-done(((bf16[32,2,256,128]{3,2,1,0:T(8,128)(2,1)}), bf16[32,2,256,128]{3,2,1,0:T(8,128)(2,1)}, u32[]{:S(2)}, u32[]{:S(2)}) %all-to-all-start.1) | async-done | bytes 4194336 | tf_op jit(solution)/shard_map/all_to_all | solution.py:576
  176.4 9.4 %all-to-all-start.2 = ((f32[32,8,128]{2,1,0:T(8,128)}), f32[32,8,128]{2,1,0:T(8,128)S(1)}, u32[]{:S(2)}, u32[]{:S(2)}) async-start(f32[32,8,128]{2,1,0:T(8,128)} %pack.1), calls=%async_computation.2 | async-start | bytes 262144 | tf_op jit(solution)/shard_map/all_to_all | solution.py:576
  185.9 7.7 %slopes.1 = (bf16[256,4096]{1,0:T(8,128)(2,1)}, bf16[256,4096]{1,0:T(8,128)(2,1)}, bf16[256,4096]{1,0:T(8,128)(2,1)}) custom-call(bf16[256,4096]{1,0:T(8,128)(2,1)} %bitcast.20, bf16[256,4096]{1,0:T(8,128)(2,1)} %bitcast.22), custom_call_target="tpu_custom_call" | custom-call | flops 104857600 | bytes 16777216 | tf_op jit(solution)/shard_map/slopes/pallas_call | solution.py:160
  193.6 5.3 %collective-permute-start.16 = (bf16[128,1024]{1,0:T(8,128)(2,1)S(1)}, bf16[128,1024]{1,0:T(8,128)(2,1)S(1)}, u32[]{:S(2)}, u32[]{:S(2)}) collective-permute-start(bf16[128,1024]{1,0:T(8,128)(2,1)S(1)} %last.1), channel_id=1, source_target_pairs={{0,0},{32,1},{64,2},{96,3},{128,4},{160,5},{192,6},{224,7},{33,32}... | collective-permute-start | bytes 786440 | tf_op jit(solution)/shard_map/ppermute | solution.py:606
  200.1 8.4 %epilogue.1 = (bf16[256,4096]{1,0:T(8,128)(2,1)}, bf16[256,4096]{1,0:T(8,128)(2,1)}) custom-call(bf16[32,2,256,128]{3,2,1,0:T(8,128)(2,1)} %all-to-all-done.1.recv_hbm, bf16[256,4096]{1,0:T(8,128)(2,1)} %bitcast.18, bf16[256,4096]{1,0:T(8,128)(2,1)} %get-tuple-element.48.up_slope_hbm, bf16[256,4096]{1,0:T(8,128)(2,1)} %get-tuple-element.49.val_slope_hbm, ...), custom_call_target="tpu_custom_call" | custom-call | flops 20971520 | bytes 23068672 | tf_op jit(solution)/shard_map/epilogue/pallas_call | solution.py:540
  208.6 8.1 %collective-permute-done.16 = bf16[128,1024]{1,0:T(8,128)(2,1)S(1)} collective-permute-done((bf16[128,1024]{1,0:T(8,128)(2,1)S(1)}, bf16[128,1024]{1,0:T(8,128)(2,1)S(1)}, u32[]{:S(2)}, u32[]{:S(2)}) %collective-permute-start.16) | collective-permute-done | bytes 262176 | tf_op jit(solution)/shard_map/ppermute | solution.py:606
  (37 shorter events, 9.6 us)
Async XLA Ops:
  8.5 8.0 %copy-start.4 = (bf16[1,128,1024]{2,1,0:T(8,128)(2,1)S(1)}, bf16[1,128,1024]{2,1,0:T(8,128)(2,1)}, u32[]{:S(2)}) copy-start(bf16[1,128,1024]{2,1,0:T(8,128)(2,1)} %param.9) | copy-start | bytes 786436
  8.5 85.6 %copy-start.5 = (f32[1,1024]{1,0:T(1,128)S(1)}, f32[1,1024]{1,0:T(1,128)}, u32[]{:S(2)}) copy-start(f32[1,1024]{1,0:T(1,128)} %param.10) | copy-start | bytes 12292
  8.5 92.9 %all-to-all-start = ((bf16[32,2,256,128]{3,2,1,0:T(8,128)(2,1)}), bf16[32,2,256,128]{3,2,1,0:T(8,128)(2,1)}, u32[]{:S(2)}, u32[]{:S(2)}) async-start(bf16[32,2,256,128]{3,2,1,0:T(8,128)(2,1)} %get-tuple-element.30), calls=%async_computation | async-start | bytes 8388608 | tf_op jit(solution)/shard_map/all_to_all | solution.py:576
  16.5 19.5 %collective-permute-start = (bf16[128,1024]{1,0:T(8,128)(2,1)S(1)}, bf16[128,1024]{1,0:T(8,128)(2,1)S(1)}, u32[]{:S(2)}, u32[]{:S(2)}) collective-permute-start(bf16[128,1024]{1,0:T(8,128)(2,1)S(1)} %bitcast.27), channel_id=1, source_target_pairs={{0,0},{1,32},{2,64},{3,96},{4,128},{5,160},{6,192},{7,224},{32,33}... | collective-permute-start | bytes 786440 | tf_op jit(solution)/shard_map/ppermute | solution.py:581
  36.0 37.8 %collective-permute-start.4 = (bf16[128,1024]{1,0:T(8,128)(2,1)S(1)}, bf16[128,1024]{1,0:T(8,128)(2,1)S(1)}, u32[]{:S(2)}, u32[]{:S(2)}) collective-permute-start(bf16[128,1024]{1,0:T(8,128)(2,1)S(1)} %collective-permute-done.refs_0_), channel_id=1, source_target_pairs={{0,224},{32,0},{64,32},{96,64},{128,96},{160,128},{192,160},{224,1... | collective-permute-start | bytes 786440 | tf_op jit(solution)/shard_map/ppermute | solution.py:579
  70.5 8.8 %collective-permute-start.1 = (bf16[128,1024]{1,0:T(8,128)(2,1)S(1)}, bf16[128,1024]{1,0:T(8,128)(2,1)S(1)}, u32[]{:S(2)}, u32[]{:S(2)}) collective-permute-start(bf16[128,1024]{1,0:T(8,128)(2,1)S(1)} %collective-permute-done.refs_0_), channel_id=1, source_target_pairs={{0,32},{32,64},{64,96},{96,128},{128,160},{160,192},{192,224},{224... | collective-permute-start | bytes 786440 | tf_op jit(solution)/shard_map/ppermute | solution.py:579
  73.8 8.7 %collective-permute-start.5 = (bf16[128,1024]{1,0:T(8,128)(2,1)S(1)}, bf16[128,1024]{1,0:T(8,128)(2,1)S(1)}, u32[]{:S(2)}, u32[]{:S(2)}) collective-permute-start(bf16[128,1024]{1,0:T(8,128)(2,1)S(1)} %collective-permute-done.4.refs_4_), channel_id=1, source_target_pairs={{0,224},{32,0},{64,32},{96,64},{128,96},{160,128},{192,160},{224,1... | collective-permute-start | bytes 786440 | tf_op jit(solution)/shard_map/ppermute | solution.py:579
  79.3 8.8 %collective-permute-start.2 = (bf16[128,1024]{1,0:T(8,128)(2,1)S(1)}, bf16[128,1024]{1,0:T(8,128)(2,1)S(1)}, u32[]{:S(2)}, u32[]{:S(2)}) collective-permute-start(bf16[128,1024]{1,0:T(8,128)(2,1)S(1)} %collective-permute-done.1.refs_1_), channel_id=1, source_target_pairs={{0,32},{32,64},{64,96},{96,128},{128,160},{160,192},{192,224},{224... | collective-permute-start | bytes 786440 | tf_op jit(solution)/shard_map/ppermute | solution.py:579
  82.5 8.1 %collective-permute-start.6 = (bf16[128,1024]{1,0:T(8,128)(2,1)S(1)}, bf16[128,1024]{1,0:T(8,128)(2,1)S(1)}, u32[]{:S(2)}, u32[]{:S(2)}) collective-permute-start(bf16[128,1024]{1,0:T(8,128)(2,1)S(1)} %collective-permute-done.5.refs_5_), channel_id=1, source_target_pairs={{0,224},{32,0},{64,32},{96,64},{128,96},{160,128},{192,160},{224,1... | collective-permute-start | bytes 786440 | tf_op jit(solution)/shard_map/ppermute | solution.py:579
  88.1 8.0 %collective-permute-start.3 = (bf16[128,1024]{1,0:T(8,128)(2,1)S(1)}, bf16[128,1024]{1,0:T(8,128)(2,1)S(1)}, u32[]{:S(2)}, u32[]{:S(2)}) collective-permute-start(bf16[128,1024]{1,0:T(8,128)(2,1)S(1)} %collective-permute-done.2.refs_2_), channel_id=1, source_target_pairs={{0,32},{32,64},{64,96},{96,128},{128,160},{160,192},{192,224},{224... | collective-permute-start | bytes 786440 | tf_op jit(solution)/shard_map/ppermute | solution.py:579
  90.6 7.4 %collective-permute-start.7 = (bf16[128,1024]{1,0:T(8,128)(2,1)S(1)}, bf16[128,1024]{1,0:T(8,128)(2,1)S(1)}, u32[]{:S(2)}, u32[]{:S(2)}) collective-permute-start(bf16[128,1024]{1,0:T(8,128)(2,1)S(1)} %collective-permute-done.6.refs_6_), channel_id=1, source_target_pairs={{0,224},{32,0},{64,32},{96,64},{128,96},{160,128},{192,160},{224,1... | collective-permute-start | bytes 786440 | tf_op jit(solution)/shard_map/ppermute | solution.py:579
  94.0 7.4 %collective-permute-start.8 = (f32[1,1024]{1,0:T(1,128)S(1)}, f32[1,1024]{1,0:T(1,128)S(1)}, u32[]{:S(2)}, u32[]{:S(2)}) collective-permute-start(f32[1,1024]{1,0:T(1,128)S(1)} %copy-done.5), channel_id=1, source_target_pairs={{0,0},{1,32},{2,64},{3,96},{4,128},{5,160},{6,192},{7,224},{32,33}... | collective-permute-start | bytes 12296 | tf_op jit(solution)/shard_map/ppermute | solution.py:582
  98.8 1.3 copy-start.1
  100.1 1.3 copy-start.2
  101.4 0.6 copy-start.6
  111.9 15.5 %copy-start.3 = (f32[1,128]{1,0:T(1,128)S(1)}, f32[1,128]{1,0:T(1,128)}, u32[]{:S(2)}) copy-start(f32[1,128]{1,0:T(1,128)} %get-tuple-element.33.sums_ref) | copy-start | bytes 1540
  111.9 64.5 %all-to-all-start.1 = ((bf16[32,2,256,128]{3,2,1,0:T(8,128)(2,1)}), bf16[32,2,256,128]{3,2,1,0:T(8,128)(2,1)}, u32[]{:S(2)}, u32[]{:S(2)}) async-start(bf16[32,2,256,128]{3,2,1,0:T(8,128)(2,1)} %bitcast.23), calls=%async_computation.1 | async-start | bytes 8388608 | tf_op jit(solution)/shard_map/all_to_all | solution.py:576
  133.8 34.4 %copy-start = (f32[4096]{0:T(1024)S(1)}, f32[4096]{0:T(1024)}, u32[]{:S(2)}) copy-start(f32[4096]{0:T(1024)} %param.11) | copy-start | bytes 49156
  133.8 9.2 %collective-permute-start.10 = (bf16[136,1024]{1,0:T(8,128)(2,1)S(1)}, bf16[136,1024]{1,0:T(8,128)(2,1)S(1)}, u32[]{:S(2)}, u32[]{:S(2)}) collective-permute-start(bf16[136,1024]{1,0:T(8,128)(2,1)S(1)} %get-tuple-element.40), channel_id=1, source_target_pairs={{0,224},{32,0},{64,32},{96,64},{128,96},{160,128},{192,160},{224,1... | collective-permute-start | bytes 835592 | tf_op jit(solution)/shard_map/ppermute | solution.py:579
  137.3 8.9 %collective-permute-start.9 = (bf16[136,1024]{1,0:T(8,128)(2,1)S(1)}, bf16[136,1024]{1,0:T(8,128)(2,1)S(1)}, u32[]{:S(2)}, u32[]{:S(2)}) collective-permute-start(bf16[136,1024]{1,0:T(8,128)(2,1)S(1)} %get-tuple-element.39), channel_id=1, source_target_pairs={{0,32},{32,64},{64,96},{96,128},{128,160},{160,192},{192,224},{224... | collective-permute-start | bytes 835592 | tf_op jit(solution)/shard_map/ppermute | solution.py:579
  146.4 8.3 %collective-permute-start.11 = (bf16[136,1024]{1,0:T(8,128)(2,1)S(1)}, bf16[136,1024]{1,0:T(8,128)(2,1)S(1)}, u32[]{:S(2)}, u32[]{:S(2)}) collective-permute-start(bf16[136,1024]{1,0:T(8,128)(2,1)S(1)} %get-tuple-element.41), channel_id=1, source_target_pairs={{0,32},{32,64},{64,96},{96,128},{128,160},{160,192},{192,224},{224... | collective-permute-start | bytes 835592 | tf_op jit(solution)/shard_map/ppermute | solution.py:579
  146.7 8.0 %collective-permute-start.12 = (bf16[136,1024]{1,0:T(8,128)(2,1)S(1)}, bf16[136,1024]{1,0:T(8,128)(2,1)S(1)}, u32[]{:S(2)}, u32[]{:S(2)}) collective-permute-start(bf16[136,1024]{1,0:T(8,128)(2,1)S(1)} %get-tuple-element.42), channel_id=1, source_target_pairs={{0,224},{32,0},{64,32},{96,64},{128,96},{160,128},{192,160},{224,1... | collective-permute-start | bytes 835592 | tf_op jit(solution)/shard_map/ppermute | solution.py:579
  154.9 6.2 %collective-permute-start.14 = (bf16[136,1024]{1,0:T(8,128)(2,1)S(1)}, bf16[136,1024]{1,0:T(8,128)(2,1)S(1)}, u32[]{:S(2)}, u32[]{:S(2)}) collective-permute-start(bf16[136,1024]{1,0:T(8,128)(2,1)S(1)} %get-tuple-element.45), channel_id=1, source_target_pairs={{0,224},{32,0},{64,32},{96,64},{128,96},{160,128},{192,160},{224,1... | collective-permute-start | bytes 835592 | tf_op jit(solution)/shard_map/ppermute | solution.py:579
  157.5 7.2 %collective-permute-start.13 = (bf16[136,1024]{1,0:T(8,128)(2,1)S(1)}, bf16[136,1024]{1,0:T(8,128)(2,1)S(1)}, u32[]{:S(2)}, u32[]{:S(2)}) collective-permute-start(bf16[136,1024]{1,0:T(8,128)(2,1)S(1)} %get-tuple-element.43), channel_id=1, source_target_pairs={{0,32},{32,64},{64,96},{96,128},{128,160},{160,192},{192,224},{224... | collective-permute-start | bytes 835592 | tf_op jit(solution)/shard_map/ppermute | solution.py:579
  161.2 7.0 %collective-permute-start.15 = (bf16[136,1024]{1,0:T(8,128)(2,1)S(1)}, bf16[136,1024]{1,0:T(8,128)(2,1)S(1)}, u32[]{:S(2)}, u32[]{:S(2)}) collective-permute-start(bf16[136,1024]{1,0:T(8,128)(2,1)S(1)} %hop.5), channel_id=1, source_target_pairs={{0,224},{32,0},{64,32},{96,64},{128,96},{160,128},{192,160},{224,1... | collective-permute-start | bytes 835592 | tf_op jit(solution)/shard_map/ppermute | solution.py:579
  176.4 22.5 %all-to-all-start.2 = ((f32[32,8,128]{2,1,0:T(8,128)}), f32[32,8,128]{2,1,0:T(8,128)S(1)}, u32[]{:S(2)}, u32[]{:S(2)}) async-start(f32[32,8,128]{2,1,0:T(8,128)} %pack.1), calls=%async_computation.2 | async-start | bytes 262144 | tf_op jit(solution)/shard_map/all_to_all | solution.py:576
  193.6 23.0 %collective-permute-start.16 = (bf16[128,1024]{1,0:T(8,128)(2,1)S(1)}, bf16[128,1024]{1,0:T(8,128)(2,1)S(1)}, u32[]{:S(2)}, u32[]{:S(2)}) collective-permute-start(bf16[128,1024]{1,0:T(8,128)(2,1)S(1)} %last.1), channel_id=1, source_target_pairs={{0,0},{32,1},{64,2},{96,3},{128,4},{160,5},{192,6},{224,7},{33,32}... | collective-permute-start | bytes 786440 | tf_op jit(solution)/shard_map/ppermute | solution.py:606

commit v7 on v6

--- a/solution.py
+++ b/solution.py
@@ -12,7 +12,7 @@
 Z = "sp_0"
 SP = ("sp_0", "sp_1")
 DP = ("dp_0", "dp_1")
-PLANE = ("dp_0", "dp_1", "sp_1")
+PLANE = ("dp_1", "dp_0", "sp_1")
 Z_DP = ("sp_0", "dp_0", "dp_1")
 
 norm_floor = 0.5
@@ -171,9 +171,16 @@
     )(up, val)
 
 
+def column():
+    return lax.axis_index("dp_1") * 4 + lax.axis_index("dp_0")
+
+
+def place(column):
+    return column % 4 * 2 + column // 4
+
+
 def slab_of(z_offset):
-    z = (lax.axis_index(Z) + z_offset + 8) % 8
-    return z ^ (lax.axis_index("dp_0") * 2 + lax.axis_index("dp_1"))
+    return ((lax.axis_index(Z) + z_offset + 8) % 8) ^ column()
 
 
 OFFSETS = (0, -1, -2, -3, 1, 2, 3, 4)
@@ -437,12 +444,12 @@
 def pack_kernel(slab, seqs, parts, *refs):
     *ins, gain_ref, small_ref = refs
     sums = sum(unpack_sums(r[slab:]) for r in ins)
-    group = (lax.axis_index("dp_0") * 2 + lax.axis_index("dp_1")) * parts + lax.axis_index("sp_1")
+    group = column() * parts + lax.axis_index("sp_1")
     gain = gain_ref[:, pl.ds(pl.multiple_of(group * LANES, LANES), LANES)]
     gain_sum = sums[:, :LANES] / gain
     small_ref[...] = jnp.zeros_like(small_ref)
     for a in range(seqs):
-        at = slice((a + 1) * LANES, (a + 2) * LANES)
+        at = slice((place(a) + 1) * LANES, (place(a) + 2) * LANES)
         for y in range(parts):
             small_ref[a * parts + y, :1] = gain_sum
             small_ref[a * parts + y, 1:2] = sums[:, at]
@@ -569,7 +576,7 @@
     parts = lax.axis_size("sp_1")
     cot, up, val = cotangent[0], up_pre[0], value_pre[0]
     gain = value_gain[None]
-    away = [(z * seqs + a, (z ^ a) * seqs + z) for z in range(planes) for a in range(seqs)]
+    away = [(z * seqs + a, (z ^ a) * seqs + place(z)) for z in range(planes) for a in range(seqs)]
     home = [(there, here) for here, there in away]
 
     def exchange(x):
@@ -578,9 +585,10 @@
     def shifted(x, by):
         return lax.ppermute(x, Z, [(z, (z + by) % planes) for z in range(planes)])
 
-    weights = lax.ppermute(spatial_weight[0], Z_DP, away)
     bias = lax.ppermute(spatial_bias, Z_DP, away)
     sent, inv = prologue(cot, up, val, gain)
+    weights, sent = lax.optimization_barrier((spatial_weight[0], sent))
+    weights = lax.ppermute(weights, Z_DP, away)
     recv = exchange(sent)
     before, after = [weights], [weights]
     for _ in range(3):

time: 218 us -> 218 us (level)
  the two profiles are of different devices: /device:TPU:15 before, /device:TPU:1 now
where the time goes in v7:
time: 218 us; the launch traced here: 217 us
  starting transfers between devices  106 us (49%)
  waiting for transfers between devices  62.3 us (29%)
  Pallas kernels  42.2 us (19%)
  local copies, waits for them, and re-layouts  4.38 us (2%)
    ppermute x1, starting transfers between devices, shards(): bias = lax.ppermute(spatial_bias, Z_DP, away)  42.6 us
    ppermute x14, waiting for transfers between devices, shifted(): return lax.ppermute(x, Z, [(z, (z + by) % planes) for z in range(planes)])  34.2 us
    all_to_all x3, starting transfers between devices, exchange(): return lax.all_to_all(x, PLANE, split_axis=0, concat_axis=0, tiled=True)  26.4 us
    ppermute x14, starting transfers between devices, shifted(): return lax.ppermute(x, Z, [(z, (z + by) % planes) for z in range(planes)])  24.4 us
    all_to_all x3, waiting for transfers between devices, exchange(): return lax.all_to_all(x, PLANE, split_axis=0, concat_axis=0, tiled=True)  15.7 us
    ppermute x1, waiting for transfers between devices, shards(): weights = lax.ppermute(weights, Z_DP, away)  12.4 us
    pallas_call x1, Pallas kernels, mix(): pl.pallas_call(functools.partial(mix_kernel, seqs, parts, PER), in_specs=...  9.93 us
    ppermute x1, starting transfers between devices, shards(): grads = lax.ppermute(grads, Z_DP, home)  9.35 us
  transfers between devices with their start and end apart: 20, of which 10 were waited for; matrix products, arithmetic and copies ran while one was open for 1% of the time, Pallas kernels for 11%

profile of v7, /device:TPU:1, one launch (start us, length us, event | category | flops | bytes accessed | tf_op | source)
XLA Modules:
  0.0 217.0 jit_solution(11781048862437447429)
XLA Ops:
  0.6 7.8 %prologue.1 = (bf16[32,2,256,128]{3,2,1,0:T(8,128)(2,1)}, f32[256,128]{1,0:T(8,128)}) custom-call(bf16[256,4096]{1,0:T(8,128)(2,1)} %bitcast.17, bf16[256,4096]{1,0:T(8,128)(2,1)} %bitcast.19, bf16[256,4096]{1,0:T(8,128)(2,1)} %bitcast.21, f32[1,4096]{1,0:T(1,128)} %bitcast.14), custom_call_target="tpu_custom_call" | custom-call | flops 104857600 | bytes 10485760 | tf_op jit(solution)/shard_map/prologue/pallas_call | solution.py:114
  8.5 8.8 %all-to-all-start = ((bf16[32,2,256,128]{3,2,1,0:T(8,128)(2,1)}), bf16[32,2,256,128]{3,2,1,0:T(8,128)(2,1)}, u32[]{:S(2)}, u32[]{:S(2)}) async-start(bf16[32,2,256,128]{3,2,1,0:T(8,128)(2,1)} %get-tuple-element.33), calls=%async_computation | async-start | bytes 8388608 | tf_op jit(solution)/shard_map/all_to_all | solution.py:583
  17.3 3.7 %collective-permute-start = (bf16[128,1024]{1,0:T(8,128)(2,1)S(1)}, bf16[128,1024]{1,0:T(8,128)(2,1)S(1)}, u32[]{:S(2)}, u32[]{:S(2)}) collective-permute-start(bf16[128,1024]{1,0:T(8,128)(2,1)S(1)} %bitcast.27), channel_id=1, source_target_pairs={{0,0},{1,32},{2,64},{3,96},{4,128},{5,160},{6,192},{7,224},{32,34}... | collective-permute-start | bytes 786440 | tf_op jit(solution)/shard_map/ppermute | solution.py:591
  21.0 12.4 %collective-permute-done.refs_0_ = bf16[128,1024]{1,0:T(8,128)(2,1)S(1)} collective-permute-done((bf16[128,1024]{1,0:T(8,128)(2,1)S(1)}, bf16[128,1024]{1,0:T(8,128)(2,1)S(1)}, u32[]{:S(2)}, u32[]{:S(2)}) %collective-permute-start) | collective-permute-done | bytes 262176 | tf_op jit(solution)/shard_map/ppermute | solution.py:591
  33.4 2.3 %collective-permute-start.4 = (bf16[128,1024]{1,0:T(8,128)(2,1)S(1)}, bf16[128,1024]{1,0:T(8,128)(2,1)S(1)}, u32[]{:S(2)}, u32[]{:S(2)}) collective-permute-start(bf16[128,1024]{1,0:T(8,128)(2,1)S(1)} %collective-permute-done.refs_0_), channel_id=1, source_target_pairs={{0,224},{32,0},{64,32},{96,64},{128,96},{160,128},{192,160},{224,1... | collective-permute-start | bytes 786440 | tf_op jit(solution)/shard_map/ppermute | solution.py:586
  35.7 5.6 %collective-permute-start.1 = (bf16[128,1024]{1,0:T(8,128)(2,1)S(1)}, bf16[128,1024]{1,0:T(8,128)(2,1)S(1)}, u32[]{:S(2)}, u32[]{:S(2)}) collective-permute-start(bf16[128,1024]{1,0:T(8,128)(2,1)S(1)} %collective-permute-done.refs_0_), channel_id=1, source_target_pairs={{0,32},{32,64},{64,96},{96,128},{128,160},{160,192},{192,224},{224... | collective-permute-start | bytes 786440 | tf_op jit(solution)/shard_map/ppermute | solution.py:586
  41.3 4.2 %collective-permute-done.4.refs_4_ = bf16[128,1024]{1,0:T(8,128)(2,1)S(1)} collective-permute-done((bf16[128,1024]{1,0:T(8,128)(2,1)S(1)}, bf16[128,1024]{1,0:T(8,128)(2,1)S(1)}, u32[]{:S(2)}, u32[]{:S(2)}) %collective-permute-start.4) | collective-permute-done | bytes 262176 | tf_op jit(solution)/shard_map/ppermute | solution.py:586
  45.4 1.5 collective-permute-start.2
  46.9 4.2 %collective-permute-done.5.refs_5_ = bf16[128,1024]{1,0:T(8,128)(2,1)S(1)} collective-permute-done((bf16[128,1024]{1,0:T(8,128)(2,1)S(1)}, bf16[128,1024]{1,0:T(8,128)(2,1)S(1)}, u32[]{:S(2)}, u32[]{:S(2)}) %collective-permute-start.5) | collective-permute-done | bytes 262176 | tf_op jit(solution)/shard_map/ppermute | solution.py:586
  51.1 1.2 collective-permute-start.6
  52.5 4.2 %collective-permute-done.6.refs_6_ = bf16[128,1024]{1,0:T(8,128)(2,1)S(1)} collective-permute-done((bf16[128,1024]{1,0:T(8,128)(2,1)S(1)}, bf16[128,1024]{1,0:T(8,128)(2,1)S(1)}, u32[]{:S(2)}, u32[]{:S(2)}) %collective-permute-start.6) | collective-permute-done | bytes 262176 | tf_op jit(solution)/shard_map/ppermute | solution.py:586
  56.7 2.4 %collective-permute-start.7 = (bf16[128,1024]{1,0:T(8,128)(2,1)S(1)}, bf16[128,1024]{1,0:T(8,128)(2,1)S(1)}, u32[]{:S(2)}, u32[]{:S(2)}) collective-permute-start(bf16[128,1024]{1,0:T(8,128)(2,1)S(1)} %collective-permute-done.6.refs_6_), channel_id=1, source_target_pairs={{0,224},{32,0},{64,32},{96,64},{128,96},{160,128},{192,160},{224,1... | collective-permute-start | bytes 786440 | tf_op jit(solution)/shard_map/ppermute | solution.py:586
  59.1 42.6 %collective-permute-start.8 = (f32[1,1024]{1,0:T(1,128)S(1)}, f32[1,1024]{1,0:T(1,128)S(1)}, u32[]{:S(2)}, u32[]{:S(2)}) collective-permute-start(f32[1,1024]{1,0:T(1,128)S(1)} %copy-done.5), channel_id=1, source_target_pairs={{0,0},{1,32},{2,64},{3,96},{4,128},{5,160},{6,192},{7,224},{32,34}... | collective-permute-start | bytes 12296 | tf_op jit(solution)/shard_map/ppermute | solution.py:588
  102.5 1.3 copy-done.1
  103.8 1.3 copy-done.2
  105.7 9.9 %mix.1 = (bf16[8,4,2,256,128]{4,3,2,1,0:T(8,128)(2,1)}, f32[1,128]{1,0:T(1,128)}) custom-call(bf16[32,2,256,128]{3,2,1,0:T(8,128)(2,1)} %all-to-all-done.recv_hbm.recv_ref, bf16[1024,1024]{1,0:T(8,128)(2,1)} %copy-done.1, bf16[1024,1024]{1,0:T(8,128)(2,1)} %copy-done.2, f32[1,1024]{1,0:T(1,128)} %copy-done.6), custom_call_target="tpu_custom_call" | custom-call | flops 4294967296 | bytes 10485760 | tf_op jit(solution)/shard_map/mix/pallas_call | solution.py:291
  115.7 9.4 %all-to-all-start.1 = ((bf16[32,2,256,128]{3,2,1,0:T(8,128)(2,1)}), bf16[32,2,256,128]{3,2,1,0:T(8,128)(2,1)}, u32[]{:S(2)}, u32[]{:S(2)}) async-start(bf16[32,2,256,128]{3,2,1,0:T(8,128)(2,1)} %bitcast.23), calls=%async_computation.1 | async-start | bytes 8388608 | tf_op jit(solution)/shard_map/all_to_all | solution.py:583
  125.1 6.3 %weight_grads.1 = (bf16[136,1024]{1,0:T(8,128)(2,1)S(1)}, bf16[136,1024]{1,0:T(8,128)(2,1)S(1)}, bf16[136,1024]{1,0:T(8,128)(2,1)S(1)}, bf16[136,1024]{1,0:T(8,1...) custom-call(bf16[32,2,256,128]{3,2,1,0:T(8,128)(2,1)} %all-to-all-do, ...), custom_call_target="tpu_custom_call" | custom-call | flops 2147483648 | bytes 6291456 | tf_op jit(solution)/shard_map/weight_grads/pallas_call | solution.py:382
  131.4 2.3 %collective-permute-start.10 = (bf16[136,1024]{1,0:T(8,128)(2,1)S(1)}, bf16[136,1024]{1,0:T(8,128)(2,1)S(1)}, u32[]{:S(2)}, u32[]{:S(2)}) collective-permute-start(bf16[136,1024]{1,0:T(8,128)(2,1)S(1)} %get-tuple-element.44), channel_id=1, source_target_pairs={{0,224},{32,0},{64,32},{96,64},{128,96},{160,128},{192,160},{224,1... | collective-permute-start | bytes 835592 | tf_op jit(solution)/shard_map/ppermute | solution.py:586
  133.7 5.9 %collective-permute-done.10.refs_3_ = bf16[136,1024]{1,0:T(8,128)(2,1)S(1)} collective-permute-done((bf16[136,1024]{1,0:T(8,128)(2,1)S(1)}, bf16[136,1024]{1,0:T(8,128)(2,1)S(1)}, u32[]{:S(2)}, u32[]{:S(2)}) %collective-permute-start.10) | collective-permute-done | bytes 278560 | tf_op jit(solution)/shard_map/ppermute | solution.py:586
  139.6 3.0 %collective-permute-done.9.refs_2_ = bf16[136,1024]{1,0:T(8,128)(2,1)S(1)} collective-permute-done((bf16[136,1024]{1,0:T(8,128)(2,1)S(1)}, bf16[136,1024]{1,0:T(8,128)(2,1)S(1)}, u32[]{:S(2)}, u32[]{:S(2)}) %collective-permute-start.9) | collective-permute-done | bytes 278560 | tf_op jit(solution)/shard_map/ppermute | solution.py:586
  143.1 2.7 %collective-permute-start.12 = (bf16[136,1024]{1,0:T(8,128)(2,1)S(1)}, bf16[136,1024]{1,0:T(8,128)(2,1)S(1)}, u32[]{:S(2)}, u32[]{:S(2)}) collective-permute-start(bf16[136,1024]{1,0:T(8,128)(2,1)S(1)} %get-tuple-element.46), channel_id=1, source_target_pairs={{0,224},{32,0},{64,32},{96,64},{128,96},{160,128},{192,160},{224,1... | collective-permute-start | bytes 835592 | tf_op jit(solution)/shard_map/ppermute | solution.py:586
  145.8 5.5 %collective-permute-done.11.refs_2_ = bf16[136,1024]{1,0:T(8,128)(2,1)S(1)} collective-permute-done((bf16[136,1024]{1,0:T(8,128)(2,1)S(1)}, bf16[136,1024]{1,0:T(8,128)(2,1)S(1)}, u32[]{:S(2)}, u32[]{:S(2)}) %collective-permute-start.11) | collective-permute-done | bytes 278560 | tf_op jit(solution)/shard_map/ppermute | solution.py:586
  151.5 2.5 %collective-permute-start.14 = (bf16[136,1024]{1,0:T(8,128)(2,1)S(1)}, bf16[136,1024]{1,0:T(8,128)(2,1)S(1)}, u32[]{:S(2)}, u32[]{:S(2)}) collective-permute-start(bf16[136,1024]{1,0:T(8,128)(2,1)S(1)} %get-tuple-element.49), channel_id=1, source_target_pairs={{0,224},{32,0},{64,32},{96,64},{128,96},{160,128},{192,160},{224,1... | collective-permute-start | bytes 835592 | tf_op jit(solution)/shard_map/ppermute | solution.py:586
  154.0 3.8 %collective-permute-done.14.refs_1_ = bf16[136,1024]{1,0:T(8,128)(2,1)S(1)} collective-permute-done((bf16[136,1024]{1,0:T(8,128)(2,1)S(1)}, bf16[136,1024]{1,0:T(8,128)(2,1)S(1)}, u32[]{:S(2)}, u32[]{:S(2)}) %collective-permute-start.14) | collective-permute-done | bytes 278560 | tf_op jit(solution)/shard_map/ppermute | solution.py:586
  157.9 3.4 %collective-permute-start.15 = (bf16[136,1024]{1,0:T(8,128)(2,1)S(1)}, bf16[136,1024]{1,0:T(8,128)(2,1)S(1)}, u32[]{:S(2)}, u32[]{:S(2)}) collective-permute-start(bf16[136,1024]{1,0:T(8,128)(2,1)S(1)} %hop.5), channel_id=1, source_target_pairs={{0,224},{32,0},{64,32},{96,64},{128,96},{160,128},{192,160},{224,1... | collective-permute-start | bytes 835592 | tf_op jit(solution)/shard_map/ppermute | solution.py:586
  161.3 3.5 %collective-permute-done.15.refs_2_ = bf16[136,1024]{1,0:T(8,128)(2,1)S(1)} collective-permute-done((bf16[136,1024]{1,0:T(8,128)(2,1)S(1)}, bf16[136,1024]{1,0:T(8,128)(2,1)S(1)}, u32[]{:S(2)}, u32[]{:S(2)}) %collective-permute-start.15) | collective-permute-done | bytes 278560 | tf_op jit(solution)/shard_map/ppermute | solution.py:586
  165.5 15.7 %all-to-all-done.1.recv_hbm = bf16[32,2,256,128]{3,2,1,0:T(8,128)(2,1)} async-done(((bf16[32,2,256,128]{3,2,1,0:T(8,128)(2,1)}), bf16[32,2,256,128]{3,2,1,0:T(8,128)(2,1)}, u32[]{:S(2)}, u32[]{:S(2)}) %all-to-all-start.1) | async-done | bytes 4194336 | tf_op jit(solution)/shard_map/all_to_all | solution.py:583
  181.2 8.2 %all-to-all-start.2 = ((f32[32,8,128]{2,1,0:T(8,128)}), f32[32,8,128]{2,1,0:T(8,128)S(1)}, u32[]{:S(2)}, u32[]{:S(2)}) async-start(f32[32,8,128]{2,1,0:T(8,128)} %pack.1), calls=%async_computation.2 | async-start | bytes 262144 | tf_op jit(solution)/shard_map/all_to_all | solution.py:583
  189.4 7.7 %slopes.1 = (bf16[256,4096]{1,0:T(8,128)(2,1)}, bf16[256,4096]{1,0:T(8,128)(2,1)}, bf16[256,4096]{1,0:T(8,128)(2,1)}) custom-call(bf16[256,4096]{1,0:T(8,128)(2,1)} %bitcast.20, bf16[256,4096]{1,0:T(8,128)(2,1)} %bitcast.22), custom_call_target="tpu_custom_call" | custom-call | flops 104857600 | bytes 16777216 | tf_op jit(solution)/shard_map/slopes/pallas_call | solution.py:160
  197.2 9.4 %collective-permute-start.16 = (bf16[128,1024]{1,0:T(8,128)(2,1)S(1)}, bf16[128,1024]{1,0:T(8,128)(2,1)S(1)}, u32[]{:S(2)}, u32[]{:S(2)}) collective-permute-start(bf16[128,1024]{1,0:T(8,128)(2,1)S(1)} %last.1), channel_id=1, source_target_pairs={{0,0},{32,1},{64,2},{96,3},{128,4},{160,5},{192,6},{224,7},{34,32}... | collective-permute-start | bytes 786440 | tf_op jit(solution)/shard_map/ppermute | solution.py:614
  207.7 8.4 %epilogue.1 = (bf16[256,4096]{1,0:T(8,128)(2,1)}, bf16[256,4096]{1,0:T(8,128)(2,1)}) custom-call(bf16[32,2,256,128]{3,2,1,0:T(8,128)(2,1)} %all-to-all-done.1.recv_hbm, bf16[256,4096]{1,0:T(8,128)(2,1)} %bitcast.18, bf16[256,4096]{1,0:T(8,128)(2,1)} %get-tuple-element.52.up_slope_hbm, bf16[256,4096]{1,0:T(8,128)(2,1)} %get-tuple-element.53.val_slope_hbm, ...), custom_call_target="tpu_custom_call" | custom-call | flops 20971520 | bytes 23068672 | tf_op jit(solution)/shard_map/epilogue/pallas_call | solution.py:547
  (37 shorter events, 5.2 us)
Async XLA Ops:
  8.5 8.8 %copy-start.4 = (bf16[1,128,1024]{2,1,0:T(8,128)(2,1)S(1)}, bf16[1,128,1024]{2,1,0:T(8,128)(2,1)}, u32[]{:S(2)}) copy-start(bf16[1,128,1024]{2,1,0:T(8,128)(2,1)} %param.9) | copy-start | bytes 786436
  8.5 50.6 %copy-start.5 = (f32[1,1024]{1,0:T(1,128)S(1)}, f32[1,1024]{1,0:T(1,128)}, u32[]{:S(2)}) copy-start(f32[1,1024]{1,0:T(1,128)} %param.10) | copy-start | bytes 12292
  8.5 96.7 %all-to-all-start = ((bf16[32,2,256,128]{3,2,1,0:T(8,128)(2,1)}), bf16[32,2,256,128]{3,2,1,0:T(8,128)(2,1)}, u32[]{:S(2)}, u32[]{:S(2)}) async-start(bf16[32,2,256,128]{3,2,1,0:T(8,128)(2,1)} %get-tuple-element.33), calls=%async_computation | async-start | bytes 8388608 | tf_op jit(solution)/shard_map/all_to_all | solution.py:583
  17.3 16.1 %collective-permute-start = (bf16[128,1024]{1,0:T(8,128)(2,1)S(1)}, bf16[128,1024]{1,0:T(8,128)(2,1)S(1)}, u32[]{:S(2)}, u32[]{:S(2)}) collective-permute-start(bf16[128,1024]{1,0:T(8,128)(2,1)S(1)} %bitcast.27), channel_id=1, source_target_pairs={{0,0},{1,32},{2,64},{3,96},{4,128},{5,160},{6,192},{7,224},{32,34}... | collective-permute-start | bytes 786440 | tf_op jit(solution)/shard_map/ppermute | solution.py:591
  33.4 12.0 %collective-permute-start.4 = (bf16[128,1024]{1,0:T(8,128)(2,1)S(1)}, bf16[128,1024]{1,0:T(8,128)(2,1)S(1)}, u32[]{:S(2)}, u32[]{:S(2)}) collective-permute-start(bf16[128,1024]{1,0:T(8,128)(2,1)S(1)} %collective-permute-done.refs_0_), channel_id=1, source_target_pairs={{0,224},{32,0},{64,32},{96,64},{128,96},{160,128},{192,160},{224,1... | collective-permute-start | bytes 786440 | tf_op jit(solution)/shard_map/ppermute | solution.py:586
  35.7 9.7 %collective-permute-start.1 = (bf16[128,1024]{1,0:T(8,128)(2,1)S(1)}, bf16[128,1024]{1,0:T(8,128)(2,1)S(1)}, u32[]{:S(2)}, u32[]{:S(2)}) collective-permute-start(bf16[128,1024]{1,0:T(8,128)(2,1)S(1)} %collective-permute-done.refs_0_), channel_id=1, source_target_pairs={{0,32},{32,64},{64,96},{96,128},{128,160},{160,192},{192,224},{224... | collective-permute-start | bytes 786440 | tf_op jit(solution)/shard_map/ppermute | solution.py:586
  45.4 5.6 %collective-permute-start.5 = (bf16[128,1024]{1,0:T(8,128)(2,1)S(1)}, bf16[128,1024]{1,0:T(8,128)(2,1)S(1)}, u32[]{:S(2)}, u32[]{:S(2)}) collective-permute-start(bf16[128,1024]{1,0:T(8,128)(2,1)S(1)} %collective-permute-done.4.refs_4_), channel_id=1, source_target_pairs={{0,224},{32,0},{64,32},{96,64},{128,96},{160,128},{192,160},{224,1... | collective-permute-start | bytes 786440 | tf_op jit(solution)/shard_map/ppermute | solution.py:586
  45.4 6.8 %collective-permute-start.2 = (bf16[128,1024]{1,0:T(8,128)(2,1)S(1)}, bf16[128,1024]{1,0:T(8,128)(2,1)S(1)}, u32[]{:S(2)}, u32[]{:S(2)}) collective-permute-start(bf16[128,1024]{1,0:T(8,128)(2,1)S(1)} %collective-permute-done.1.refs_1_), channel_id=1, source_target_pairs={{0,32},{32,64},{64,96},{96,128},{128,160},{160,192},{192,224},{224... | collective-permute-start | bytes 786440 | tf_op jit(solution)/shard_map/ppermute | solution.py:586
  51.1 5.6 %collective-permute-start.6 = (bf16[128,1024]{1,0:T(8,128)(2,1)S(1)}, bf16[128,1024]{1,0:T(8,128)(2,1)S(1)}, u32[]{:S(2)}, u32[]{:S(2)}) collective-permute-start(bf16[128,1024]{1,0:T(8,128)(2,1)S(1)} %collective-permute-done.5.refs_5_), channel_id=1, source_target_pairs={{0,224},{32,0},{64,32},{96,64},{128,96},{160,128},{192,160},{224,1... | collective-permute-start | bytes 786440 | tf_op jit(solution)/shard_map/ppermute | solution.py:586
  52.3 49.4 %collective-permute-start.3 = (bf16[128,1024]{1,0:T(8,128)(2,1)S(1)}, bf16[128,1024]{1,0:T(8,128)(2,1)S(1)}, u32[]{:S(2)}, u32[]{:S(2)}) collective-permute-start(bf16[128,1024]{1,0:T(8,128)(2,1)S(1)} %collective-permute-done.2.refs_2_), channel_id=1, source_target_pairs={{0,32},{32,64},{64,96},{96,128},{128,160},{160,192},{192,224},{224... | collective-permute-start | bytes 786440 | tf_op jit(solution)/shard_map/ppermute | solution.py:586
  56.7 45.0 %collective-permute-start.7 = (bf16[128,1024]{1,0:T(8,128)(2,1)S(1)}, bf16[128,1024]{1,0:T(8,128)(2,1)S(1)}, u32[]{:S(2)}, u32[]{:S(2)}) collective-permute-start(bf16[128,1024]{1,0:T(8,128)(2,1)S(1)} %collective-permute-done.6.refs_6_), channel_id=1, source_target_pairs={{0,224},{32,0},{64,32},{96,64},{128,96},{160,128},{192,160},{224,1... | collective-permute-start | bytes 786440 | tf_op jit(solution)/shard_map/ppermute | solution.py:586
  59.1 46.0 %collective-permute-start.8 = (f32[1,1024]{1,0:T(1,128)S(1)}, f32[1,1024]{1,0:T(1,128)S(1)}, u32[]{:S(2)}, u32[]{:S(2)}) collective-permute-start(f32[1,1024]{1,0:T(1,128)S(1)} %copy-done.5), channel_id=1, source_target_pairs={{0,0},{1,32},{2,64},{3,96},{4,128},{5,160},{6,192},{7,224},{32,34}... | collective-permute-start | bytes 12296 | tf_op jit(solution)/shard_map/ppermute | solution.py:588
  102.5 1.3 copy-start.1
  103.8 1.3 copy-start.2
  105.2 0.6 copy-start.6
  115.7 9.4 %copy-start.3 = (f32[1,128]{1,0:T(1,128)S(1)}, f32[1,128]{1,0:T(1,128)}, u32[]{:S(2)}) copy-start(f32[1,128]{1,0:T(1,128)} %get-tuple-element.37.sums_ref) | copy-start | bytes 1540
  115.7 65.5 %all-to-all-start.1 = ((bf16[32,2,256,128]{3,2,1,0:T(8,128)(2,1)}), bf16[32,2,256,128]{3,2,1,0:T(8,128)(2,1)}, u32[]{:S(2)}, u32[]{:S(2)}) async-start(bf16[32,2,256,128]{3,2,1,0:T(8,128)(2,1)} %bitcast.23), calls=%async_computation.1 | async-start | bytes 8388608 | tf_op jit(solution)/shard_map/all_to_all | solution.py:583
  131.4 33.4 %copy-start = (f32[4096]{0:T(1024)S(1)}, f32[4096]{0:T(1024)}, u32[]{:S(2)}) copy-start(f32[4096]{0:T(1024)} %param.11) | copy-start | bytes 49156
  131.4 8.3 %collective-permute-start.10 = (bf16[136,1024]{1,0:T(8,128)(2,1)S(1)}, bf16[136,1024]{1,0:T(8,128)(2,1)S(1)}, u32[]{:S(2)}, u32[]{:S(2)}) collective-permute-start(bf16[136,1024]{1,0:T(8,128)(2,1)S(1)} %get-tuple-element.44), channel_id=1, source_target_pairs={{0,224},{32,0},{64,32},{96,64},{128,96},{160,128},{192,160},{224,1... | collective-permute-start | bytes 835592 | tf_op jit(solution)/shard_map/ppermute | solution.py:586
  133.7 8.9 %collective-permute-start.9 = (bf16[136,1024]{1,0:T(8,128)(2,1)S(1)}, bf16[136,1024]{1,0:T(8,128)(2,1)S(1)}, u32[]{:S(2)}, u32[]{:S(2)}) collective-permute-start(bf16[136,1024]{1,0:T(8,128)(2,1)S(1)} %get-tuple-element.43), channel_id=1, source_target_pairs={{0,32},{32,64},{64,96},{96,128},{128,160},{160,192},{192,224},{224... | collective-permute-start | bytes 835592 | tf_op jit(solution)/shard_map/ppermute | solution.py:586
  142.8 8.4 %collective-permute-start.11 = (bf16[136,1024]{1,0:T(8,128)(2,1)S(1)}, bf16[136,1024]{1,0:T(8,128)(2,1)S(1)}, u32[]{:S(2)}, u32[]{:S(2)}) collective-permute-start(bf16[136,1024]{1,0:T(8,128)(2,1)S(1)} %get-tuple-element.45), channel_id=1, source_target_pairs={{0,32},{32,64},{64,96},{96,128},{128,160},{160,192},{192,224},{224... | collective-permute-start | bytes 835592 | tf_op jit(solution)/shard_map/ppermute | solution.py:586
  143.1 8.2 %collective-permute-start.12 = (bf16[136,1024]{1,0:T(8,128)(2,1)S(1)}, bf16[136,1024]{1,0:T(8,128)(2,1)S(1)}, u32[]{:S(2)}, u32[]{:S(2)}) collective-permute-start(bf16[136,1024]{1,0:T(8,128)(2,1)S(1)} %get-tuple-element.46), channel_id=1, source_target_pairs={{0,224},{32,0},{64,32},{96,64},{128,96},{160,128},{192,160},{224,1... | collective-permute-start | bytes 835592 | tf_op jit(solution)/shard_map/ppermute | solution.py:586
  151.5 6.3 %collective-permute-start.14 = (bf16[136,1024]{1,0:T(8,128)(2,1)S(1)}, bf16[136,1024]{1,0:T(8,128)(2,1)S(1)}, u32[]{:S(2)}, u32[]{:S(2)}) collective-permute-start(bf16[136,1024]{1,0:T(8,128)(2,1)S(1)} %get-tuple-element.49), channel_id=1, source_target_pairs={{0,224},{32,0},{64,32},{96,64},{128,96},{160,128},{192,160},{224,1... | collective-permute-start | bytes 835592 | tf_op jit(solution)/shard_map/ppermute | solution.py:586
  154.0 7.3 %collective-permute-start.13 = (bf16[136,1024]{1,0:T(8,128)(2,1)S(1)}, bf16[136,1024]{1,0:T(8,128)(2,1)S(1)}, u32[]{:S(2)}, u32[]{:S(2)}) collective-permute-start(bf16[136,1024]{1,0:T(8,128)(2,1)S(1)} %get-tuple-element.47), channel_id=1, source_target_pairs={{0,32},{32,64},{64,96},{96,128},{128,160},{160,192},{192,224},{224... | collective-permute-start | bytes 835592 | tf_op jit(solution)/shard_map/ppermute | solution.py:586
  157.9 6.9 %collective-permute-start.15 = (bf16[136,1024]{1,0:T(8,128)(2,1)S(1)}, bf16[136,1024]{1,0:T(8,128)(2,1)S(1)}, u32[]{:S(2)}, u32[]{:S(2)}) collective-permute-start(bf16[136,1024]{1,0:T(8,128)(2,1)S(1)} %hop.5), channel_id=1, source_target_pairs={{0,224},{32,0},{64,32},{96,64},{128,96},{160,128},{192,160},{224,1... | collective-permute-start | bytes 835592 | tf_op jit(solution)/shard_map/ppermute | solution.py:586
  181.2 25.4 %all-to-all-start.2 = ((f32[32,8,128]{2,1,0:T(8,128)}), f32[32,8,128]{2,1,0:T(8,128)S(1)}, u32[]{:S(2)}, u32[]{:S(2)}) async-start(f32[32,8,128]{2,1,0:T(8,128)} %pack.1), calls=%async_computation.2 | async-start | bytes 262144 | tf_op jit(solution)/shard_map/all_to_all | solution.py:583
  197.2 19.0 %collective-permute-start.16 = (bf16[128,1024]{1,0:T(8,128)(2,1)S(1)}, bf16[128,1024]{1,0:T(8,128)(2,1)S(1)}, u32[]{:S(2)}, u32[]{:S(2)}) collective-permute-start(bf16[128,1024]{1,0:T(8,128)(2,1)S(1)} %last.1), channel_id=1, source_target_pairs={{0,0},{32,1},{64,2},{96,3},{128,4},{160,5},{192,6},{224,7},{34,32}... | collective-permute-start | bytes 786440 | tf_op jit(solution)/shard_map/ppermute | solution.py:614

commit v8 on v7

--- a/solution.py
+++ b/solution.py
@@ -12,7 +12,7 @@
 Z = "sp_0"
 SP = ("sp_0", "sp_1")
 DP = ("dp_0", "dp_1")
-PLANE = ("dp_1", "dp_0", "sp_1")
+PLANE = ("dp_0", "dp_1", "sp_1")
 Z_DP = ("sp_0", "dp_0", "dp_1")
 
 norm_floor = 0.5
@@ -78,7 +78,7 @@
             cols = pl.ds(pl.multiple_of(g * LANES, LANES), LANES)
             up = up_ref[at, cols].astype(F32)
             up_act = (up * normal_cdf(up)).astype(BF16).astype(F32)
-            out_ref[g, 0, at] = (cot_ref[at, cols].astype(F32) * up_act).astype(BF16)
+            out_ref[block_of(g), 0, at] = (cot_ref[at, cols].astype(F32) * up_act).astype(BF16)
             val = val_ref[at, cols].astype(F32)
             act = val * normal_cdf(val)
             act_ref[:, cols] = act
@@ -91,7 +91,7 @@
 
         def second(g, carry):
             cols = pl.ds(pl.multiple_of(g * LANES, LANES), LANES)
-            out_ref[g, 1, at] = (act_ref[:, cols] * inv * gain_ref[:, cols]).astype(BF16)
+            out_ref[block_of(g), 1, at] = (act_ref[:, cols] * inv * gain_ref[:, cols]).astype(BF16)
             return carry
 
         lax.fori_loop(0, groups, second, 0, unroll=4)
@@ -177,6 +177,11 @@
 
 def place(column):
     return column % 4 * 2 + column // 4
+
+
+def block_of(group):
+    at = group >> 2
+    return ((at & 3) * 2 + (at >> 2)) * 4 + (group & 3)
 
 
 def slab_of(z_offset):
@@ -449,7 +454,7 @@
     gain_sum = sums[:, :LANES] / gain
     small_ref[...] = jnp.zeros_like(small_ref)
     for a in range(seqs):
-        at = slice((place(a) + 1) * LANES, (place(a) + 2) * LANES)
+        at = slice((a + 1) * LANES, (a + 2) * LANES)
         for y in range(parts):
             small_ref[a * parts + y, :1] = gain_sum
             small_ref[a * parts + y, 1:2] = sums[:, at]
@@ -465,6 +470,29 @@
         compiler_params=limit(8),
         name="pack",
     )(*pieces, gain)
+
+
+def unpack_kernel(parts, small_ref, gain_ref, bias_ref):
+    for group in range(small_ref.shape[0]):
+        gain_ref[group : group + 1] = small_ref[block_of(group), :1]
+    mine = place(lax.axis_index(Z)) * parts + lax.axis_index("sp_1")
+    bias_ref[...] = small_ref[mine, 1:2]
+
+
+def unpack(small, parts):
+    count = small.shape[0]
+    gain, bias = pl.pallas_call(
+        functools.partial(unpack_kernel, parts),
+        in_specs=[VMEM],
+        out_specs=[VMEM] * 2,
+        out_shape=[
+            jax.ShapeDtypeStruct((count, LANES), F32),
+            jax.ShapeDtypeStruct((1, LANES), F32),
+        ],
+        compiler_params=limit(8),
+        name="unpack",
+    )(small)
+    return gain.reshape(-1), bias
 
 
 def epilogue_kernel(
@@ -511,9 +539,9 @@
 
         def first(g, dots):
             cols = pl.ds(pl.multiple_of(g * LANES, LANES), LANES)
-            mid = (cot_ref[at, cols].astype(F32) * recv_ref[g, 0, at].astype(F32)).astype(BF16)
+            mid = (cot_ref[at, cols].astype(F32) * recv_ref[block_of(g), 0, at].astype(F32)).astype(BF16)
             up_ref[at, cols] = (mid.astype(F32) * up_slope_ref[at, cols].astype(F32)).astype(BF16)
-            scaled = recv_ref[g, 1, at].astype(F32) * gain_ref[:, cols]
+            scaled = recv_ref[block_of(g), 1, at].astype(F32) * gain_ref[:, cols]
             return dots + scaled * act_ref[at, cols].astype(F32)
 
         dots = lax.fori_loop(0, groups, first, jnp.zeros((rows, LANES), F32), unroll=4)
@@ -523,7 +551,7 @@
 
         def second(g, carry):
             cols = pl.ds(pl.multiple_of(g * LANES, LANES), LANES)
-            scaled = recv_ref[g, 1, at].astype(F32) * gain_ref[:, cols]
+            scaled = recv_ref[block_of(g), 1, at].astype(F32) * gain_ref[:, cols]
             slope = inv * scaled - pull * act_ref[at, cols].astype(F32)
             val_ref[at, cols] = (slope * val_slope_ref[at, cols].astype(F32)).astype(BF16)
             return carry
@@ -586,9 +614,8 @@
         return lax.ppermute(x, Z, [(z, (z + by) % planes) for z in range(planes)])
 
     bias = lax.ppermute(spatial_bias, Z_DP, away)
+    weights = lax.ppermute(spatial_weight[0], Z_DP, away)
     sent, inv = prologue(cot, up, val, gain)
-    weights, sent = lax.optimization_barrier((spatial_weight[0], sent))
-    weights = lax.ppermute(weights, Z_DP, away)
     recv = exchange(sent)
     before, after = [weights], [weights]
     for _ in range(3):
@@ -613,9 +640,7 @@
     grads, back = lax.optimization_barrier((grads, back))
     grads = lax.ppermute(grads, Z_DP, home)
     small = exchange(small)
-    gain_grad = small[:, 0].reshape(-1)
-    mine = lax.axis_index(Z) * parts + lax.axis_index("sp_1")
-    bias_grad = lax.dynamic_slice_in_dim(small, mine, 1, axis=0)[:, 1]
+    gain_grad, bias_grad = unpack(small, parts)
     up_grad, value_grad = epilogue(back, cot, up_slope, val_slope, act, inv, gain)
     return (up_grad[None], value_grad[None], grads[None].astype(F32), bias_grad, gain_grad)
 

time: 218 us -> 207 us (0.950)
  starting transfers between devices: 106 us -> 97.3 us
    ppermute x1, starting transfers between devices: 42.6 us -> 32.8 us  [shards(): bias = lax.ppermute(spatial_bias, Z_DP, away)]
    all_to_all x3, waiting for transfers between devices: 15.7 us -> 11.5 us  [exchange(): return lax.all_to_all(x, PLANE, split_axis=0, concat_axis=0, tiled=True)]
    ppermute x1, waiting for transfers between devices: 0.01 us -> 3.47 us  [shards(): bias = lax.ppermute(spatial_bias, Z_DP, away)]
    all_to_all x3, starting transfers between devices: 26.4 us -> 29.3 us  [exchange(): return lax.all_to_all(x, PLANE, split_axis=0, concat_axis=0, tiled=True)]
  transfers between devices with their start and end apart: 20 -> 20, of which waited for: 10 -> 11; matrix products, arithmetic and copies ran while one was open for 1% -> 0% of each run, Pallas kernels for 11% -> 12%
where the time goes in v8:
time: 207 us; the launch traced here: 206 us
  starting transfers between devices  97.3 us (47%)
  waiting for transfers between devices  61.4 us (30%)
  Pallas kernels  42.8 us (21%)
  local copies, waits for them, and re-layouts  3.25 us (2%)
    ppermute x14, waiting for transfers between devices, shifted(): return lax.ppermute(x, Z, [(z, (z + by) % planes) for z in range(planes)])  34.2 us
    ppermute x1, starting transfers between devices, shards(): bias = lax.ppermute(spatial_bias, Z_DP, away)  32.8 us
    all_to_all x3, starting transfers between devices, exchange(): return lax.all_to_all(x, PLANE, split_axis=0, concat_axis=0, tiled=True)  29.3 us
    ppermute x14, starting transfers between devices, shifted(): return lax.ppermute(x, Z, [(z, (z + by) % planes) for z in range(planes)])  23.7 us
    ppermute x1, waiting for transfers between devices, shards(): weights = lax.ppermute(spatial_weight[0], Z_DP, away)  12.3 us
    all_to_all x3, waiting for transfers between devices, exchange(): return lax.all_to_all(x, PLANE, split_axis=0, concat_axis=0, tiled=True)  11.5 us
    pallas_call x1, Pallas kernels, mix(): pl.pallas_call(functools.partial(mix_kernel, seqs, parts, PER), in_specs=...  9.93 us
    pallas_call x1, Pallas kernels, epilogue(): pl.pallas_call(functools.partial(epilogue_kernel, groups, rows), in_specs...  8.31 us
  transfers between devices with their start and end apart: 20, of which 11 were waited for; matrix products, arithmetic and copies ran while one was open for 0% of the time, Pallas kernels for 12%

profile of v8, /device:TPU:1, one launch (start us, length us, event | category | flops | bytes accessed | tf_op | source)
XLA Modules:
  0.0 206.4 jit_solution(4916132065309508215)
XLA Ops:
  0.6 7.9 %prologue.1 = (bf16[32,2,256,128]{3,2,1,0:T(8,128)(2,1)}, f32[256,128]{1,0:T(8,128)}) custom-call(bf16[256,4096]{1,0:T(8,128)(2,1)} %bitcast.15, bf16[256,4096]{1,0:T(8,128)(2,1)} %bitcast.17, bf16[256,4096]{1,0:T(8,128)(2,1)} %bitcast.19, f32[1,4096]{1,0:T(1,128)} %bitcast.12), custom_call_target="tpu_custom_call" | custom-call | flops 104857600 | bytes 10485760 | tf_op jit(solution)/shard_map/prologue/pallas_call | solution.py:114
  8.6 8.8 %all-to-all-start = ((bf16[32,2,256,128]{3,2,1,0:T(8,128)(2,1)}), bf16[32,2,256,128]{3,2,1,0:T(8,128)(2,1)}, u32[]{:S(2)}, u32[]{:S(2)}) async-start(bf16[32,2,256,128]{3,2,1,0:T(8,128)(2,1)} %get-tuple-element.32), calls=%async_computation | async-start | bytes 8388608 | tf_op jit(solution)/shard_map/all_to_all | solution.py:611
  17.4 3.7 %collective-permute-start = (bf16[128,1024]{1,0:T(8,128)(2,1)S(1)}, bf16[128,1024]{1,0:T(8,128)(2,1)S(1)}, u32[]{:S(2)}, u32[]{:S(2)}) collective-permute-start(bf16[128,1024]{1,0:T(8,128)(2,1)S(1)} %bitcast.24), channel_id=1, source_target_pairs={{0,0},{1,32},{2,64},{3,96},{4,128},{5,160},{6,192},{7,224},{32,34}... | collective-permute-start | bytes 786440 | tf_op jit(solution)/shard_map/ppermute | solution.py:617
  21.2 12.3 %collective-permute-done.refs_0_ = bf16[128,1024]{1,0:T(8,128)(2,1)S(1)} collective-permute-done((bf16[128,1024]{1,0:T(8,128)(2,1)S(1)}, bf16[128,1024]{1,0:T(8,128)(2,1)S(1)}, u32[]{:S(2)}, u32[]{:S(2)}) %collective-permute-start) | collective-permute-done | bytes 262176 | tf_op jit(solution)/shard_map/ppermute | solution.py:617
  33.4 2.5 %collective-permute-start.4 = (bf16[128,1024]{1,0:T(8,128)(2,1)S(1)}, bf16[128,1024]{1,0:T(8,128)(2,1)S(1)}, u32[]{:S(2)}, u32[]{:S(2)}) collective-permute-start(bf16[128,1024]{1,0:T(8,128)(2,1)S(1)} %collective-permute-done.refs_0_), channel_id=1, source_target_pairs={{0,224},{32,0},{64,32},{96,64},{128,96},{160,128},{192,160},{224,1... | collective-permute-start | bytes 786440 | tf_op jit(solution)/shard_map/ppermute | solution.py:614
  35.9 5.5 %collective-permute-start.1 = (bf16[128,1024]{1,0:T(8,128)(2,1)S(1)}, bf16[128,1024]{1,0:T(8,128)(2,1)S(1)}, u32[]{:S(2)}, u32[]{:S(2)}) collective-permute-start(bf16[128,1024]{1,0:T(8,128)(2,1)S(1)} %collective-permute-done.refs_0_), channel_id=1, source_target_pairs={{0,32},{32,64},{64,96},{96,128},{128,160},{160,192},{192,224},{224... | collective-permute-start | bytes 786440 | tf_op jit(solution)/shard_map/ppermute | solution.py:614
  41.4 4.2 %collective-permute-done.4.refs_4_ = bf16[128,1024]{1,0:T(8,128)(2,1)S(1)} collective-permute-done((bf16[128,1024]{1,0:T(8,128)(2,1)S(1)}, bf16[128,1024]{1,0:T(8,128)(2,1)S(1)}, u32[]{:S(2)}, u32[]{:S(2)}) %collective-permute-start.4) | collective-permute-done | bytes 262176 | tf_op jit(solution)/shard_map/ppermute | solution.py:614
  45.6 1.5 collective-permute-start.2
  47.1 4.2 %collective-permute-done.5.refs_5_ = bf16[128,1024]{1,0:T(8,128)(2,1)S(1)} collective-permute-done((bf16[128,1024]{1,0:T(8,128)(2,1)S(1)}, bf16[128,1024]{1,0:T(8,128)(2,1)S(1)}, u32[]{:S(2)}, u32[]{:S(2)}) %collective-permute-start.5) | collective-permute-done | bytes 262176 | tf_op jit(solution)/shard_map/ppermute | solution.py:614
  52.7 4.2 %collective-permute-done.6.refs_6_ = bf16[128,1024]{1,0:T(8,128)(2,1)S(1)} collective-permute-done((bf16[128,1024]{1,0:T(8,128)(2,1)S(1)}, bf16[128,1024]{1,0:T(8,128)(2,1)S(1)}, u32[]{:S(2)}, u32[]{:S(2)}) %collective-permute-start.6) | collective-permute-done | bytes 262176 | tf_op jit(solution)/shard_map/ppermute | solution.py:614
  56.8 2.4 %collective-permute-start.7 = (bf16[128,1024]{1,0:T(8,128)(2,1)S(1)}, bf16[128,1024]{1,0:T(8,128)(2,1)S(1)}, u32[]{:S(2)}, u32[]{:S(2)}) collective-permute-start(bf16[128,1024]{1,0:T(8,128)(2,1)S(1)} %collective-permute-done.6.refs_6_), channel_id=1, source_target_pairs={{0,224},{32,0},{64,32},{96,64},{128,96},{160,128},{192,160},{224,1... | collective-permute-start | bytes 786440 | tf_op jit(solution)/shard_map/ppermute | solution.py:614
  59.3 32.8 %collective-permute-start.8 = (f32[1,1024]{1,0:T(1,128)S(1)}, f32[1,1024]{1,0:T(1,128)S(1)}, u32[]{:S(2)}, u32[]{:S(2)}) collective-permute-start(f32[1,1024]{1,0:T(1,128)S(1)} %copy-done.5), channel_id=1, source_target_pairs={{0,0},{1,32},{2,64},{3,96},{4,128},{5,160},{6,192},{7,224},{32,34}... | collective-permute-start | bytes 12296 | tf_op jit(solution)/shard_map/ppermute | solution.py:616
  92.9 1.3 copy-done.1
  94.2 1.3 copy-done.2
  95.5 3.5 %collective-permute-done.8.bias_row_ref = f32[1,1024]{1,0:T(1,128)S(1)} collective-permute-done((f32[1,1024]{1,0:T(1,128)S(1)}, f32[1,1024]{1,0:T(1,128)S(1)}, u32[]{:S(2)}, u32[]{:S(2)}) %collective-permute-start.8) | collective-permute-done | bytes 4128 | tf_op jit(solution)/shard_map/ppermute | solution.py:616
  99.6 9.9 %mix.1 = (bf16[8,4,2,256,128]{4,3,2,1,0:T(8,128)(2,1)}, f32[1,128]{1,0:T(1,128)}) custom-call(bf16[32,2,256,128]{3,2,1,0:T(8,128)(2,1)} %all-to-all-done.recv_hbm.recv_ref, bf16[1024,1024]{1,0:T(8,128)(2,1)} %copy-done.1, bf16[1024,1024]{1,0:T(8,128)(2,1)} %copy-done.2, f32[1,1024]{1,0:T(1,128)} %copy-done.6), custom_call_target="tpu_custom_call" | custom-call | flops 4294967296 | bytes 10485760 | tf_op jit(solution)/shard_map/mix/pallas_call | solution.py:296
  109.5 15.1 %all-to-all-start.1 = ((bf16[32,2,256,128]{3,2,1,0:T(8,128)(2,1)}), bf16[32,2,256,128]{3,2,1,0:T(8,128)(2,1)}, u32[]{:S(2)}, u32[]{:S(2)}) async-start(bf16[32,2,256,128]{3,2,1,0:T(8,128)(2,1)} %bitcast.21), calls=%async_computation.1 | async-start | bytes 8388608 | tf_op jit(solution)/shard_map/all_to_all | solution.py:611
  124.7 6.3 %weight_grads.1 = (bf16[136,1024]{1,0:T(8,128)(2,1)S(1)}, bf16[136,1024]{1,0:T(8,128)(2,1)S(1)}, bf16[136,1024]{1,0:T(8,128)(2,1)S(1)}, bf16[136,1024]{1,0:T(8,1...) custom-call(bf16[32,2,256,128]{3,2,1,0:T(8,128)(2,1)} %all-to-all-do, ...), custom_call_target="tpu_custom_call" | custom-call | flops 2147483648 | bytes 6291456 | tf_op jit(solution)/shard_map/weight_grads/pallas_call | solution.py:387
  131.0 1.5 collective-permute-start.10
  132.5 6.6 %collective-permute-done.10.refs_3_ = bf16[136,1024]{1,0:T(8,128)(2,1)S(1)} collective-permute-done((bf16[136,1024]{1,0:T(8,128)(2,1)S(1)}, bf16[136,1024]{1,0:T(8,128)(2,1)S(1)}, u32[]{:S(2)}, u32[]{:S(2)}) %collective-permute-start.10) | collective-permute-done | bytes 278560 | tf_op jit(solution)/shard_map/ppermute | solution.py:614
  139.1 2.3 %collective-permute-done.9.refs_2_ = bf16[136,1024]{1,0:T(8,128)(2,1)S(1)} collective-permute-done((bf16[136,1024]{1,0:T(8,128)(2,1)S(1)}, bf16[136,1024]{1,0:T(8,128)(2,1)S(1)}, u32[]{:S(2)}, u32[]{:S(2)}) %collective-permute-start.9) | collective-permute-done | bytes 278560 | tf_op jit(solution)/shard_map/ppermute | solution.py:614
  141.9 2.7 %collective-permute-start.12 = (bf16[136,1024]{1,0:T(8,128)(2,1)S(1)}, bf16[136,1024]{1,0:T(8,128)(2,1)S(1)}, u32[]{:S(2)}, u32[]{:S(2)}) collective-permute-start(bf16[136,1024]{1,0:T(8,128)(2,1)S(1)} %get-tuple-element.44), channel_id=1, source_target_pairs={{0,224},{32,0},{64,32},{96,64},{128,96},{160,128},{192,160},{224,1... | collective-permute-start | bytes 835592 | tf_op jit(solution)/shard_map/ppermute | solution.py:614
  144.5 5.5 %collective-permute-done.11.refs_2_ = bf16[136,1024]{1,0:T(8,128)(2,1)S(1)} collective-permute-done((bf16[136,1024]{1,0:T(8,128)(2,1)S(1)}, bf16[136,1024]{1,0:T(8,128)(2,1)S(1)}, u32[]{:S(2)}, u32[]{:S(2)}) %collective-permute-start.11) | collective-permute-done | bytes 278560 | tf_op jit(solution)/shard_map/ppermute | solution.py:614
  150.3 2.5 %collective-permute-start.14 = (bf16[136,1024]{1,0:T(8,128)(2,1)S(1)}, bf16[136,1024]{1,0:T(8,128)(2,1)S(1)}, u32[]{:S(2)}, u32[]{:S(2)}) collective-permute-start(bf16[136,1024]{1,0:T(8,128)(2,1)S(1)} %get-tuple-element.47), channel_id=1, source_target_pairs={{0,224},{32,0},{64,32},{96,64},{128,96},{160,128},{192,160},{224,1... | collective-permute-start | bytes 835592 | tf_op jit(solution)/shard_map/ppermute | solution.py:614
  152.7 3.8 %collective-permute-done.14.refs_1_ = bf16[136,1024]{1,0:T(8,128)(2,1)S(1)} collective-permute-done((bf16[136,1024]{1,0:T(8,128)(2,1)S(1)}, bf16[136,1024]{1,0:T(8,128)(2,1)S(1)}, u32[]{:S(2)}, u32[]{:S(2)}) %collective-permute-start.14) | collective-permute-done | bytes 278560 | tf_op jit(solution)/shard_map/ppermute | solution.py:614
  156.7 3.4 %collective-permute-start.15 = (bf16[136,1024]{1,0:T(8,128)(2,1)S(1)}, bf16[136,1024]{1,0:T(8,128)(2,1)S(1)}, u32[]{:S(2)}, u32[]{:S(2)}) collective-permute-start(bf16[136,1024]{1,0:T(8,128)(2,1)S(1)} %hop.5), channel_id=1, source_target_pairs={{0,224},{32,0},{64,32},{96,64},{128,96},{160,128},{192,160},{224,1... | collective-permute-start | bytes 835592 | tf_op jit(solution)/shard_map/ppermute | solution.py:614
  160.1 3.5 %collective-permute-done.15.refs_2_ = bf16[136,1024]{1,0:T(8,128)(2,1)S(1)} collective-permute-done((bf16[136,1024]{1,0:T(8,128)(2,1)S(1)}, bf16[136,1024]{1,0:T(8,128)(2,1)S(1)}, u32[]{:S(2)}, u32[]{:S(2)}) %collective-permute-start.15) | collective-permute-done | bytes 278560 | tf_op jit(solution)/shard_map/ppermute | solution.py:614
  163.7 11.5 %all-to-all-done.1.recv_hbm = bf16[32,2,256,128]{3,2,1,0:T(8,128)(2,1)} async-done(((bf16[32,2,256,128]{3,2,1,0:T(8,128)(2,1)}), bf16[32,2,256,128]{3,2,1,0:T(8,128)(2,1)}, u32[]{:S(2)}, u32[]{:S(2)}) %all-to-all-start.1) | async-done | bytes 4194336 | tf_op jit(solution)/shard_map/all_to_all | solution.py:611
  175.1 7.7 %collective-permute-start.16 = (bf16[128,1024]{1,0:T(8,128)(2,1)S(1)}, bf16[128,1024]{1,0:T(8,128)(2,1)S(1)}, u32[]{:S(2)}, u32[]{:S(2)}) collective-permute-start(bf16[128,1024]{1,0:T(8,128)(2,1)S(1)} %last.1), channel_id=1, source_target_pairs={{0,0},{32,1},{64,2},{96,3},{128,4},{160,5},{192,6},{224,7},{34,32}... | collective-permute-start | bytes 786440 | tf_op jit(solution)/shard_map/ppermute | solution.py:641
  183.6 5.4 %all-to-all-start.2 = ((f32[32,8,128]{2,1,0:T(8,128)}), f32[32,8,128]{2,1,0:T(8,128)S(1)}, u32[]{:S(2)}, u32[]{:S(2)}) async-start(f32[32,8,128]{2,1,0:T(8,128)} %pack.1), calls=%async_computation.2 | async-start | bytes 262144 | tf_op jit(solution)/shard_map/all_to_all | solution.py:611
  189.0 7.7 %slopes.1 = (bf16[256,4096]{1,0:T(8,128)(2,1)}, bf16[256,4096]{1,0:T(8,128)(2,1)}, bf16[256,4096]{1,0:T(8,128)(2,1)}) custom-call(bf16[256,4096]{1,0:T(8,128)(2,1)} %bitcast.18, bf16[256,4096]{1,0:T(8,128)(2,1)} %bitcast.20), custom_call_target="tpu_custom_call" | custom-call | flops 104857600 | bytes 16777216 | tf_op jit(solution)/shard_map/slopes/pallas_call | solution.py:160
  197.3 8.3 %epilogue.1 = (bf16[256,4096]{1,0:T(8,128)(2,1)}, bf16[256,4096]{1,0:T(8,128)(2,1)}) custom-call(bf16[32,2,256,128]{3,2,1,0:T(8,128)(2,1)} %all-to-all-done.1.recv_hbm, bf16[256,4096]{1,0:T(8,128)(2,1)} %bitcast.16, bf16[256,4096]{1,0:T(8,128)(2,1)} %get-tuple-element.50.up_slope_hbm, bf16[256,4096]{1,0:T(8,128)(2,1)} %get-tuple-element.51.val_slope_hbm, ...), custom_call_target="tpu_custom_call" | custom-call | flops 20971520 | bytes 23068672 | tf_op jit(solution)/shard_map/epilogue/pallas_call | solution.py:575
  (35 shorter events, 6.0 us)
Async XLA Ops:
  8.6 8.8 %copy-start.4 = (bf16[1,128,1024]{2,1,0:T(8,128)(2,1)S(1)}, bf16[1,128,1024]{2,1,0:T(8,128)(2,1)}, u32[]{:S(2)}) copy-start(bf16[1,128,1024]{2,1,0:T(8,128)(2,1)} %param.9) | copy-start | bytes 786436
  8.6 50.7 %copy-start.5 = (f32[1,1024]{1,0:T(1,128)S(1)}, f32[1,1024]{1,0:T(1,128)}, u32[]{:S(2)}) copy-start(f32[1,1024]{1,0:T(1,128)} %param.10) | copy-start | bytes 12292
  8.6 90.4 %all-to-all-start = ((bf16[32,2,256,128]{3,2,1,0:T(8,128)(2,1)}), bf16[32,2,256,128]{3,2,1,0:T(8,128)(2,1)}, u32[]{:S(2)}, u32[]{:S(2)}) async-start(bf16[32,2,256,128]{3,2,1,0:T(8,128)(2,1)} %get-tuple-element.32), calls=%async_computation | async-start | bytes 8388608 | tf_op jit(solution)/shard_map/all_to_all | solution.py:611
  17.4 16.0 %collective-permute-start = (bf16[128,1024]{1,0:T(8,128)(2,1)S(1)}, bf16[128,1024]{1,0:T(8,128)(2,1)S(1)}, u32[]{:S(2)}, u32[]{:S(2)}) collective-permute-start(bf16[128,1024]{1,0:T(8,128)(2,1)S(1)} %bitcast.24), channel_id=1, source_target_pairs={{0,0},{1,32},{2,64},{3,96},{4,128},{5,160},{6,192},{7,224},{32,34}... | collective-permute-start | bytes 786440 | tf_op jit(solution)/shard_map/ppermute | solution.py:617
  33.4 12.2 %collective-permute-start.4 = (bf16[128,1024]{1,0:T(8,128)(2,1)S(1)}, bf16[128,1024]{1,0:T(8,128)(2,1)S(1)}, u32[]{:S(2)}, u32[]{:S(2)}) collective-permute-start(bf16[128,1024]{1,0:T(8,128)(2,1)S(1)} %collective-permute-done.refs_0_), channel_id=1, source_target_pairs={{0,224},{32,0},{64,32},{96,64},{128,96},{160,128},{192,160},{224,1... | collective-permute-start | bytes 786440 | tf_op jit(solution)/shard_map/ppermute | solution.py:614
  35.9 9.7 %collective-permute-start.1 = (bf16[128,1024]{1,0:T(8,128)(2,1)S(1)}, bf16[128,1024]{1,0:T(8,128)(2,1)S(1)}, u32[]{:S(2)}, u32[]{:S(2)}) collective-permute-start(bf16[128,1024]{1,0:T(8,128)(2,1)S(1)} %collective-permute-done.refs_0_), channel_id=1, source_target_pairs={{0,32},{32,64},{64,96},{96,128},{128,160},{160,192},{192,224},{224... | collective-permute-start | bytes 786440 | tf_op jit(solution)/shard_map/ppermute | solution.py:614
  45.6 5.6 %collective-permute-start.5 = (bf16[128,1024]{1,0:T(8,128)(2,1)S(1)}, bf16[128,1024]{1,0:T(8,128)(2,1)S(1)}, u32[]{:S(2)}, u32[]{:S(2)}) collective-permute-start(bf16[128,1024]{1,0:T(8,128)(2,1)S(1)} %collective-permute-done.4.refs_4_), channel_id=1, source_target_pairs={{0,224},{32,0},{64,32},{96,64},{128,96},{160,128},{192,160},{224,1... | collective-permute-start | bytes 786440 | tf_op jit(solution)/shard_map/ppermute | solution.py:614
  45.6 6.8 %collective-permute-start.2 = (bf16[128,1024]{1,0:T(8,128)(2,1)S(1)}, bf16[128,1024]{1,0:T(8,128)(2,1)S(1)}, u32[]{:S(2)}, u32[]{:S(2)}) collective-permute-start(bf16[128,1024]{1,0:T(8,128)(2,1)S(1)} %collective-permute-done.1.refs_1_), channel_id=1, source_target_pairs={{0,32},{32,64},{64,96},{96,128},{128,160},{160,192},{192,224},{224... | collective-permute-start | bytes 786440 | tf_op jit(solution)/shard_map/ppermute | solution.py:614
  51.2 5.6 %collective-permute-start.6 = (bf16[128,1024]{1,0:T(8,128)(2,1)S(1)}, bf16[128,1024]{1,0:T(8,128)(2,1)S(1)}, u32[]{:S(2)}, u32[]{:S(2)}) collective-permute-start(bf16[128,1024]{1,0:T(8,128)(2,1)S(1)} %collective-permute-done.5.refs_5_), channel_id=1, source_target_pairs={{0,224},{32,0},{64,32},{96,64},{128,96},{160,128},{192,160},{224,1... | collective-permute-start | bytes 786440 | tf_op jit(solution)/shard_map/ppermute | solution.py:614
  52.4 39.6 %collective-permute-start.3 = (bf16[128,1024]{1,0:T(8,128)(2,1)S(1)}, bf16[128,1024]{1,0:T(8,128)(2,1)S(1)}, u32[]{:S(2)}, u32[]{:S(2)}) collective-permute-start(bf16[128,1024]{1,0:T(8,128)(2,1)S(1)} %collective-permute-done.2.refs_2_), channel_id=1, source_target_pairs={{0,32},{32,64},{64,96},{96,128},{128,160},{160,192},{192,224},{224... | collective-permute-start | bytes 786440 | tf_op jit(solution)/shard_map/ppermute | solution.py:614
  56.8 35.3 %collective-permute-start.7 = (bf16[128,1024]{1,0:T(8,128)(2,1)S(1)}, bf16[128,1024]{1,0:T(8,128)(2,1)S(1)}, u32[]{:S(2)}, u32[]{:S(2)}) collective-permute-start(bf16[128,1024]{1,0:T(8,128)(2,1)S(1)} %collective-permute-done.6.refs_6_), channel_id=1, source_target_pairs={{0,224},{32,0},{64,32},{96,64},{128,96},{160,128},{192,160},{224,1... | collective-permute-start | bytes 786440 | tf_op jit(solution)/shard_map/ppermute | solution.py:614
  59.3 39.7 %collective-permute-start.8 = (f32[1,1024]{1,0:T(1,128)S(1)}, f32[1,1024]{1,0:T(1,128)S(1)}, u32[]{:S(2)}, u32[]{:S(2)}) collective-permute-start(f32[1,1024]{1,0:T(1,128)S(1)} %copy-done.5), channel_id=1, source_target_pairs={{0,0},{1,32},{2,64},{3,96},{4,128},{5,160},{6,192},{7,224},{32,34}... | collective-permute-start | bytes 12296 | tf_op jit(solution)/shard_map/ppermute | solution.py:616
  92.9 1.3 copy-start.1
  94.2 1.3 copy-start.2
  99.0 0.6 copy-start.6
  109.5 15.1 %copy-start.3 = (f32[1,128]{1,0:T(1,128)S(1)}, f32[1,128]{1,0:T(1,128)}, u32[]{:S(2)}) copy-start(f32[1,128]{1,0:T(1,128)} %get-tuple-element.35.sums_ref) | copy-start | bytes 1540
  109.5 65.6 %all-to-all-start.1 = ((bf16[32,2,256,128]{3,2,1,0:T(8,128)(2,1)}), bf16[32,2,256,128]{3,2,1,0:T(8,128)(2,1)}, u32[]{:S(2)}, u32[]{:S(2)}) async-start(bf16[32,2,256,128]{3,2,1,0:T(8,128)(2,1)} %bitcast.21), calls=%async_computation.1 | async-start | bytes 8388608 | tf_op jit(solution)/shard_map/all_to_all | solution.py:611
  131.0 51.9 %copy-start = (f32[4096]{0:T(1024)S(1)}, f32[4096]{0:T(1024)}, u32[]{:S(2)}) copy-start(f32[4096]{0:T(1024)} %param.11) | copy-start | bytes 49156
  131.0 8.1 %collective-permute-start.10 = (bf16[136,1024]{1,0:T(8,128)(2,1)S(1)}, bf16[136,1024]{1,0:T(8,128)(2,1)S(1)}, u32[]{:S(2)}, u32[]{:S(2)}) collective-permute-start(bf16[136,1024]{1,0:T(8,128)(2,1)S(1)} %get-tuple-element.42), channel_id=1, source_target_pairs={{0,224},{32,0},{64,32},{96,64},{128,96},{160,128},{192,160},{224,1... | collective-permute-start | bytes 835592 | tf_op jit(solution)/shard_map/ppermute | solution.py:614
  132.4 8.9 %collective-permute-start.9 = (bf16[136,1024]{1,0:T(8,128)(2,1)S(1)}, bf16[136,1024]{1,0:T(8,128)(2,1)S(1)}, u32[]{:S(2)}, u32[]{:S(2)}) collective-permute-start(bf16[136,1024]{1,0:T(8,128)(2,1)S(1)} %get-tuple-element.41), channel_id=1, source_target_pairs={{0,32},{32,64},{64,96},{96,128},{128,160},{160,192},{192,224},{224... | collective-permute-start | bytes 835592 | tf_op jit(solution)/shard_map/ppermute | solution.py:614
  141.6 8.5 %collective-permute-start.11 = (bf16[136,1024]{1,0:T(8,128)(2,1)S(1)}, bf16[136,1024]{1,0:T(8,128)(2,1)S(1)}, u32[]{:S(2)}, u32[]{:S(2)}) collective-permute-start(bf16[136,1024]{1,0:T(8,128)(2,1)S(1)} %get-tuple-element.43), channel_id=1, source_target_pairs={{0,32},{32,64},{64,96},{96,128},{128,160},{160,192},{192,224},{224... | collective-permute-start | bytes 835592 | tf_op jit(solution)/shard_map/ppermute | solution.py:614
  141.9 8.2 %collective-permute-start.12 = (bf16[136,1024]{1,0:T(8,128)(2,1)S(1)}, bf16[136,1024]{1,0:T(8,128)(2,1)S(1)}, u32[]{:S(2)}, u32[]{:S(2)}) collective-permute-start(bf16[136,1024]{1,0:T(8,128)(2,1)S(1)} %get-tuple-element.44), channel_id=1, source_target_pairs={{0,224},{32,0},{64,32},{96,64},{128,96},{160,128},{192,160},{224,1... | collective-permute-start | bytes 835592 | tf_op jit(solution)/shard_map/ppermute | solution.py:614
  150.3 6.3 %collective-permute-start.14 = (bf16[136,1024]{1,0:T(8,128)(2,1)S(1)}, bf16[136,1024]{1,0:T(8,128)(2,1)S(1)}, u32[]{:S(2)}, u32[]{:S(2)}) collective-permute-start(bf16[136,1024]{1,0:T(8,128)(2,1)S(1)} %get-tuple-element.47), channel_id=1, source_target_pairs={{0,224},{32,0},{64,32},{96,64},{128,96},{160,128},{192,160},{224,1... | collective-permute-start | bytes 835592 | tf_op jit(solution)/shard_map/ppermute | solution.py:614
  152.7 7.3 %collective-permute-start.13 = (bf16[136,1024]{1,0:T(8,128)(2,1)S(1)}, bf16[136,1024]{1,0:T(8,128)(2,1)S(1)}, u32[]{:S(2)}, u32[]{:S(2)}) collective-permute-start(bf16[136,1024]{1,0:T(8,128)(2,1)S(1)} %get-tuple-element.45), channel_id=1, source_target_pairs={{0,32},{32,64},{64,96},{96,128},{128,160},{160,192},{192,224},{224... | collective-permute-start | bytes 835592 | tf_op jit(solution)/shard_map/ppermute | solution.py:614
  156.7 6.9 %collective-permute-start.15 = (bf16[136,1024]{1,0:T(8,128)(2,1)S(1)}, bf16[136,1024]{1,0:T(8,128)(2,1)S(1)}, u32[]{:S(2)}, u32[]{:S(2)}) collective-permute-start(bf16[136,1024]{1,0:T(8,128)(2,1)S(1)} %hop.5), channel_id=1, source_target_pairs={{0,224},{32,0},{64,32},{96,64},{128,96},{160,128},{192,160},{224,1... | collective-permute-start | bytes 835592 | tf_op jit(solution)/shard_map/ppermute | solution.py:614
  175.1 30.5 %collective-permute-start.16 = (bf16[128,1024]{1,0:T(8,128)(2,1)S(1)}, bf16[128,1024]{1,0:T(8,128)(2,1)S(1)}, u32[]{:S(2)}, u32[]{:S(2)}) collective-permute-start(bf16[128,1024]{1,0:T(8,128)(2,1)S(1)} %last.1), channel_id=1, source_target_pairs={{0,0},{32,1},{64,2},{96,3},{128,4},{160,5},{192,6},{224,7},{34,32}... | collective-permute-start | bytes 786440 | tf_op jit(solution)/shard_map/ppermute | solution.py:641
  183.6 13.1 %all-to-all-start.2 = ((f32[32,8,128]{2,1,0:T(8,128)}), f32[32,8,128]{2,1,0:T(8,128)S(1)}, u32[]{:S(2)}, u32[]{:S(2)}) async-start(f32[32,8,128]{2,1,0:T(8,128)} %pack.1), calls=%async_computation.2 | async-start | bytes 262144 | tf_op jit(solution)/shard_map/all_to_all | solution.py:611

commit v9 on v8

--- a/solution.py
+++ b/solution.py
@@ -623,7 +623,6 @@
         after.append(shifted(after[-1], -1))
     after.append(shifted(after[-1], -1))
     pieces = before + after[1:]
-    up_slope, val_slope, act = slopes(up, val)
     w, wt = arrange(pieces)
     back, sums = mix(recv, w, wt, bias, seqs, parts)
     back = exchange(back)
@@ -636,8 +635,10 @@
     (minus,) = hop((m1,), (minus,))
     minus = shifted(minus, -1)
     grads = last((own, plus, minus))
+    later_up, later_val, grads = lax.optimization_barrier((up, val, grads))
+    up_slope, val_slope, act = slopes(later_up, later_val)
     small = pack((own, plus, minus), gain, seqs, parts)
-    grads, back = lax.optimization_barrier((grads, back))
+    grads, up_slope = lax.optimization_barrier((grads, up_slope))
     grads = lax.ppermute(grads, Z_DP, home)
     small = exchange(small)
     gain_grad, bias_grad = unpack(small, parts)

time: 207 us -> 256 us (1.24)
  the two profiles are of different devices: /device:TPU:1 before, /device:TPU:98 now
where the time goes in v9:
time: 256 us; the launch traced here: 255 us
  waiting for transfers between devices  115 us (45%)
  starting transfers between devices  68.4 us (27%)
  Pallas kernels  42.2 us (16%)
  blocking collectives  24.2 us (9%)
  local copies, waits for them, and re-layouts  3.89 us (2%)
    ppermute x14, starting transfers between devices, shifted(): return lax.ppermute(x, Z, [(z, (z + by) % planes) for z in range(planes)])  47.7 us
    ppermute x14, waiting for transfers between devices, shifted(): return lax.ppermute(x, Z, [(z, (z + by) % planes) for z in range(planes)])  47.1 us
    all_to_all x2, waiting for transfers between devices, exchange(): return lax.all_to_all(x, PLANE, split_axis=0, concat_axis=0, tiled=True)  37.5 us
    all_to_all x1, blocking collectives, exchange(): return lax.all_to_all(x, PLANE, split_axis=0, concat_axis=0, tiled=True)  24.2 us
    ppermute x1, waiting for transfers between devices, shards(): grads = lax.ppermute(grads, Z_DP, home)  17.5 us
    all_to_all x2, starting transfers between devices, exchange(): return lax.all_to_all(x, PLANE, split_axis=0, concat_axis=0, tiled=True)  13.8 us
    ppermute x1, waiting for transfers between devices, shards(): weights = lax.ppermute(spatial_weight[0], Z_DP, away)  12.5 us
    pallas_call x1, Pallas kernels, mix(): pl.pallas_call(functools.partial(mix_kernel, seqs, parts, PER), in_specs=...  9.98 us
  transfers between devices with their start and end apart: 19, of which 15 were waited for; matrix products, arithmetic and copies ran while one was open for 0% of the time, Pallas kernels for 4%

profile of v9, /device:TPU:98, one launch (start us, length us, event | category | flops | bytes accessed | tf_op | source)
XLA Modules:
  0.0 255.3 jit_solution(16549068551927657397)
XLA Ops:
  0.6 8.0 %prologue.1 = (bf16[32,2,256,128]{3,2,1,0:T(8,128)(2,1)}, f32[256,128]{1,0:T(8,128)}) custom-call(bf16[256,4096]{1,0:T(8,128)(2,1)} %bitcast.15, bf16[256,4096]{1,0:T(8,128)(2,1)} %bitcast.17, bf16[256,4096]{1,0:T(8,128)(2,1)} %bitcast.19, f32[1,4096]{1,0:T(1,128)} %bitcast.12), custom_call_target="tpu_custom_call" | custom-call | flops 104857600 | bytes 10485760 | tf_op jit(solution)/shard_map/prologue/pallas_call | solution.py:114
  8.7 7.8 %all-to-all-start = ((bf16[32,2,256,128]{3,2,1,0:T(8,128)(2,1)}), bf16[32,2,256,128]{3,2,1,0:T(8,128)(2,1)}, u32[]{:S(2)}, u32[]{:S(2)}) async-start(bf16[32,2,256,128]{3,2,1,0:T(8,128)(2,1)} %get-tuple-element.35), calls=%async_computation | async-start | bytes 8388608 | tf_op jit(solution)/shard_map/all_to_all | solution.py:611
  16.5 3.1 %collective-permute-start = (bf16[128,1024]{1,0:T(8,128)(2,1)S(1)}, bf16[128,1024]{1,0:T(8,128)(2,1)S(1)}, u32[]{:S(2)}, u32[]{:S(2)}) collective-permute-start(bf16[128,1024]{1,0:T(8,128)(2,1)S(1)} %bitcast.24), channel_id=1, source_target_pairs={{0,0},{1,32},{2,64},{3,96},{4,128},{5,160},{6,192},{7,224},{32,34}... | collective-permute-start | bytes 786440 | tf_op jit(solution)/shard_map/ppermute | solution.py:617
  19.7 12.5 %collective-permute-done.refs_0_ = bf16[128,1024]{1,0:T(8,128)(2,1)S(1)} collective-permute-done((bf16[128,1024]{1,0:T(8,128)(2,1)S(1)}, bf16[128,1024]{1,0:T(8,128)(2,1)S(1)}, u32[]{:S(2)}, u32[]{:S(2)}) %collective-permute-start) | collective-permute-done | bytes 262176 | tf_op jit(solution)/shard_map/ppermute | solution.py:617
  32.2 5.8 %collective-permute-start.1 = (bf16[128,1024]{1,0:T(8,128)(2,1)S(1)}, bf16[128,1024]{1,0:T(8,128)(2,1)S(1)}, u32[]{:S(2)}, u32[]{:S(2)}) collective-permute-start(bf16[128,1024]{1,0:T(8,128)(2,1)S(1)} %collective-permute-done.refs_0_), channel_id=1, source_target_pairs={{0,32},{32,64},{64,96},{96,128},{128,160},{160,192},{192,224},{224... | collective-permute-start | bytes 786440 | tf_op jit(solution)/shard_map/ppermute | solution.py:614
  38.0 4.3 %collective-permute-done.4.refs_4_ = bf16[128,1024]{1,0:T(8,128)(2,1)S(1)} collective-permute-done((bf16[128,1024]{1,0:T(8,128)(2,1)S(1)}, bf16[128,1024]{1,0:T(8,128)(2,1)S(1)}, u32[]{:S(2)}, u32[]{:S(2)}) %collective-permute-start.4) | collective-permute-done | bytes 262176 | tf_op jit(solution)/shard_map/ppermute | solution.py:614
  42.3 27.8 %collective-permute-start.5 = (bf16[128,1024]{1,0:T(8,128)(2,1)S(1)}, bf16[128,1024]{1,0:T(8,128)(2,1)S(1)}, u32[]{:S(2)}, u32[]{:S(2)}) collective-permute-start(bf16[128,1024]{1,0:T(8,128)(2,1)S(1)} %collective-permute-done.4.refs_4_), channel_id=1, source_target_pairs={{0,224},{32,0},{64,32},{96,64},{128,96},{160,128},{192,160},{224,1... | collective-permute-start | bytes 786440 | tf_op jit(solution)/shard_map/ppermute | solution.py:614
  70.6 3.4 %collective-permute-done.5.refs_5_ = bf16[128,1024]{1,0:T(8,128)(2,1)S(1)} collective-permute-done((bf16[128,1024]{1,0:T(8,128)(2,1)S(1)}, bf16[128,1024]{1,0:T(8,128)(2,1)S(1)}, u32[]{:S(2)}, u32[]{:S(2)}) %collective-permute-start.5) | collective-permute-done | bytes 262176 | tf_op jit(solution)/shard_map/ppermute | solution.py:614
  74.0 2.5 collective-permute-start.6
  78.2 4.2 %collective-permute-done.6.refs_6_ = bf16[128,1024]{1,0:T(8,128)(2,1)S(1)} collective-permute-done((bf16[128,1024]{1,0:T(8,128)(2,1)S(1)}, bf16[128,1024]{1,0:T(8,128)(2,1)S(1)}, u32[]{:S(2)}, u32[]{:S(2)}) %collective-permute-start.6) | collective-permute-done | bytes 262176 | tf_op jit(solution)/shard_map/ppermute | solution.py:614
  82.4 2.5 collective-permute-start.7
  84.9 1.9 collective-permute-start.8
  86.8 4.9 %collective-permute-done.7.refs_7_ = bf16[128,1024]{1,0:T(8,128)(2,1)S(1)} collective-permute-done((bf16[128,1024]{1,0:T(8,128)(2,1)S(1)}, bf16[128,1024]{1,0:T(8,128)(2,1)S(1)}, u32[]{:S(2)}, u32[]{:S(2)}) %collective-permute-start.7) | collective-permute-done | bytes 262176 | tf_op jit(solution)/shard_map/ppermute | solution.py:614
  92.5 1.3 copy-done.1
  93.8 1.3 copy-done.2
  95.7 10.0 %mix.1 = (bf16[8,4,2,256,128]{4,3,2,1,0:T(8,128)(2,1)}, f32[1,128]{1,0:T(1,128)}) custom-call(bf16[32,2,256,128]{3,2,1,0:T(8,128)(2,1)} %all-to-all-done.recv_hbm.recv_ref, bf16[1024,1024]{1,0:T(8,128)(2,1)} %copy-done.1, bf16[1024,1024]{1,0:T(8,128)(2,1)} %copy-done.2, f32[1,1024]{1,0:T(1,128)} %copy-done.6), custom_call_target="tpu_custom_call" | custom-call | flops 4294967296 | bytes 10485760 | tf_op jit(solution)/shard_map/mix/pallas_call | solution.py:296
  106.4 6.3 %weight_grads.1 = (bf16[136,1024]{1,0:T(8,128)(2,1)S(1)}, bf16[136,1024]{1,0:T(8,128)(2,1)S(1)}, bf16[136,1024]{1,0:T(8,128)(2,1)S(1)}, bf16[136,1024]{1,0:T(8,1...) custom-call(bf16[32,2,256,128]{3,2,1,0:T(8,128)(2,1)} %all-to-all-do, ...), custom_call_target="tpu_custom_call" | custom-call | flops 2147483648 | bytes 6291456 | tf_op jit(solution)/shard_map/weight_grads/pallas_call | solution.py:387
  112.7 2.2 collective-permute-start.10
  114.9 7.3 %collective-permute-done.9.refs_2_ = bf16[136,1024]{1,0:T(8,128)(2,1)S(1)} collective-permute-done((bf16[136,1024]{1,0:T(8,128)(2,1)S(1)}, bf16[136,1024]{1,0:T(8,128)(2,1)S(1)}, u32[]{:S(2)}, u32[]{:S(2)}) %collective-permute-start.9) | collective-permute-done | bytes 278560 | tf_op jit(solution)/shard_map/ppermute | solution.py:614
  122.2 1.3 collective-permute-done.10.refs_3_
  126.0 6.6 %collective-permute-done.11.refs_2_ = bf16[136,1024]{1,0:T(8,128)(2,1)S(1)} collective-permute-done((bf16[136,1024]{1,0:T(8,128)(2,1)S(1)}, bf16[136,1024]{1,0:T(8,128)(2,1)S(1)}, u32[]{:S(2)}, u32[]{:S(2)}) %collective-permute-start.11) | collective-permute-done | bytes 278560 | tf_op jit(solution)/shard_map/ppermute | solution.py:614
  132.6 1.3 collective-permute-done.12.refs_3_
  134.6 2.8 %collective-permute-start.13 = (bf16[136,1024]{1,0:T(8,128)(2,1)S(1)}, bf16[136,1024]{1,0:T(8,128)(2,1)S(1)}, u32[]{:S(2)}, u32[]{:S(2)}) collective-permute-start(bf16[136,1024]{1,0:T(8,128)(2,1)S(1)} %get-tuple-element.49), channel_id=1, source_target_pairs={{0,32},{32,64},{64,96},{96,128},{128,160},{160,192},{192,224},{224... | collective-permute-start | bytes 835592 | tf_op jit(solution)/shard_map/ppermute | solution.py:614
  137.4 5.1 %collective-permute-done.14.refs_1_ = bf16[136,1024]{1,0:T(8,128)(2,1)S(1)} collective-permute-done((bf16[136,1024]{1,0:T(8,128)(2,1)S(1)}, bf16[136,1024]{1,0:T(8,128)(2,1)S(1)}, u32[]{:S(2)}, u32[]{:S(2)}) %collective-permute-start.14) | collective-permute-done | bytes 278560 | tf_op jit(solution)/shard_map/ppermute | solution.py:614
  142.7 7.7 %collective-permute-done.15.refs_2_ = bf16[136,1024]{1,0:T(8,128)(2,1)S(1)} collective-permute-done((bf16[136,1024]{1,0:T(8,128)(2,1)S(1)}, bf16[136,1024]{1,0:T(8,128)(2,1)S(1)}, u32[]{:S(2)}, u32[]{:S(2)}) %collective-permute-start.15) | collective-permute-done | bytes 278560 | tf_op jit(solution)/shard_map/ppermute | solution.py:614
  150.5 24.2 %all_to_all.15.small_ref = f32[32,8,128]{2,1,0:T(8,128)S(1)} all-to-all(f32[32,8,128]{2,1,0:T(8,128)S(1)} %pack.1), channel_id=1, replica_groups=mesh['sp_0'=8,'sp_1'=4,'dp_0'=4,'dp_1'=2] {'dp_0','dp_1','sp_1'}, dimensions={0} | all-to-all | bytes 262144 | tf_op jit(solution)/shard_map/all_to_all | solution.py:611
  174.7 5.9 %all-to-all-start.1 = ((bf16[32,2,256,128]{3,2,1,0:T(8,128)(2,1)}), bf16[32,2,256,128]{3,2,1,0:T(8,128)(2,1)}, u32[]{:S(2)}, u32[]{:S(2)}) async-start(bf16[32,2,256,128]{3,2,1,0:T(8,128)(2,1)} %bitcast.21), calls=%async_computation.1 | async-start | bytes 8388608 | tf_op jit(solution)/shard_map/all_to_all | solution.py:611
  180.7 7.6 %slopes.1 = (bf16[256,4096]{1,0:T(8,128)(2,1)}, bf16[256,4096]{1,0:T(8,128)(2,1)}, bf16[256,4096]{1,0:T(8,128)(2,1)}) custom-call(bf16[256,4096]{1,0:T(8,128)(2,1)} %bitcast.18, bf16[256,4096]{1,0:T(8,128)(2,1)} %bitcast.20), custom_call_target="tpu_custom_call" | custom-call | flops 104857600 | bytes 16777216 | tf_op jit(solution)/shard_map/slopes/pallas_call | solution.py:160
  188.3 1.9 collective-permute-start.16
  190.9 17.5 %collective-permute-done.16 = bf16[128,1024]{1,0:T(8,128)(2,1)S(1)} collective-permute-done((bf16[128,1024]{1,0:T(8,128)(2,1)S(1)}, bf16[128,1024]{1,0:T(8,128)(2,1)S(1)}, u32[]{:S(2)}, u32[]{:S(2)}) %collective-permute-start.16) | collective-permute-done | bytes 262176 | tf_op jit(solution)/shard_map/ppermute | solution.py:642
  209.3 37.5 %all-to-all-done.1.recv_hbm = bf16[32,2,256,128]{3,2,1,0:T(8,128)(2,1)} async-done(((bf16[32,2,256,128]{3,2,1,0:T(8,128)(2,1)}), bf16[32,2,256,128]{3,2,1,0:T(8,128)(2,1)}, u32[]{:S(2)}, u32[]{:S(2)}) %all-to-all-start.1) | async-done | bytes 4194336 | tf_op jit(solution)/shard_map/all_to_all | solution.py:611
  246.8 8.3 %epilogue.1 = (bf16[256,4096]{1,0:T(8,128)(2,1)}, bf16[256,4096]{1,0:T(8,128)(2,1)}) custom-call(bf16[32,2,256,128]{3,2,1,0:T(8,128)(2,1)} %all-to-all-done.1.recv_hbm, bf16[256,4096]{1,0:T(8,128)(2,1)} %bitcast.16, bf16[256,4096]{1,0:T(8,128)(2,1)} %get-tuple-element.56.up_slope_hbm, bf16[256,4096]{1,0:T(8,128)(2,1)} %get-tuple-element.57.val_slope_hbm, ...), custom_call_target="tpu_custom_call" | custom-call | flops 20971520 | bytes 23068672 | tf_op jit(solution)/shard_map/epilogue/pallas_call | solution.py:575
  (34 shorter events, 9.2 us)
Async XLA Ops:
  8.7 7.9 %copy-start.4 = (bf16[1,128,1024]{2,1,0:T(8,128)(2,1)S(1)}, bf16[1,128,1024]{2,1,0:T(8,128)(2,1)}, u32[]{:S(2)}) copy-start(bf16[1,128,1024]{2,1,0:T(8,128)(2,1)} %param.9) | copy-start | bytes 786436
  8.7 76.2 %copy-start.5 = (f32[1,1024]{1,0:T(1,128)S(1)}, f32[1,1024]{1,0:T(1,128)}, u32[]{:S(2)}) copy-start(f32[1,1024]{1,0:T(1,128)} %param.10) | copy-start | bytes 12292
  8.7 86.4 %all-to-all-start = ((bf16[32,2,256,128]{3,2,1,0:T(8,128)(2,1)}), bf16[32,2,256,128]{3,2,1,0:T(8,128)(2,1)}, u32[]{:S(2)}, u32[]{:S(2)}) async-start(bf16[32,2,256,128]{3,2,1,0:T(8,128)(2,1)} %get-tuple-element.35), calls=%async_computation | async-start | bytes 8388608 | tf_op jit(solution)/shard_map/all_to_all | solution.py:611
  16.5 15.7 %collective-permute-start = (bf16[128,1024]{1,0:T(8,128)(2,1)S(1)}, bf16[128,1024]{1,0:T(8,128)(2,1)S(1)}, u32[]{:S(2)}, u32[]{:S(2)}) collective-permute-start(bf16[128,1024]{1,0:T(8,128)(2,1)S(1)} %bitcast.24), channel_id=1, source_target_pairs={{0,0},{1,32},{2,64},{3,96},{4,128},{5,160},{6,192},{7,224},{32,34}... | collective-permute-start | bytes 786440 | tf_op jit(solution)/shard_map/ppermute | solution.py:617
  32.2 10.1 %collective-permute-start.4 = (bf16[128,1024]{1,0:T(8,128)(2,1)S(1)}, bf16[128,1024]{1,0:T(8,128)(2,1)S(1)}, u32[]{:S(2)}, u32[]{:S(2)}) collective-permute-start(bf16[128,1024]{1,0:T(8,128)(2,1)S(1)} %collective-permute-done.refs_0_), channel_id=1, source_target_pairs={{0,224},{32,0},{64,32},{96,64},{128,96},{160,128},{192,160},{224,1... | collective-permute-start | bytes 786440 | tf_op jit(solution)/shard_map/ppermute | solution.py:614
  32.2 38.4 %collective-permute-start.1 = (bf16[128,1024]{1,0:T(8,128)(2,1)S(1)}, bf16[128,1024]{1,0:T(8,128)(2,1)S(1)}, u32[]{:S(2)}, u32[]{:S(2)}) collective-permute-start(bf16[128,1024]{1,0:T(8,128)(2,1)S(1)} %collective-permute-done.refs_0_), channel_id=1, source_target_pairs={{0,32},{32,64},{64,96},{96,128},{128,160},{160,192},{192,224},{224... | collective-permute-start | bytes 786440 | tf_op jit(solution)/shard_map/ppermute | solution.py:614
  42.3 31.7 %collective-permute-start.5 = (bf16[128,1024]{1,0:T(8,128)(2,1)S(1)}, bf16[128,1024]{1,0:T(8,128)(2,1)S(1)}, u32[]{:S(2)}, u32[]{:S(2)}) collective-permute-start(bf16[128,1024]{1,0:T(8,128)(2,1)S(1)} %collective-permute-done.4.refs_4_), channel_id=1, source_target_pairs={{0,224},{32,0},{64,32},{96,64},{128,96},{160,128},{192,160},{224,1... | collective-permute-start | bytes 786440 | tf_op jit(solution)/shard_map/ppermute | solution.py:614
  70.6 6.4 %collective-permute-start.2 = (bf16[128,1024]{1,0:T(8,128)(2,1)S(1)}, bf16[128,1024]{1,0:T(8,128)(2,1)S(1)}, u32[]{:S(2)}, u32[]{:S(2)}) collective-permute-start(bf16[128,1024]{1,0:T(8,128)(2,1)S(1)} %collective-permute-done.1.refs_1_), channel_id=1, source_target_pairs={{0,32},{32,64},{64,96},{96,128},{128,160},{160,192},{192,224},{224... | collective-permute-start | bytes 786440 | tf_op jit(solution)/shard_map/ppermute | solution.py:614
  74.0 8.4 %collective-permute-start.6 = (bf16[128,1024]{1,0:T(8,128)(2,1)S(1)}, bf16[128,1024]{1,0:T(8,128)(2,1)S(1)}, u32[]{:S(2)}, u32[]{:S(2)}) collective-permute-start(bf16[128,1024]{1,0:T(8,128)(2,1)S(1)} %collective-permute-done.5.refs_5_), channel_id=1, source_target_pairs={{0,224},{32,0},{64,32},{96,64},{128,96},{160,128},{192,160},{224,1... | collective-permute-start | bytes 786440 | tf_op jit(solution)/shard_map/ppermute | solution.py:614
  77.0 9.9 %collective-permute-start.3 = (bf16[128,1024]{1,0:T(8,128)(2,1)S(1)}, bf16[128,1024]{1,0:T(8,128)(2,1)S(1)}, u32[]{:S(2)}, u32[]{:S(2)}) collective-permute-start(bf16[128,1024]{1,0:T(8,128)(2,1)S(1)} %collective-permute-done.2.refs_2_), channel_id=1, source_target_pairs={{0,32},{32,64},{64,96},{96,128},{128,160},{160,192},{192,224},{224... | collective-permute-start | bytes 786440 | tf_op jit(solution)/shard_map/ppermute | solution.py:614
  82.4 9.3 %collective-permute-start.7 = (bf16[128,1024]{1,0:T(8,128)(2,1)S(1)}, bf16[128,1024]{1,0:T(8,128)(2,1)S(1)}, u32[]{:S(2)}, u32[]{:S(2)}) collective-permute-start(bf16[128,1024]{1,0:T(8,128)(2,1)S(1)} %collective-permute-done.6.refs_6_), channel_id=1, source_target_pairs={{0,224},{32,0},{64,32},{96,64},{128,96},{160,128},{192,160},{224,1... | collective-permute-start | bytes 786440 | tf_op jit(solution)/shard_map/ppermute | solution.py:614
  84.9 10.3 %collective-permute-start.8 = (f32[1,1024]{1,0:T(1,128)S(1)}, f32[1,1024]{1,0:T(1,128)S(1)}, u32[]{:S(2)}, u32[]{:S(2)}) collective-permute-start(f32[1,1024]{1,0:T(1,128)S(1)} %copy-done.5), channel_id=1, source_target_pairs={{0,0},{1,32},{2,64},{3,96},{4,128},{5,160},{6,192},{7,224},{32,34}... | collective-permute-start | bytes 12296 | tf_op jit(solution)/shard_map/ppermute | solution.py:616
  92.5 1.3 copy-start.1
  93.8 1.3 copy-start.2
  95.1 0.6 copy-start.6
  105.7 0.7 copy-start.3
  112.6 37.8 %copy-start = (f32[4096]{0:T(1024)S(1)}, f32[4096]{0:T(1024)}, u32[]{:S(2)}) copy-start(f32[4096]{0:T(1024)} %param.11) | copy-start | bytes 49156
  112.7 9.6 %collective-permute-start.9 = (bf16[136,1024]{1,0:T(8,128)(2,1)S(1)}, bf16[136,1024]{1,0:T(8,128)(2,1)S(1)}, u32[]{:S(2)}, u32[]{:S(2)}) collective-permute-start(bf16[136,1024]{1,0:T(8,128)(2,1)S(1)} %get-tuple-element.45), channel_id=1, source_target_pairs={{0,32},{32,64},{64,96},{96,128},{128,160},{160,192},{192,224},{224... | collective-permute-start | bytes 835592 | tf_op jit(solution)/shard_map/ppermute | solution.py:614
  112.7 10.8 %collective-permute-start.10 = (bf16[136,1024]{1,0:T(8,128)(2,1)S(1)}, bf16[136,1024]{1,0:T(8,128)(2,1)S(1)}, u32[]{:S(2)}, u32[]{:S(2)}) collective-permute-start(bf16[136,1024]{1,0:T(8,128)(2,1)S(1)} %get-tuple-element.46), channel_id=1, source_target_pairs={{0,224},{32,0},{64,32},{96,64},{128,96},{160,128},{192,160},{224,1... | collective-permute-start | bytes 835592 | tf_op jit(solution)/shard_map/ppermute | solution.py:614
  123.7 8.9 %collective-permute-start.11 = (bf16[136,1024]{1,0:T(8,128)(2,1)S(1)}, bf16[136,1024]{1,0:T(8,128)(2,1)S(1)}, u32[]{:S(2)}, u32[]{:S(2)}) collective-permute-start(bf16[136,1024]{1,0:T(8,128)(2,1)S(1)} %get-tuple-element.47), channel_id=1, source_target_pairs={{0,32},{32,64},{64,96},{96,128},{128,160},{160,192},{192,224},{224... | collective-permute-start | bytes 835592 | tf_op jit(solution)/shard_map/ppermute | solution.py:614
  124.7 9.2 %collective-permute-start.12 = (bf16[136,1024]{1,0:T(8,128)(2,1)S(1)}, bf16[136,1024]{1,0:T(8,128)(2,1)S(1)}, u32[]{:S(2)}, u32[]{:S(2)}) collective-permute-start(bf16[136,1024]{1,0:T(8,128)(2,1)S(1)} %get-tuple-element.48), channel_id=1, source_target_pairs={{0,224},{32,0},{64,32},{96,64},{128,96},{160,128},{192,160},{224,1... | collective-permute-start | bytes 835592 | tf_op jit(solution)/shard_map/ppermute | solution.py:614
  134.1 8.4 %collective-permute-start.14 = (bf16[136,1024]{1,0:T(8,128)(2,1)S(1)}, bf16[136,1024]{1,0:T(8,128)(2,1)S(1)}, u32[]{:S(2)}, u32[]{:S(2)}) collective-permute-start(bf16[136,1024]{1,0:T(8,128)(2,1)S(1)} %get-tuple-element.51), channel_id=1, source_target_pairs={{0,224},{32,0},{64,32},{96,64},{128,96},{160,128},{192,160},{224,1... | collective-permute-start | bytes 835592 | tf_op jit(solution)/shard_map/ppermute | solution.py:614
  134.6 8.1 %collective-permute-start.13 = (bf16[136,1024]{1,0:T(8,128)(2,1)S(1)}, bf16[136,1024]{1,0:T(8,128)(2,1)S(1)}, u32[]{:S(2)}, u32[]{:S(2)}) collective-permute-start(bf16[136,1024]{1,0:T(8,128)(2,1)S(1)} %get-tuple-element.49), channel_id=1, source_target_pairs={{0,32},{32,64},{64,96},{96,128},{128,160},{160,192},{192,224},{224... | collective-permute-start | bytes 835592 | tf_op jit(solution)/shard_map/ppermute | solution.py:614
  142.6 7.8 %collective-permute-start.15 = (bf16[136,1024]{1,0:T(8,128)(2,1)S(1)}, bf16[136,1024]{1,0:T(8,128)(2,1)S(1)}, u32[]{:S(2)}, u32[]{:S(2)}) collective-permute-start(bf16[136,1024]{1,0:T(8,128)(2,1)S(1)} %hop.5), channel_id=1, source_target_pairs={{0,224},{32,0},{64,32},{96,64},{128,96},{160,128},{192,160},{224,1... | collective-permute-start | bytes 835592 | tf_op jit(solution)/shard_map/ppermute | solution.py:614
  174.7 72.1 %all-to-all-start.1 = ((bf16[32,2,256,128]{3,2,1,0:T(8,128)(2,1)}), bf16[32,2,256,128]{3,2,1,0:T(8,128)(2,1)}, u32[]{:S(2)}, u32[]{:S(2)}) async-start(bf16[32,2,256,128]{3,2,1,0:T(8,128)(2,1)} %bitcast.21), calls=%async_computation.1 | async-start | bytes 8388608 | tf_op jit(solution)/shard_map/all_to_all | solution.py:611
  188.3 20.1 %collective-permute-start.16 = (bf16[128,1024]{1,0:T(8,128)(2,1)S(1)}, bf16[128,1024]{1,0:T(8,128)(2,1)S(1)}, u32[]{:S(2)}, u32[]{:S(2)}) collective-permute-start(bf16[128,1024]{1,0:T(8,128)(2,1)S(1)} %last.1), channel_id=1, source_target_pairs={{0,0},{32,1},{64,2},{96,3},{128,4},{160,5},{192,6},{224,7},{34,32}... | collective-permute-start | bytes 786440 | tf_op jit(solution)/shard_map/ppermute | solution.py:642
